TPU v7x, 128 devices: a whole 4x4x4 slice. The times are simulated.
128 devices in a mesh: sp: 16 (over z, y), tp: 8 (over x, core).
Axes of the slice: x: 4, y: 4, z: 4, core: 2. Of those that a mesh axis runs over, the one named last changes fastest.
Arguments:
- residual: bfloat16 [10240, 2048], P(('sp', 'tp')), may hold values from -6 to 6
- small_value_inputs: bfloat16 [10240, 1024], P('sp', 'tp'), may hold values from -6 to 6
- large_value_inputs: bfloat16 [10240, 1024], P('sp', 'tp'), may hold values from -6 to 6
- small_gate_inputs: bfloat16 [10240, 1024], P('sp', 'tp'), may hold values from -6 to 6
- large_gate_inputs: bfloat16 [10240, 1024], P('sp', 'tp'), may hold values from -6 to 6
- state_projections: bfloat16 [10240, 4, 128], P('sp'), may hold values from -6 to 6
- small_step_inputs: bfloat16 [10240, 16], P('sp', 'tp'), may hold values from -2.5 to 2.5
- large_step_inputs: bfloat16 [10240, 8], P('sp', 'tp'), may hold values from -2.5 to 2.5
- small_decay_offsets: float32 [10240, 16], P('sp', 'tp'), may hold values from -1.4 to 0
- large_decay_offsets: float32 [10240, 8], P('sp', 'tp'), may hold values from -1.4 to 0
- small_decay_rates: float32 [16], P('tp'), may hold values from -11.1 to -3.1
- large_decay_rates: float32 [8], P('tp'), may hold values from -11.1 to -3.1
- small_filter_taps: bfloat16 [4, 1024], P(None, 'tp'), may hold values from -3 to 3
- large_filter_taps: bfloat16 [4, 1024], P(None, 'tp'), may hold values from -3 to 3
- state_filter_taps: bfloat16 [4, 4, 128], replicated, may hold values from -3 to 3
- small_head_gains: float32 [1024], P('tp'), may hold values from 0.1 to 1.9
- large_head_gains: float32 [1024], P('tp'), may hold values from 0.1 to 1.9
- small_output_projection: bfloat16 [1024, 2048], P('tp'), may hold values from -0.125 to 0.125
- large_output_projection: bfloat16 [1024, 2048], P('tp'), may hold values from -0.125 to 0.125
- channel_norm_gain: float32 [2048], replicated, may hold values from 0.1 to 1.9
- gate_matrix: bfloat16 [2048, 5632], P('sp', 'tp'), may hold values from -0.125 to 0.125
- up_matrix: bfloat16 [2048, 5632], P('sp', 'tp'), may hold values from -0.125 to 0.125
- down_matrix: bfloat16 [5632, 2048], P('tp', 'sp'), may hold values from -0.078125 to 0.078125
Outputs:
- layer_out: bfloat16 [10240, 2048], P(('sp', 'tp'))
All inputs are finite; a program needn't handle non-finite values.
Results may differ from a plain program's by a relative error of at most 0.015.
Values may be sent and summed in bfloat16 or wider, within the bound.
A program may use at most 64 MiB of HBM per device.

v0:
```python
import jax
import jax.numpy as jnp
from jax import lax
from jax.sharding import Mesh
from jax.sharding import PartitionSpec as P

BLOCK = 64
SP = ("sp_0", "sp_1")
SP_TP = ("sp_0", "sp_1", "tp")


head_eps = 1e-05
row_eps = 1e-06


def side_by_side(arrays, axis, dim, along):
    ends, at = ([], 0)
    for a in arrays[:-1]:
        at += a.shape[along]
        ends.append(at)
    both = jnp.concatenate(arrays, axis=along)
    return tuple(jnp.split(lax.all_gather(both, axis, axis=dim, tiled=True), ends, axis=along))


def shifted(x, axis, by):
    size = lax.axis_size(axis)
    pairs = [(i, i + by) for i in range(size) if 0 <= i + by < size]
    return lax.ppermute(x, axis, pairs)


def nothing_yet(x, identity):
    return jax.tree.map(
        lambda part, zero: jnp.zeros_like(part) + jnp.asarray(zero, part.dtype), x, identity
    )


def gathered_once(x, axis):
    leaves = jax.tree.leaves(x)
    order = sorted(range(len(leaves)), key=lambda k: -leaves[k].size)
    width = (1, *leaves[order[0]].shape)[-1]
    lines = [
        jnp.pad(leaves[k].reshape(-1), (0, -leaves[k].size % width)).reshape(-1, width)
        for k in order
    ]
    both, at, found = (lax.all_gather(jnp.concatenate(lines), axis), 0, {})
    for k, line in zip(order, lines):
        slab = both[:, at : at + len(line)].reshape(len(both), -1)
        found[k] = slab[:, : leaves[k].size].reshape(-1, *leaves[k].shape)
        at += len(line)
    numbers = iter(range(len(leaves)))
    return jax.tree.map(lambda _: found[next(numbers)], x)


def prefix_by_axis(x, axes, combine, identity):
    before = start = nothing_yet(x, identity)
    so_far = x
    for axis in reversed(axes):
        size, here = (lax.axis_size(axis), lax.axis_index(axis))
        pieces = gathered_once(
            jax.tree.map(
                lambda part, kind: part.astype(kind),
                so_far,
                (jnp.bfloat16, jnp.bfloat16, jnp.bfloat16, jnp.bfloat16),
            ),
            axis,
        )
        inside, so_far = (start, start)
        for k in range(size):
            passed = k < here
            so_far = combine(
                so_far, jax.tree.map(lambda part, own: part[k].astype(own.dtype), pieces, x)
            )
            inside = jax.tree.map(lambda new, old: jnp.where(passed, new, old), so_far, inside)
        before = combine(inside, before)
    return before


def in_blocks(x, dim, size):
    before, after = (x.shape[:dim], x.shape[dim + 1 :])
    return jnp.moveaxis(x.reshape(*before, size, -1, *after), dim, 0)


def sum_at_owner(x, axis, dim):
    size = lax.axis_size(axis)
    pieces = lax.all_to_all(in_blocks(x, dim, size), axis, 0, 0, tiled=True)
    return jnp.sum(pieces.astype(jnp.float32), axis=0)


def copy_for_each(x, axis):
    copies = jnp.broadcast_to(x, (lax.axis_size(axis), *x.shape))
    return lax.all_to_all(copies, axis, split_axis=0, concat_axis=0, tiled=True)


def in_order(pieces, dim):
    pieces = jnp.moveaxis(pieces, 0, dim)
    shape = pieces.shape
    return pieces.reshape(*shape[:dim], shape[dim] * shape[dim + 1], *shape[dim + 2 :])


def gathered_copies(x, axis, dim):
    pieces = copy_for_each(x, axis)
    return in_order(pieces, dim)


def causal_conv(series, prior_tokens, filter_taps):
    width = filter_taps.shape[0]
    length = series.shape[0]
    padded = jnp.concatenate([prior_tokens.astype(jnp.float32), series.astype(jnp.float32)], axis=0)
    total = jnp.zeros(series.shape, jnp.float32)
    for offset in range(width):
        total = (
            total
            + filter_taps[offset].astype(jnp.float32)[None, :] * padded[offset : offset + length]
        )
    return jax.nn.silu(total)


def block_scan(driven, decay_logarithm, key_vectors, read_vectors, state):
    length, head_outputs, size = driven.shape
    blocks = length // BLOCK
    mask = jnp.tril(jnp.ones((BLOCK, BLOCK), dtype=bool))[:, :, None]

    def advance(carry, pieces):
        values, decays, key_rows, read_rows = pieces
        within = jnp.cumsum(decays, axis=0)
        spread = within[:, None, :] - within[None, :, :]
        weights = jnp.where(mask, jnp.exp(jnp.where(mask, spread, 0.0)), 0.0)
        scores = jnp.dot(read_rows, key_rows.T)
        inner = jnp.einsum("ls,lsh,shp->lhp", scores, weights, values)
        carried = jnp.einsum("ln,hpn,lh->lhp", read_rows, carry, jnp.exp(within))
        tail = jnp.exp(within[-1][None, :] - within)
        fresh = jnp.einsum("ln,lh,lhp->hpn", key_rows, tail, values)
        return (carry * jnp.exp(within[-1])[:, None, None] + fresh, inner + carried)

    pieces = (
        driven.reshape(blocks, BLOCK, head_outputs, size),
        decay_logarithm.reshape(blocks, BLOCK, head_outputs),
        key_vectors.reshape(blocks, BLOCK, key_vectors.shape[1]),
        read_vectors.reshape(blocks, BLOCK, read_vectors.shape[1]),
    )
    final, outs = lax.scan(advance, state, pieces)
    return (final, outs.reshape(length, head_outputs, size))


def device_heads(
    input_rows,
    prior_tokens,
    step_inputs,
    decay_offsets,
    decay_rates,
    filter_taps,
    key_vectors,
    read_vectors,
):
    length, width = input_rows.shape
    head_outputs = decay_rates.shape[0]
    size = width // head_outputs
    conv_values = causal_conv(input_rows, prior_tokens, filter_taps)
    step_amount = jax.nn.softplus(step_inputs.astype(jnp.float32))
    decay_logarithm = -jnp.exp(decay_rates)[None, :] * step_amount + decay_offsets
    driven = conv_values.reshape(length, head_outputs, size) * step_amount[:, :, None]
    start_state = jnp.zeros((head_outputs, size, key_vectors.shape[1]), jnp.float32)
    final, local_out = block_scan(driven, decay_logarithm, key_vectors, read_vectors, start_state)
    running = jnp.cumsum(decay_logarithm, axis=0)
    return (local_out, final, jnp.exp(running[-1]), jnp.exp(running))


def finish_heads(local, incoming, read_vectors, gate_inputs, head_gains):
    local_out, final, total, growth = local
    length, head_outputs, size = local_out.shape
    scan_out = local_out + jnp.einsum("tn,hpn,th->thp", read_vectors, incoming, growth)
    gated = scan_out * jax.nn.silu(
        gate_inputs.reshape(length, head_outputs, size).astype(jnp.float32)
    )
    scale = lax.rsqrt(jnp.mean(gated * gated, axis=-1, keepdims=True) + head_eps)
    normed = gated * scale * head_gains.reshape(head_outputs, size)
    return normed.reshape(length, head_outputs * size).astype(jnp.bfloat16)


def chain(earlier, later):
    return (
        earlier[0] * later[0],
        earlier[1] * later[0][:, None, None] + later[1],
        earlier[2] * later[2],
        earlier[3] * later[2][:, None, None] + later[3],
    )


def row_norm(rows, gain):
    wide = rows.astype(jnp.float32)
    scale = lax.rsqrt(jnp.mean(wide * wide, axis=-1, keepdims=True) + row_eps)
    return (wide * scale * gain[None, :]).astype(jnp.bfloat16)


def expand_late(normed_all, gate_matrix, up_matrix):
    pieces = side_by_side((gate_matrix, up_matrix), SP, 0, 1)
    gate = jnp.dot(normed_all, pieces[0], preferred_element_type=jnp.float32)
    up = jnp.dot(normed_all, pieces[1], preferred_element_type=jnp.float32)
    return (jax.nn.silu(gate) * up).astype(jnp.bfloat16)


def on_device(
    residual,
    small_value_inputs,
    large_value_inputs,
    small_gate_inputs,
    large_gate_inputs,
    state_projections,
    small_step_inputs,
    large_step_inputs,
    small_decay_offsets,
    large_decay_offsets,
    small_decay_rates,
    large_decay_rates,
    small_filter_taps,
    large_filter_taps,
    state_filter_taps,
    small_head_gains,
    large_head_gains,
    small_output_projection,
    large_output_projection,
    channel_norm_gain,
    gate_matrix,
    up_matrix,
    down_matrix,
):
    margin = state_filter_taps.shape[0] - 1
    length = small_value_inputs.shape[0]
    planes = state_projections.shape[1] * state_projections.shape[2]
    flat = state_projections.reshape(length, planes)
    before_small, before_large, before_state = shifted(
        (
            small_value_inputs[length - margin :],
            large_value_inputs[length - margin :],
            flat[length - margin :],
        ),
        SP,
        1,
    )
    convolved_state_maps = causal_conv(
        flat, before_state, state_filter_taps.reshape(margin + 1, planes)
    )
    convolved_state_maps = convolved_state_maps.reshape(
        length, state_projections.shape[1], state_projections.shape[2]
    )
    small = device_heads(
        small_value_inputs,
        before_small,
        small_step_inputs,
        small_decay_offsets,
        small_decay_rates,
        small_filter_taps,
        convolved_state_maps[:, 0],
        convolved_state_maps[:, 1],
    )
    large = device_heads(
        large_value_inputs,
        before_large,
        large_step_inputs,
        large_decay_offsets,
        large_decay_rates,
        large_filter_taps,
        convolved_state_maps[:, 2],
        convolved_state_maps[:, 3],
    )
    identity = (
        jnp.ones_like(small[2]),
        jnp.zeros_like(small[1]),
        jnp.ones_like(large[2]),
        jnp.zeros_like(large[1]),
    )
    carried = prefix_by_axis((small[2], small[1], large[2], large[1]), SP, chain, identity)
    small_head_outputs = finish_heads(
        small, carried[1], convolved_state_maps[:, 1], small_gate_inputs, small_head_gains
    )
    large_head_outputs = finish_heads(
        large, carried[3], convolved_state_maps[:, 3], large_gate_inputs, large_head_gains
    )
    mixed = sum_at_owner(
        (
            jnp.dot(small_head_outputs, small_output_projection, preferred_element_type=jnp.float32)
            + jnp.dot(
                large_head_outputs, large_output_projection, preferred_element_type=jnp.float32
            )
        ).astype(jnp.bfloat16),
        "tp",
        0,
    )
    middle = (residual.astype(jnp.float32) + mixed).astype(jnp.bfloat16)
    normed = row_norm(middle, channel_norm_gain)
    normed_all = gathered_copies(normed, "tp", 0)
    hidden = expand_late(normed_all, gate_matrix, up_matrix)
    partial_sums = jnp.dot(
        hidden,
        lax.all_gather(down_matrix, SP, axis=1, tiled=True),
        preferred_element_type=jnp.float32,
    )
    down = sum_at_owner(partial_sums.astype(jnp.bfloat16), "tp", 0)
    return (middle.astype(jnp.float32) + down).astype(jnp.bfloat16)


def solution(mesh):
    split = Mesh(mesh.devices.reshape(4, 4, mesh.shape["tp"]), ("sp_0", "sp_1", "tp"))
    in_specs = (
        P(SP_TP, None),
        P(SP, "tp"),
        P(SP, "tp"),
        P(SP, "tp"),
        P(SP, "tp"),
        P(SP, None, None),
        P(SP, "tp"),
        P(SP, "tp"),
        P(SP, "tp"),
        P(SP, "tp"),
        P("tp"),
        P("tp"),
        P(None, "tp"),
        P(None, "tp"),
        P(),
        P("tp"),
        P("tp"),
        P("tp", None),
        P("tp", None),
        P(),
        P(SP, "tp"),
        P(SP, "tp"),
        P("tp", SP),
    )
    out_specs = P(SP_TP, None)
    return jax.shard_map(
        on_device, mesh=split, in_specs=in_specs, out_specs=out_specs, check_vma=False
    )
```

profile of v0, /device:TPU:1, one launch (start us, length us, event | category | flops | bytes accessed | tf_op | source)
XLA Modules:
  0.0 302.6 jit_solution(8511046870527017675)
XLA Ops:
  6.5 0.8 slice.293
  7.5 4.0 %collective-permute-start.1 = (bf16[3,512]{0,1:T(8,128)(2,1)S(1)}, bf16[3,512]{0,1:T(8,128)(2,1)S(1)}, u32[]{:S(2)}, u32[]{:S(2)}) collective-permute-start(bf16[3,512]{0,1:T(8,128)(2,1)S(1)} %bitcast.379), channel_id=1, source_target_pairs={{0,8},{8,16},{16,24},{24,32},{32,40},{40,48},{48,56},{56,64},{64,7... | collective-permute-start | bytes 9224 | tf_op jit(solution)/shard_map/ppermute | solution.py:28
  11.5 0.7 slice.306
  12.2 0.7 copy.118
  13.0 3.8 %collective-permute-start.2 = (bf16[3,128]{0,1:T(8,128)(2,1)}, bf16[3,128]{0,1:T(8,128)(2,1)}, u32[]{:S(2)}, u32[]{:S(2)}) collective-permute-start(bf16[3,128]{0,1:T(8,128)(2,1)} %copy.118), channel_id=1, source_target_pairs={{0,8},{8,16},{16,24},{24,32},{32,40},{40,48},{48,56},{56,64},{64,7... | collective-permute-start | bytes 2312 | tf_op jit(solution)/shard_map/ppermute | solution.py:28
  16.8 0.7 slice.285
  17.7 2.4 collective-permute-start
  20.1 1.8 pad_maximum_fusion.1
  21.9 1.8 copy.112
  33.8 0.7 convert_element_type.414
  34.6 0.9 copy.129
  35.5 0.8 copy.127
  36.3 0.9 copy.125
  38.8 1.8 broadcast_multiply_fusion
  40.6 0.8 convert_element_type.413
  41.4 2.0 multiply_multiply_fusion
  43.4 0.9 copy.120
  44.3 2.4 divide_multiply_fusion
  46.9 0.8 copy.122
  48.1 13.2 %while.28 = (s32[]{:T(128)}, f32[2,64,128]{2,1,0:T(8,128)S(1)}, f32[10,64,2,64]{3,1,0,2:T(8,128)S(1)}, f32[10,64,2]{1,0,2:T(8,128)S(1)}, f32[10,64,2,64]{3,2,1,0...) while((s32[]{:T(128)}, f32[2,64,128]{2,1,0:T(8,128)S(1)}, ...), condition=%wide.region_2.3_spmd.clone.clone, body=%wide.region_0.2_spmd.clone.clone.sunk | while | flops 6426627 | bytes 643752 | solution.py:141
  61.3 62.7 %while.29 = (s32[]{:T(128)}, f32[1,128,128]{2,1,0:T(8,128)S(1)}, f32[10,64,1,128]{3,1,2,0:T(8,128)}, f32[10,64,1]{1,2,0:T(1,128)}, f32[10,64,1,128]{3,2,1,0:T(1,...) while((s32[]{:T(128)}, f32[1,128,128]{2,1,0:T(8,128)S(1)}, ...), condition=%wide.region_7.8_spmd.clone.clone, body=%wide.region_5.7_spmd.clone.clone.sunk | while | flops 6410243 | bytes 498340 | solution.py:141
  62.3 0.8 constant_dynamic-slice_fusion.9
  63.1 1.0 fusion.267
  65.2 1.5 fusion.268
  68.5 0.8 constant_dynamic-slice_fusion.9
  69.3 1.0 fusion.267
  71.4 1.5 fusion.268
  74.8 0.8 constant_dynamic-slice_fusion.9
  75.6 1.0 fusion.267
  77.7 1.5 fusion.268
  81.1 0.8 constant_dynamic-slice_fusion.9
  81.9 1.0 fusion.267
  84.0 1.5 fusion.268
  87.3 0.8 constant_dynamic-slice_fusion.9
  88.1 1.0 fusion.267
  90.2 1.5 fusion.268
  93.6 0.8 constant_dynamic-slice_fusion.9
  94.4 1.0 fusion.267
  96.5 1.5 fusion.268
  99.9 0.8 constant_dynamic-slice_fusion.9
  100.7 1.0 fusion.267
  102.8 1.5 fusion.268
  106.2 0.8 constant_dynamic-slice_fusion.9
  106.9 1.0 fusion.267
  109.1 1.5 fusion.268
  112.5 0.8 constant_dynamic-slice_fusion.9
  113.2 1.0 fusion.267
  115.4 1.5 fusion.268
  118.7 0.8 constant_dynamic-slice_fusion.9
  119.5 1.0 fusion.267
  121.7 1.5 fusion.268
  124.2 10.1 %all-gather.2 = bf16[4,258,128]{2,1,0:T(8,128)(2,1)S(1)} all-gather(bf16[1,258,128]{2,1,0:T(8,128)(2,1)S(1)} %maximum_bitcast_fusion), channel_id=2, replica_groups=mesh['sp_0'=4,'sp_1'=4,'tp'=8] {'sp_1'}, dimensions={0}, use_global_device_ids=true | all-gather | bytes 330240 | tf_op jit(solution)/shard_map/all_gather | solution.py:45
  139.0 10.9 %all-gather.3 = bf16[4,258,128]{2,1,0:T(8,128)(2,1)S(1)} all-gather(bf16[1,258,128]{2,1,0:T(8,128)(2,1)S(1)} %maximum_bitcast_fusion.1), channel_id=3, replica_groups=mesh['sp_0'=4,'sp_1'=4,'tp'=8] {'sp_0'}, dimensions={0}, use_global_device_ids=true | all-gather | bytes 330240 | tf_op jit(solution)/shard_map/all_gather | solution.py:45
  153.3 1.0 copy.124
  156.6 0.9 fusion.212
  157.7 2.5 add_convert_fusion
  160.2 11.3 %all-to-all-start = ((bf16[8,80,2048]{2,1,0:T(8,128)(2,1)}), bf16[8,80,2048]{2,1,0:T(8,128)(2,1)S(1)}, u32[]{:S(2)}, u32[]{:S(2)}) async-start(bf16[8,80,2048]{2,1,0:T(8,128)(2,1)} %bitcast.359), calls=%async_computation | async-start | bytes 5242880 | tf_op jit(solution)/shard_map/all_to_all | solution.py:85
  171.5 0.7 all-gather.9.cloned.1.call-update
  172.2 31.1 %all-to-all-done = bf16[8,80,2048]{2,1,0:T(8,128)(2,1)S(1)} async-done(((bf16[8,80,2048]{2,1,0:T(8,128)(2,1)}), bf16[8,80,2048]{2,1,0:T(8,128)(2,1)S(1)}, u32[]{:S(2)}, u32[]{:S(2)}) %all-to-all-start) | async-done | bytes 2621472 | tf_op jit(solution)/shard_map/all_to_all | solution.py:85
  204.5 35.2 %all_to_all.15 = bf16[8,80,2048]{2,1,0:T(8,128)(2,1)S(1)} all-to-all(bf16[8,80,2048]{2,1,0:T(8,128)(2,1)S(1)} %broadcast_in_dim.52), channel_id=1, replica_groups=mesh['sp_0'=4,'sp_1'=4,'tp'=8] {'tp'}, dimensions={0} | all-to-all | bytes 5242880 | tf_op jit(solution)/shard_map/all_to_all | solution.py:91
  239.7 5.5 %fusion.79 = f32[640,704]{0,1:T(8,128)} fusion(bf16[640,2048]{1,0:T(8,128)(2,1)S(1)} %bitcast.363, bf16[2048,1408]{0,1:T(8,128)(2,1)} %all-gather.7.cloned.1.call-done), kind=kOutput, calls=%fused_computation.91 | convolution fusion | flops 1845493760 | bytes 7307264 | tf_op jit(solution)/shard_map/dot_general | solution.py:197
  245.2 12.9 %convolution_convert_fusion = bf16[640,2048]{1,0:T(8,128)(2,1)} fusion(bf16[704,2048]{1,0:T(8,128)(2,1)} %all-gather.9.cloned.1.call-done, f32[640,704]{0,1:T(8,128)} %fusion.79, bf16[640,2048]{1,0:T(8,128)(2,1)S(1)} %bitcast.364, bf16[2048,1408]{0,1:T(8,128)(2,1)} %all-gather.7.cloned.1.call-done), kind=kOutput, calls=%fused_computation.88 | convolution fusion | flops 3695001600 | bytes 12812288 | tf_op jit(solution)/shard_map/dot_general | solution.py:293
  258.1 36.4 %all_to_all.16 = bf16[8,80,2048]{2,1,0:T(8,128)(2,1)S(1)} all-to-all(bf16[8,80,2048]{2,1,0:T(8,128)(2,1)} %bitcast.365), channel_id=1, replica_groups=mesh['sp_0'=4,'sp_1'=4,'tp'=8] {'tp'}, dimensions={0} | all-to-all | bytes 5242880 | tf_op jit(solution)/shard_map/all_to_all | solution.py:85
  295.0 0.8 fusion.101
  (380 shorter events, 52.6 us)
Async XLA Ops:
  6.5 150.1 %copy-start = (bf16[128,2048]{1,0:T(8,128)(2,1)S(1)}, bf16[128,2048]{1,0:T(8,128)(2,1)}, u32[]{:S(2)}) copy-start(bf16[128,2048]{1,0:T(8,128)(2,1)} %param.44) | copy-start | bytes 1572868
  6.5 17.2 %copy-start.7 = (bf16[640,128]{1,0:T(8,128)(2,1)S(1)}, bf16[640,128]{1,0:T(8,128)(2,1)}, u32[]{:S(2)}) copy-start(bf16[640,128]{1,0:T(8,128)(2,1)} %param.29) | copy-start | bytes 491524
  6.5 17.4 %copy-start.8 = (bf16[640,128]{1,0:T(8,128)(2,1)S(1)}, bf16[640,128]{1,0:T(8,128)(2,1)}, u32[]{:S(2)}) copy-start(bf16[640,128]{1,0:T(8,128)(2,1)} %param.28) | copy-start | bytes 491524
  6.5 233.2 %all-gather.7.cloned.1.call-start = ((), (), s32[]{:S(2)}) async-start(), calls=%async_computation.3 | async-start | bytes 6127616 | tf_op jit(solution)/shard_map/all_gather | solution.py:22
  7.5 36.8 %collective-permute-start.1 = (bf16[3,512]{0,1:T(8,128)(2,1)S(1)}, bf16[3,512]{0,1:T(8,128)(2,1)S(1)}, u32[]{:S(2)}, u32[]{:S(2)}) collective-permute-start(bf16[3,512]{0,1:T(8,128)(2,1)S(1)} %bitcast.379), channel_id=1, source_target_pairs={{0,8},{8,16},{16,24},{24,32},{32,40},{40,48},{48,56},{56,64},{64,7... | collective-permute-start | bytes 9224 | tf_op jit(solution)/shard_map/ppermute | solution.py:28
  13.0 27.6 %collective-permute-start.2 = (bf16[3,128]{0,1:T(8,128)(2,1)}, bf16[3,128]{0,1:T(8,128)(2,1)}, u32[]{:S(2)}, u32[]{:S(2)}) collective-permute-start(bf16[3,128]{0,1:T(8,128)(2,1)} %copy.118), channel_id=1, source_target_pairs={{0,8},{8,16},{16,24},{24,32},{32,40},{40,48},{48,56},{56,64},{64,7... | collective-permute-start | bytes 2312 | tf_op jit(solution)/shard_map/ppermute | solution.py:28
  17.6 7.2 %copy-start.19 = (f32[640,1]{0,1:T(1,128)S(1)}, f32[640,1]{0,1:T(1,128)}, u32[]{:S(2)}) copy-start(f32[640,1]{0,1:T(1,128)} %param.36) | copy-start | bytes 7684
  17.6 7.2 %copy-start.20 = (bf16[640,1]{0,1:T(2,128)(2,1)S(1)}, bf16[640,1]{0,1:T(2,128)(2,1)}, u32[]{:S(2)}) copy-start(bf16[640,1]{0,1:T(2,128)(2,1)} %param.34) | copy-start | bytes 3844
  17.6 9.9 %copy-start.15 = (bf16[4,4,128]{2,1,0:T(4,128)(2,1)S(1)}, bf16[4,4,128]{2,1,0:T(4,128)(2,1)}, u32[]{:S(2)}) copy-start(bf16[4,4,128]{2,1,0:T(4,128)(2,1)} %param.41) | copy-start | bytes 12292
  17.6 10.5 %copy-start.17 = (bf16[4,128]{1,0:T(4,128)(2,1)S(1)}, bf16[4,128]{1,0:T(4,128)(2,1)}, u32[]{:S(2)}) copy-start(bf16[4,128]{1,0:T(4,128)(2,1)} %param.40) | copy-start | bytes 3076
  17.6 11.1 %copy-start.18 = (bf16[4,128]{1,0:T(4,128)(2,1)S(1)}, bf16[4,128]{1,0:T(4,128)(2,1)}, u32[]{:S(2)}) copy-start(bf16[4,128]{1,0:T(4,128)(2,1)} %param.39) | copy-start | bytes 3076
  17.6 11.1 %copy-start.26 = (f32[2]{0:T(128)S(1)}, f32[2]{0:T(128)}, u32[]{:S(2)}) copy-start(f32[2]{0:T(128)} %param.37) | copy-start | bytes 28
  17.6 11.1 %copy-start.13 = (f32[640,2]{0,1:T(2,128)S(1)}, f32[640,2]{0,1:T(2,128)}, u32[]{:S(2)}) copy-start(f32[640,2]{0,1:T(2,128)} %param.35) | copy-start | bytes 15364
  17.6 11.1 %copy-start.21 = (bf16[640,2]{0,1:T(2,128)(2,1)S(1)}, bf16[640,2]{0,1:T(2,128)(2,1)}, u32[]{:S(2)}) copy-start(bf16[640,2]{0,1:T(2,128)(2,1)} %param.33) | copy-start | bytes 7684
  17.7 20.1 %collective-permute-start = (bf16[3,128]{0,1:T(8,128)(2,1)S(1)}, bf16[3,128]{0,1:T(8,128)(2,1)S(1)}, u32[]{:S(2)}, u32[]{:S(2)}) collective-permute-start(bf16[3,128]{0,1:T(8,128)(2,1)S(1)} %copy.107), channel_id=1, source_target_pairs={{0,8},{8,16},{16,24},{24,32},{32,40},{40,48},{48,56},{56,64},{64,7... | collective-permute-start | bytes 2312 | tf_op jit(solution)/shard_map/ppermute | solution.py:28
  21.9 13.6 %copy-start.9 = (bf16[640,128]{1,0:T(8,128)(2,1)S(1)}, bf16[640,128]{1,0:T(8,128)(2,1)}, u32[]{:S(2)}) copy-start(bf16[640,128]{1,0:T(8,128)(2,1)} %param.31) | copy-start | bytes 491524
  21.9 14.4 %copy-start.11 = (bf16[640,128]{1,0:T(8,128)(2,1)S(1)}, bf16[640,128]{1,0:T(8,128)(2,1)}, u32[]{:S(2)}) copy-start(bf16[640,128]{1,0:T(8,128)(2,1)} %param.30) | copy-start | bytes 491524
  23.7 13.4 %copy-start.27 = (f32[128]{0:T(128)S(1)}, f32[128]{0:T(128)}, u32[]{:S(2)}) copy-start(f32[128]{0:T(128)} %param.42) | copy-start | bytes 1540
  46.7 1.4 copy-start.1
  61.3 62.8 %copy-start.22 = (bf16[1,128]{1,0:T(2,128)(2,1)S(1)}, bf16[1,128]{1,0:T(2,128)(2,1)}, u32[]{:S(2)}) copy-start(bf16[1,128]{1,0:T(2,128)(2,1)} %get-tuple-element.323) | copy-start | bytes 772
  61.3 62.8 %copy-start.23 = (bf16[1,128]{1,0:T(2,128)(2,1)S(1)}, bf16[1,128]{1,0:T(2,128)(2,1)}, u32[]{:S(2)}) copy-start(bf16[1,128]{1,0:T(2,128)(2,1)} %get-tuple-element.324) | copy-start | bytes 772
  124.1 28.3 %copy-start.3 = (f32[10,64,1,128]{3,1,2,0:T(8,128)S(1)}, f32[10,64,1,128]{3,1,2,0:T(8,128)}, u32[]{:S(2)}) copy-start(f32[10,64,1,128]{3,1,2,0:T(8,128)} %get-tuple-element.100) | copy-start | bytes 983044
  124.1 31.6 %copy-start.10 = (bf16[640,128]{0,1:T(8,128)(2,1)S(1)}, bf16[640,128]{0,1:T(8,128)(2,1)}, u32[]{:S(2)}) copy-start(bf16[640,128]{0,1:T(8,128)(2,1)} %copy.127) | copy-start | bytes 491524
  124.1 31.6 %copy-start.16 = (f32[640]{0:T(1024)S(1)}, f32[640]{0:T(1024)}, u32[]{:S(2)}) copy-start(f32[640]{0:T(1024)} %fusion.193) | copy-start | bytes 7684
  153.3 2.8 copy-start.4
  153.3 2.9 copy-start.14
  154.3 1.9 copy-start.6
  155.9 0.6 copy-start.24
  156.6 1.0 copy-start.2
  156.6 1.0 copy-start.25
  160.2 43.1 %all-to-all-start = ((bf16[8,80,2048]{2,1,0:T(8,128)(2,1)}), bf16[8,80,2048]{2,1,0:T(8,128)(2,1)S(1)}, u32[]{:S(2)}, u32[]{:S(2)}) async-start(bf16[8,80,2048]{2,1,0:T(8,128)(2,1)} %bitcast.359), calls=%async_computation | async-start | bytes 5242880 | tf_op jit(solution)/shard_map/all_to_all | solution.py:85
  171.5 32.3 %copy-start.5 = (bf16[80,2048]{1,0:T(8,128)(2,1)S(1)}, bf16[80,2048]{1,0:T(8,128)(2,1)}, u32[]{:S(2)}) copy-start(bf16[80,2048]{1,0:T(8,128)(2,1)} %param.27) | copy-start | bytes 983044
  171.5 73.7 %all-gather.9.cloned.1.call-start = ((), (), s32[]{:S(2)}) async-start(), calls=%async_computation.4 | async-start | bytes 3063808 | tf_op jit(solution)/shard_map/all_gather | solution.py:295
  172.2 31.8 %copy-start.12 = (f32[2048]{0:T(1024)S(1)}, f32[2048]{0:T(1024)}, u32[]{:S(2)}) copy-start(f32[2048]{0:T(1024)} %param.46) | copy-start | bytes 24580
Sparse Core Ops, SparseCore 0:
  22.0 66.3 all-gather.6
  174.4 48.5 all-gather.8
where the time goes:
time: 305 us; the launch traced here: 303 us
  blocking collectives  92.5 us (30%)
  matrix products  56.9 us (19%)
  local copies, waits for them, and re-layouts  43.7 us (14%)
  waiting for transfers between devices  31.8 us (10%)
  other arithmetic  26.2 us (9%)
  between operations  22.5 us (7%)
  starting transfers between devices  21.6 us (7%)
  loops' own time  7.43 us (2%)
    all_to_all x1, blocking collectives, sum_at_owner(): pieces = lax.all_to_all(in_blocks(x, dim, size), axis, 0, 0, tiled=True)  36.4 us
    all_to_all x1, blocking collectives, copy_for_each(): return lax.all_to_all(copies, axis, split_axis=0, concat_axis=0, tiled=True)  35.2 us
    all_to_all x1, waiting for transfers between devices, sum_at_owner(): pieces = lax.all_to_all(in_blocks(x, dim, size), axis, 0, 0, tiled=True)  31.1 us
    all_gather x2, blocking collectives, gathered_once(): both, at, found = (lax.all_gather(jnp.concatenate(lines), axis), 0, {})  20.9 us
    dot_general x20, matrix products, advance(): carried = jnp.einsum('ln,hpn,lh->lhp', read_rows, carry, jnp.exp(within))  16.2 us
    dot_general x1, matrix products, on_device(): jnp.dot(hidden, lax.all_gather(down_matrix, SP, axis=1, tiled=True), pref...  12.9 us
    dot_general x20, matrix products, advance(): inner = jnp.einsum('ls,lsh,shp->lhp', scores, weights, values)  11.8 us
    all_to_all x1, starting transfers between devices, sum_at_owner(): pieces = lax.all_to_all(in_blocks(x, dim, size), axis, 0, 0, tiled=True)  11.3 us
  transfers between devices with their start and end apart: 6, of which 1 were waited for; matrix products, arithmetic and copies ran while one was open for 37% of the time, Pallas kernels for 0%

commit v1 on v0

v1 whole, which is shorter than its diff:
```python
import jax
import jax.numpy as jnp
from jax import lax
from jax.experimental import pallas as pl
from jax.experimental.pallas import tpu as pltpu
from jax.sharding import Mesh
from jax.sharding import PartitionSpec as P

F32 = jnp.float32
BF16 = jnp.bfloat16
SP = ("z", "y")
TP = ("x", "c")
SP_TP = ("z", "y", "x", "c")

T = 640
L = 128
NB = T // L
R = 80
FD = 704
DM = 2048
H = 1024
KROWS = 128
CUT = 352

head_eps = 1e-05
row_eps = 1e-06


def silu(x):
    return x / (1.0 + jnp.exp(-x))


def dot(a, b):
    return jnp.dot(a, b, preferred_element_type=F32)


def dot_nt(a, b):
    return lax.dot_general(a, b, (((1,), (1,)), ((), ())), preferred_element_type=F32)


def dot_tn(a, b):
    return lax.dot_general(a, b, (((0,), (0,)), ((), ())), preferred_element_type=F32)


def kernel(
    res_in, vs_in, vl_in, gs_in, gl_in, sp_in, ws_in, wl_in, g_in, u_in, d_in,
    meta, taps_s, taps_l, taps_m, gain_s, gain_l, gain_n,
    out,
    xin, gin, resv, halo, cbuf, conv_k, drive, fresh, inner, heads, hpart, lhs,
    wo, wg, wu, wd, st1, st2, psend, rp, rm, ag, hid, psend2, rp2, rm2, midv,
    loc_sem, halo_sem, w_send, w_recv, pair_sem, st_sem, hp_sem, rs_sem, ag_sem, rs2_sem,
):
    z, y, x, c = (lax.axis_index(n) for n in ("z", "y", "x", "c"))
    rem = lax.rem
    o = 1 - c

    def at(base, by):
        return rem(base + (by % 4), 4)

    last = y == 3
    first = y == 0
    nxt = {"z": rem(z + lax.div(y + 1, 4), 4), "y": rem(y + 1, 4)}
    prv = {"z": rem(z + 3 + lax.div(y + 3, 4), 4), "y": rem(y + 3, 4)}

    def there(**kw):
        base = {"z": z, "y": y, "x": x, "c": c}
        base.update(kw)
        return (base["z"], base["y"], base["x"], base["c"])

    def remote(src, dst, send, recv, **kw):
        return pltpu.make_async_remote_copy(
            src_ref=src, dst_ref=dst, send_sem=send, recv_sem=recv,
            device_id=there(**kw), device_id_type=pl.DeviceIdType.MESH,
        )

    pending = []

    def go(cp):
        cp.start()
        pending.append(cp)
        return cp

    def yl(i):
        return pl.ds(pl.multiple_of(i * 128, 128), 128)

    local = [
        (vs_in, xin.at[:, pl.ds(0, 128)]),
        (vl_in, xin.at[:, pl.ds(128, 128)]),
        (sp_in, xin.at[:, pl.ds(256, 512)]),
        (gs_in, gin.at[:, pl.ds(0, 128)]),
        (gl_in, gin.at[:, pl.ds(128, 128)]),
        (res_in, resv),
        (ws_in, wo.at[c, pl.ds(0, 128)]),
        (wl_in, wo.at[c, pl.ds(128, 128)]),
        (g_in, wg.at[c, z, y]),
        (u_in, wu.at[c, z, y]),
        (d_in, wd.at[c, z, :, yl(y)]),
    ]
    local = [pltpu.make_async_copy(a, b, loc_sem.at[i]) for i, (a, b) in enumerate(local)]
    for cp in local:
        cp.start()

    barrier = pltpu.get_barrier_semaphore()
    peers = [
        dict(c=o), dict(x=at(x, 1)), dict(x=at(x, 3)),
        dict(y=at(y, 1)), dict(y=at(y, 2)), dict(y=at(y, 3)),
        dict(z=at(z, 1)), dict(z=at(z, 2)), dict(z=at(z, 3)),
        nxt, prv,
    ]
    for p in peers:
        pl.semaphore_signal(barrier, inc=1, device_id=there(**p), device_id_type=pl.DeviceIdType.MESH)
    pl.semaphore_wait(barrier, len(peers))

    tail = pl.ds(T - 16, 16)
    halos = [
        go(remote(src.at[tail], halo.at[:, cols], halo_sem.at[0, i], halo_sem.at[1, i], **nxt))
        for i, (src, cols) in enumerate(
            ((vs_in, pl.ds(0, 128)), (vl_in, pl.ds(128, 128)), (sp_in, pl.ds(256, 512)))
        )
    ]

    names = ("G", "U", "A", "B")
    own_src = {
        "G": g_in, "U": u_in,
        "A": d_in.at[pl.ds(0, CUT)], "B": d_in.at[pl.ds(CUT, CUT)],
    }

    def unit(name, rz, ry):
        zz, yy = at(z, rz), at(y, ry)
        if name == "G":
            return wg.at[c, zz, yy]
        if name == "U":
            return wu.at[c, zz, yy]
        rows = pl.ds(0, CUT) if name == "A" else pl.ds(CUT, CUT)
        return wd.at[c, zz, rows, yl(yy)]

    n_sent = [0]

    def w_sem(name, rz, ry):
        return w_recv.at[names.index(name), rz % 4, ry % 4]

    def wsend(name, rz, ry, dz=0, dy=0):
        src = own_src[name] if (rz, ry) == (0, 0) else unit(name, rz, ry)
        k = n_sent[0]
        n_sent[0] += 1
        go(remote(
            src, unit(name, rz, ry), w_send.at[k], w_sem(name, rz - dz, ry - dy),
            z=at(z, dz), y=at(y, dy),
        ))

    def wwait(name, rz, ry):
        ref = unit(name, rz, ry)
        remote(ref, ref, w_send.at[0], w_sem(name, rz, ry)).wait_recv()

    def send(name, first_axis, second_axis, step):
        swap = name in ("U", "B")
        rz, ry = (first_axis, second_axis) if swap else (second_axis, first_axis)
        dz, dy = step if swap else (step[1], step[0])
        wsend(name, rz, ry, dz, dy)

    def wait(name, first_axis, second_axis):
        if name in ("U", "B"):
            wwait(name, first_axis, second_axis)
        else:
            wwait(name, second_axis, first_axis)

    UP, DOWN = 1, -1

    def w_own(pair):
        for n in pair:
            send(n, 0, 0, (UP, 0))
            send(n, 0, 0, (DOWN, 0))
        for n in pair:
            send(n, 0, 0, (0, UP))
            send(n, 0, 0, (0, DOWN))

    def w_first_relay(pair):
        for n in pair:
            if n in ("G", "U"):
                wait(n, -1, 0)
                send(n, -1, 0, (UP, 0))
                wait(n, 1, 0)
            else:
                wait(n, 1, 0)
                send(n, 1, 0, (DOWN, 0))
                wait(n, -1, 0)

    def w_second(pair, r):
        for n in pair:
            if r == 2:
                wait(n, 2, 0)
            send(n, r, 0, (0, UP))
            send(n, r, 0, (0, DOWN))

    def w_second_relay(pair, r):
        for n in pair:
            if r in (0, 1):
                wait(n, r, -1)
                send(n, r, -1, (0, UP))
                wait(n, r, 1)
            else:
                wait(n, r, 1)
                send(n, r, 1, (0, DOWN))
                wait(n, r, -1)

    def w_last(pair):
        for n in pair:
            for r in (0, 1, -1, 2):
                wait(n, r, 2)

    n_pair = [0]
    pair_waits = []

    def plane(name, core, k):
        if name == "G":
            return wg.at[core, k]
        if name == "A":
            return wd.at[core, k, pl.ds(0, CUT)]
        if name == "U":
            return wu.at[core, :, k]
        return wd.at[core, :, pl.ds(CUT, CUT), yl(k)]

    def share(name, r):
        k = n_pair[0]
        n_pair[0] += 1
        pos = at(y, r) if name in ("U", "B") else at(z, r)
        go(remote(plane(name, c, pos), plane(name, c, pos), pair_sem.at[0, k], pair_sem.at[1, k], c=o))
        got = plane(name, o, pos)
        pair_waits.append((name, remote(got, got, pair_sem.at[0, k], pair_sem.at[1, k], c=o)))

    w_own(("G", "U"))

    wo_copies = [
        go(remote(src, wo.at[c, rows], hp_sem.at[0, 4 + i], hp_sem.at[1, 4 + i], c=o))
        for i, (src, rows) in enumerate(((ws_in, pl.ds(0, 128)), (wl_in, pl.ds(128, 128))))
    ]

    lane = lax.broadcasted_iota(jnp.int32, (8, L), 1)
    rows = []
    both = []
    row8 = lax.broadcasted_iota(jnp.int32, (8, L), 0)
    for k in range(NB):
        raw = meta[:, k * L : (k + 1) * L]
        acc = raw
        for sft in (1, 2, 4, 8, 16, 32, 64):
            acc = acc + jnp.where(lane >= sft, pltpu.roll(acc, sft, 1), 0.0)
        rows.append(acc)
        both.append(jnp.where(row8 < 3, acc, raw))
    both.append(jnp.zeros((L - 8 * NB, L), F32))
    cols = jnp.concatenate(both, axis=0).T
    grown = jnp.exp(cols)
    shrunk = jnp.exp(cols[L - 1 : L, :] - cols)

    half = lax.broadcasted_iota(jnp.int32, (L, L), 1) < 64
    half1 = lax.broadcasted_iota(jnp.int32, (1, L), 1) < 64

    def spread(m, k, off):
        b = 8 * k + off
        small = jnp.where(half, m[:, b : b + 1], m[:, b + 1 : b + 2])
        large = jnp.broadcast_to(m[:, b + 2 : b + 3], (L, L))
        return small, large

    def block_decay(k):
        b = 8 * k
        e = grown[L - 1 : L]
        small = jnp.where(half1, e[:, b : b + 1], e[:, b + 1 : b + 2])
        large = jnp.broadcast_to(e[:, b + 2 : b + 3], (1, L))
        return jnp.concatenate([small, large], axis=1)

    tap_rows = []
    for j in range(4):
        m = taps_m[j].astype(F32)
        tap_rows.append(
            [taps_s[j : j + 1].astype(F32), taps_l[j : j + 1].astype(F32)]
            + [m[i : i + 1] for i in range(4)]
        )

    def conv(k, g):
        total = None
        for j in range(4):
            part = tap_rows[j][g] * cbuf[k * L + 5 + j : k * L + 5 + j + L, g * 128 : g * 128 + 128]
            total = part if total is None else total + part
        return silu(total)

    for i in range(3):
        local[i].wait()
    for k in range(NB):
        cbuf[8 + k * L : 8 + (k + 1) * L, :] = xin[k * L : (k + 1) * L, :].astype(F32)
    decays = [block_decay(k) for k in range(NB)]

    def first_pass(k):
        dt_s, dt_l = spread(cols, k, 3)
        sh_s, sh_l = spread(shrunk, k, 0)
        d_s = conv(k, 0) * dt_s
        d_l = conv(k, 1) * dt_l
        blk = pl.ds(k * L, L)
        drive[blk, 0:128] = d_s.astype(BF16)
        drive[blk, 128:256] = d_l.astype(BF16)
        k_s = conv(k, 2).astype(BF16)
        k_l = conv(k, 4).astype(BF16)
        conv_k[blk, 0:128] = k_s
        conv_k[blk, 128:256] = conv(k, 3).astype(BF16)
        conv_k[blk, 256:384] = k_l
        conv_k[blk, 384:512] = conv(k, 5).astype(BF16)
        fresh[k, :, 0:128] = dot_tn(k_s, (d_s * sh_s).astype(BF16))
        fresh[k, :, 128:256] = dot_tn(k_l, (d_l * sh_l).astype(BF16))

    for k in range(1, NB):
        first_pass(k)
    for cp in halos:
        cp.wait_recv()
    start = jnp.where(jnp.logical_and(z == 0, y == 0), 0.0, 1.0)
    cbuf[0:8, :] = halo[8:16, :].astype(F32) * start
    first_pass(0)

    state = fresh[0]
    total = decays[0]
    for k in range(1, NB):
        state = state * decays[k] + fresh[k]
        total = total * decays[k]

    st1[0, 0:128] = state.astype(BF16)
    st1[0, 128:144] = jnp.broadcast_to(total, (16, 256)).astype(BF16)
    for r in (1, 2, 3):
        go(remote(st1.at[0], st1.at[r], st_sem.at[0, r], st_sem.at[1, r], y=at(y, r)))

    mask = lax.broadcasted_iota(jnp.int32, (L, L), 0) >= lax.broadcasted_iota(jnp.int32, (L, L), 1)

    def weights_of(k, h):
        b = 8 * k + h
        diff = cols[:, b : b + 1] - rows[k][h : h + 1, :]
        return jnp.exp(jnp.where(mask, diff, -1e30))

    def second_pass(k):
        blk = pl.ds(k * L, L)
        s_s = dot_nt(conv_k[blk, 128:256], conv_k[blk, 0:128])
        s_l = dot_nt(conv_k[blk, 384:512], conv_k[blk, 256:384])
        d_s = drive[blk, 0:128]
        o_0 = dot((s_s * weights_of(k, 0)).astype(BF16), d_s)
        o_1 = dot((s_s * weights_of(k, 1)).astype(BF16), d_s)
        inner[blk, 0:128] = jnp.where(half, o_0, o_1)
        inner[blk, 128:256] = dot((s_l * weights_of(k, 2)).astype(BF16), drive[blk, 128:256])

    second_pass(0)
    second_pass(1)

    def slot_of(buf, me, other):
        return buf[rem(me - other + 4, 4)].astype(F32)

    for r in (1, 2, 3):
        remote(st1.at[0], st1.at[r], st_sem.at[0, r], st_sem.at[1, r]).wait_recv()
    inside = jnp.zeros((128, 256), F32)
    inside_d = jnp.ones((1, 256), F32)
    line = jnp.zeros((128, 256), F32)
    line_d = jnp.ones((1, 256), F32)
    for j in range(4):
        blob = slot_of(st1, y, j)
        s_j, d_j = blob[0:128], blob[128:129]
        line = line * d_j + s_j
        line_d = line_d * d_j
        inside = jnp.where(j < y, line, inside)
        inside_d = jnp.where(j < y, line_d, inside_d)
    st2[0, 0:128] = line.astype(BF16)
    st2[0, 128:144] = jnp.broadcast_to(line_d, (16, 256)).astype(BF16)
    for r in (1, 2, 3):
        go(remote(st2.at[0], st2.at[r], st_sem.at[2, r], st_sem.at[3, r], z=at(z, r)))

    w_first_relay(("G", "U"))
    w_second(("G", "U"), 1)
    w_second(("G", "U"), -1)
    w_own(("A", "B"))

    for k in range(2, NB):
        second_pass(k)

    for r in (1, 2, 3):
        remote(st2.at[0], st2.at[r], st_sem.at[2, r], st_sem.at[3, r]).wait_recv()
    before = jnp.zeros((128, 256), F32)
    run = jnp.zeros((128, 256), F32)
    for j in range(4):
        blob = slot_of(st2, z, j)
        run = run * blob[128:129] + blob[0:128]
        before = jnp.where(j < z, run, before)
    carry = before * inside_d + inside

    for i in (3, 4):
        local[i].wait()

    for k in range(NB):
        blk = pl.ds(k * L, L)
        gr_s, gr_l = spread(grown, k, 0)
        h_in = carry.astype(BF16)
        o_s = inner[blk, 0:128] + dot(conv_k[blk, 128:256], h_in[:, 0:128]) * gr_s
        o_l = inner[blk, 128:256] + dot(conv_k[blk, 384:512], h_in[:, 128:256]) * gr_l
        carry = carry * decays[k] + fresh[k]
        o_s = o_s * silu(gin[blk, 0:128].astype(F32))
        o_l = o_l * silu(gin[blk, 128:256].astype(F32))
        q = o_s * o_s
        q_0 = jnp.sum(jnp.where(half, q, 0.0), axis=1, keepdims=True)
        q_1 = jnp.sum(jnp.where(half, 0.0, q), axis=1, keepdims=True)
        q_l = jnp.sum(o_l * o_l, axis=1, keepdims=True)
        sc_0 = lax.rsqrt(q_0 * (1.0 / 64) + head_eps)
        sc_1 = lax.rsqrt(q_1 * (1.0 / 64) + head_eps)
        sc_l = lax.rsqrt(q_l * (1.0 / 128) + head_eps)
        heads[blk, 0:128] = (o_s * jnp.where(half, sc_0, sc_1) * gain_s[...]).astype(BF16)
        heads[blk, 128:256] = (o_l * sc_l * gain_l[...]).astype(BF16)

    def rows_of(b, core):
        return pl.ds(pl.multiple_of((2 * b + core) * R, 16), R)

    for b in range(4):
        go(remote(heads.at[rows_of(b, o)], hpart.at[b], hp_sem.at[0, b], hp_sem.at[1, b], c=o))
    for b in range(4):
        lhs[b] = heads[rows_of(b, c), :]
    for i in (6, 7):
        local[i].wait()
    own_rows = lhs[...].reshape(4 * R, 256)
    for cp in wo_copies:
        cp.wait_recv()
    for b in range(4):
        remote(hpart.at[b], hpart.at[b], hp_sem.at[0, b], hp_sem.at[1, b]).wait_recv()
    part_rows = hpart[...].reshape(4 * R, 256)

    x1, x2, x3 = at(x, 1), at(x, 2), at(x, 3)

    class Sum:
        def __init__(self, parts, from_left, from_right, sems):
            self.parts, self.left, self.right, self.sems = parts, from_left, from_right, sems

        def to_right(self, slot, block, h):
            go(remote(self.parts.at[block, h], self.left.at[slot], self.sems.at[0, slot], self.sems.at[1, slot], x=x1))

        def to_left(self, slot, block, h):
            go(remote(self.parts.at[block, h], self.right.at[slot], self.sems.at[2, slot], self.sems.at[3, slot], x=x3))

        def wait_left(self, slot):
            remote(self.left.at[slot], self.left.at[slot], self.sems.at[0, slot], self.sems.at[1, slot]).wait_recv()

        def wait_right(self, slot):
            remote(self.right.at[slot], self.right.at[slot], self.sems.at[2, slot], self.sems.at[3, slot]).wait_recv()

        def after_half(self, h):
            if h == 0:
                self.to_right(0, x2, 0)
                self.to_left(1, x3, 0)
            else:
                self.to_right(1, x1, 1)
                self.to_left(0, x2, 1)

        def merge(self):
            self.wait_left(0)
            self.parts[x1, 0] = (self.parts[x1, 0].astype(F32) + self.left[0].astype(F32)).astype(BF16)
            self.to_right(2, x1, 0)
            self.wait_right(0)
            self.parts[x3, 1] = (self.parts[x3, 1].astype(F32) + self.right[0].astype(F32)).astype(BF16)
            self.to_left(2, x3, 1)

        def result(self):
            self.wait_right(1)
            self.wait_left(1)
            self.wait_left(2)
            self.wait_right(2)
            lo = self.parts[x, 0].astype(F32) + self.left[2].astype(F32) + self.right[1].astype(F32)
            hi = self.parts[x, 1].astype(F32) + self.left[1].astype(F32) + self.right[2].astype(F32)
            return lo, hi

    mixed = Sum(psend, rp, rm, rs_sem)
    for h in range(2):
        for q in range(4):
            n = pl.ds(h * H + q * 256, 256)
            acc = dot(own_rows, wo[c, :, n]) + dot(part_rows, wo[o, :, n])
            psend[:, h, :, q * 256 : (q + 1) * 256] = acc.reshape(4, R, 256).astype(BF16)
        mixed.after_half(h)
    mixed.merge()

    w_first_relay(("A", "B"))
    w_second_relay(("G", "U"), 0)

    local[5].wait()
    lo, hi = mixed.result()
    mid_lo = (resv[:, 0:H].astype(F32) + lo).astype(BF16)
    mid_hi = (resv[:, H:DM].astype(F32) + hi).astype(BF16)
    midv[0] = mid_lo
    midv[1] = mid_hi
    f_lo, f_hi = mid_lo.astype(F32), mid_hi.astype(F32)
    square = jnp.sum(f_lo * f_lo, axis=1, keepdims=True) + jnp.sum(f_hi * f_hi, axis=1, keepdims=True)
    scale = lax.rsqrt(square * (1.0 / DM) + row_eps)
    ag[x, 0] = (f_lo * scale * gain_n[:, 0:H]).astype(BF16)
    ag[x, 1] = (f_hi * scale * gain_n[:, H:DM]).astype(BF16)

    def ag_right(slot, block, h):
        go(remote(ag.at[block, h], ag.at[block, h], ag_sem.at[0, slot], ag_sem.at[1, slot], x=x1))

    def ag_left(slot, block, h):
        go(remote(ag.at[block, h], ag.at[block, h], ag_sem.at[2, slot], ag_sem.at[3, slot], x=x3))

    def ag_wait(side, slot, block, h):
        remote(ag.at[block, h], ag.at[block, h], ag_sem.at[0, slot], ag_sem.at[side, slot]).wait_recv()

    ag_right(0, x, 0)
    ag_left(0, x, 1)
    ag_right(1, x, 1)
    ag_left(1, x, 0)

    w_second(("G", "U"), 2)
    w_second_relay(("G", "U"), 1)
    w_second_relay(("G", "U"), -1)

    ag_wait(1, 0, x3, 0)
    ag_right(2, x3, 0)
    ag_wait(3, 0, x1, 1)
    ag_left(2, x1, 1)

    for i in (8, 9, 10):
        local[i].wait()
    for n in ("G", "U"):
        share(n, 0)
    w_second_relay(("G", "U"), 2)
    for n in ("G", "U"):
        share(n, 1)
        share(n, -1)
    w_second(("A", "B"), 1)
    w_second(("A", "B"), -1)
    w_second(("A", "B"), 2)
    for r in (0, 1, -1, 2):
        w_second_relay(("A", "B"), r)
    w_last(("G", "U"))
    for n in ("G", "U"):
        share(n, 2)
    for n in ("A", "B"):
        share(n, 0)
        share(n, 1)
        share(n, -1)

    ag_wait(1, 1, x3, 1)
    ag_wait(3, 1, x1, 0)
    ag_wait(1, 2, x2, 0)
    ag_wait(3, 2, x2, 1)

    def expand(core):
        for n0, n in ((0, 256), (256, 256), (512, 192)):
            gate = up = None
            for h in range(2):
                a = ag[:, h].reshape(4 * R, H)
                zs = slice(2 * h, 2 * h + 2)
                w_gate = wg[core, zs, :, :, n0 : n0 + n].reshape(H, n)
                w_up = wu[core, zs, :, :, n0 : n0 + n].reshape(H, n)
                gate = dot(a, w_gate) if gate is None else gate + dot(a, w_gate)
                up = dot(a, w_up) if up is None else up + dot(a, w_up)
            hid[core, :, n0 : n0 + n] = (silu(gate) * up).astype(BF16)

    expand(c)
    for name, w in pair_waits:
        if name in ("G", "U"):
            w.wait_recv()
    expand(o)

    w_last(("A", "B"))
    for n in ("A", "B"):
        share(n, 2)
    for name, w in pair_waits:
        if name in ("A", "B"):
            w.wait_recv()

    down = Sum(psend2, rp2, rm2, rs2_sem)
    for h in range(2):
        for q in range(4):
            zz, n0 = 2 * h + q // 2, (q % 2) * 256
            acc = dot(hid[0], wd[0, zz, :, n0 : n0 + 256]) + dot(hid[1], wd[1, zz, :, n0 : n0 + 256])
            psend2[:, h, :, q * 256 : (q + 1) * 256] = acc.reshape(4, R, 256).astype(BF16)
        down.after_half(h)
    down.merge()
    lo, hi = down.result()
    out[:, 0:H] = (midv[0].astype(F32) + lo).astype(BF16)
    out[:, H:DM] = (midv[1].astype(F32) + hi).astype(BF16)

    for cp in pending:
        cp.wait_send()


def on_device(
    residual, small_value_inputs, large_value_inputs, small_gate_inputs, large_gate_inputs,
    state_projections, small_step_inputs, large_step_inputs, small_decay_offsets,
    large_decay_offsets, small_decay_rates, large_decay_rates, small_filter_taps,
    large_filter_taps, state_filter_taps, small_head_gains, large_head_gains,
    small_output_projection, large_output_projection, channel_norm_gain, gate_matrix,
    up_matrix, down_matrix,
):
    flat = state_projections.reshape(T, 512)
    steps = jnp.concatenate([small_step_inputs, large_step_inputs], axis=1).astype(F32)
    offsets = jnp.concatenate([small_decay_offsets, large_decay_offsets], axis=1)
    rates = jnp.concatenate([small_decay_rates, large_decay_rates])
    dt = jax.nn.softplus(steps)
    log_decay = -jnp.exp(rates)[None, :] * dt + offsets
    meta = jnp.concatenate([log_decay.T, dt.T, jnp.zeros((2, T), F32)], axis=0)

    anywhere = pl.BlockSpec(memory_space=pl.ANY)
    vmem = pl.BlockSpec(memory_space=pltpu.VMEM)
    dma = pltpu.SemaphoreType.DMA
    V = pltpu.VMEM
    return pl.pallas_call(
        kernel,
        out_shape=jax.ShapeDtypeStruct((R, DM), BF16),
        in_specs=[anywhere] * 11 + [vmem] * 7,
        out_specs=vmem,
        scratch_shapes=[
            V((T, 768), BF16),
            V((T, 256), BF16),
            V((R, DM), BF16),
            V((16, 768), BF16),
            V((T + 8, 768), F32),
            V((T, 512), BF16),
            V((T, 256), BF16),
            V((NB, 128, 256), F32),
            V((T, 256), F32),
            V((T, 256), BF16),
            V((4, R, 256), BF16),
            V((4, R, 256), BF16),
            V((2, 256, DM), BF16),
            V((2, 4, 4, KROWS, FD), BF16),
            V((2, 4, 4, KROWS, FD), BF16),
            V((2, 4, FD, 512), BF16),
            V((4, 144, 256), BF16),
            V((4, 144, 256), BF16),
            V((4, 2, R, H), BF16),
            V((3, R, H), BF16),
            V((3, R, H), BF16),
            V((4, 2, R, H), BF16),
            V((2, 4 * R, FD), BF16),
            V((4, 2, R, H), BF16),
            V((3, R, H), BF16),
            V((3, R, H), BF16),
            V((2, R, H), BF16),
            dma((11,)),
            dma((2, 3)),
            dma((60,)),
            dma((4, 4, 4)),
            dma((2, 16)),
            dma((4, 4)),
            dma((2, 6)),
            dma((4, 3)),
            dma((4, 3)),
            dma((4, 3)),
        ],
        compiler_params=pltpu.CompilerParams(
            collective_id=0, has_side_effects=True, vmem_limit_bytes=60 * 1024 * 1024
        ),
    )(
        residual, small_value_inputs, large_value_inputs, small_gate_inputs, large_gate_inputs,
        flat, small_output_projection, large_output_projection, gate_matrix, up_matrix, down_matrix,
        meta, small_filter_taps, large_filter_taps, state_filter_taps,
        small_head_gains.reshape(1, 128), large_head_gains.reshape(1, 128),
        channel_norm_gain.reshape(1, DM),
    )


def solution(mesh):
    split = Mesh(mesh.devices.reshape(4, 4, 4, 2), ("z", "y", "x", "c"))
    in_specs = (
        P(SP_TP, None),
        P(SP, TP),
        P(SP, TP),
        P(SP, TP),
        P(SP, TP),
        P(SP, None, None),
        P(SP, TP),
        P(SP, TP),
        P(SP, TP),
        P(SP, TP),
        P(TP),
        P(TP),
        P(None, TP),
        P(None, TP),
        P(),
        P(TP),
        P(TP),
        P(TP, None),
        P(TP, None),
        P(),
        P(SP, TP),
        P(SP, TP),
        P(TP, SP),
    )
    return jax.shard_map(
        on_device, mesh=split, in_specs=in_specs, out_specs=P(SP_TP, None), check_vma=False
    )
```

time: 305 us -> 101 us (0.33)
  blocking collectives: 92.5 us -> 0 us
  Pallas kernels: 0 us -> 90.3 us
  matrix products: 56.9 us -> 0 us
  local copies, waits for them, and re-layouts: 43.7 us -> 6.22 us
  waiting for transfers between devices: 31.8 us -> 0 us
  other arithmetic: 26.2 us -> 2.21 us
  between operations: 22.5 us -> 0.73 us
  starting transfers between devices: 21.6 us -> 0 us
  loops' own time: 7.43 us -> 0 us
    pallas_call x0 -> x1, Pallas kernels: none -> 90.3 us  [on_device(): pl.pallas_call(kernel, out_shape=jax.ShapeDtypeStruct((R, DM), BF16), in_...]
    all_to_all x2 -> x0, blocking collectives: 71.6 us -> none  [the longest x1 36.4 us: sum_at_owner(): pieces = lax.all_to_all(in_blocks(x, dim, size), axis, 0, 0, tiled=True)]
    dot_general x76 -> x0, matrix products: 56.9 us -> none  [the longest x20 16.2 us: advance(): carried = jnp.einsum('ln,hpn,lh->lhp', read_rows, carry, jnp.exp(within))]
    all_to_all x1 -> x0, waiting for transfers between devices: 31.1 us -> none  [sum_at_owner(): pieces = lax.all_to_all(in_blocks(x, dim, size), axis, 0, 0, tiled=True)]
    all_gather x2 -> x0, blocking collectives: 20.9 us -> none  [gathered_once(): both, at, found = (lax.all_gather(jnp.concatenate(lines), axis), 0, {})]
    slice x27 -> x0, local copies, waits for them, and re-layouts: 12.4 us -> none  [the longest x10 5.47 us: advance(): return (carry * jnp.exp(within[-1])[:, None, None] + fresh, inner + carried)]
    all_to_all x1 -> x0, starting transfers between devices: 11.3 us -> none  [sum_at_owner(): pieces = lax.all_to_all(in_blocks(x, dim, size), axis, 0, 0, tiled=True)]
    ppermute x3 -> x0, starting transfers between devices: 10.3 us -> none  [shifted(): return lax.ppermute(x, axis, pairs)]
  transfers between devices with their start and end apart: 6 -> 0, of which waited for: 1 -> 0; matrix products, arithmetic and copies ran while one was open for 37% -> 0% of each run, Pallas kernels for 0% -> 0%
where the time goes in v1:
time: 101 us; the launch traced here: 99.5 us
  Pallas kernels  90.3 us (89%)
  local copies, waits for them, and re-layouts  6.22 us (6%)
  other arithmetic  2.21 us (2%)
    pallas_call x1, Pallas kernels, on_device(): pl.pallas_call(kernel, out_shape=jax.ShapeDtypeStruct((R, DM), BF16), in_...  90.3 us
    unnamed x6, local copies, waits for them, and re-layouts  6.14 us

profile of v1, /device:TPU:1, one launch (start us, length us, event | category | flops | bytes accessed | tf_op | source)
XLA Modules:
  0.0 99.5 jit_solution(11899620246064055850)
XLA Ops:
  0.0 0.0 copy-start
  0.7 0.7 fusion.5
  1.5 0.1 pad.2.clone
  1.5 0.8 fusion.4
  2.3 0.7 maximum_maximum_fusion.meta
  3.0 1.7 %copy.24.g_in = bf16[128,704]{1,0:T(8,128)(2,1)} copy(bf16[128,704]{0,1:T(8,128)(2,1)} %param.43) | data formatting | bytes 360448 | tf_op args[20]
  4.7 1.7 %copy.25.u_in = bf16[128,704]{1,0:T(8,128)(2,1)} copy(bf16[128,704]{0,1:T(8,128)(2,1)} %param.44) | data formatting | bytes 360448 | tf_op args[21]
  6.5 0.0 copy-done
  6.5 0.9 copy.28
  7.4 90.3 %shard_map.217 = bf16[80,2048]{1,0:T(8,128)(2,1)} custom-call(bf16[80,2048]{1,0:T(8,128)(2,1)} %res_in.1, bf16[640,128]{1,0:T(8,128)(2,1)} %vs_in.1, bf16[640,128]{1,0:T(8,128)(2,1)} %vl_in.1, bf16[640,128]{1,0:T(8,128)(2,1)} %gs_in.1, bf16[640,128]{1,0:T(8,128)(2,1)} %gl_in.1, bf16[640,512]{1,0:T(8,128)(2,1)} %bitcast.11, bf16[128,2048]{1,0:T(8,128)(2,1)} %ws_in.1, ...), custom_call_target="tpu_custom_call" | custom-call | tf_op jit(solution)/shard_map/pallas_call | solution.py:601
  97.8 1.7 %copy.31 = bf16[80,2048]{1,0:T(8,128)(2,1)} copy(bf16[80,2048]{1,0:T(8,128)(2,1)} %shard_map.217) | data formatting | bytes 655360
  (1 shorter events, 0.0 us)
Async XLA Ops:
  0.0 6.5 %copy-start = (bf16[640,4,128]{2,1,0:T(4,128)(2,1)S(1)}, bf16[640,4,128]{2,1,0:T(4,128)(2,1)}, u32[]{:S(2)}) copy-start(bf16[640,4,128]{2,1,0:T(4,128)(2,1)} %param.28) | copy-start | bytes 1966084

commit v2 on v1

--- a/solution.py
+++ b/solution.py
@@ -21,6 +21,8 @@
 H = 1024
 KROWS = 128
 CUT = 352
+Q = 512
+ORDER = (0, 2, 1, 3)
 
 head_eps = 1e-05
 row_eps = 1e-06
@@ -44,7 +46,7 @@
 
 def kernel(
     res_in, vs_in, vl_in, gs_in, gl_in, sp_in, ws_in, wl_in, g_in, u_in, d_in,
-    meta, taps_s, taps_l, taps_m, gain_s, gain_l, gain_n,
+    steps_s, steps_l, offs_s, offs_l, rates_s, rates_l, taps_s, taps_l, taps_m, gain_s, gain_l, gain_n,
     out,
     xin, gin, resv, halo, cbuf, conv_k, drive, fresh, inner, heads, hpart, lhs,
     wo, wg, wu, wd, st1, st2, psend, rp, rm, ag, hid, psend2, rp2, rm2, midv,
@@ -57,8 +59,6 @@
     def at(base, by):
         return rem(base + (by % 4), 4)
 
-    last = y == 3
-    first = y == 0
     nxt = {"z": rem(z + lax.div(y + 1, 4), 4), "y": rem(y + 1, 4)}
     prv = {"z": rem(z + 3 + lax.div(y + 3, 4), 4), "y": rem(y + 3, 4)}
 
@@ -79,9 +79,6 @@
         cp.start()
         pending.append(cp)
         return cp
-
-    def yl(i):
-        return pl.ds(pl.multiple_of(i * 128, 128), 128)
 
     local = [
         (vs_in, xin.at[:, pl.ds(0, 128)]),
@@ -94,7 +91,7 @@
         (wl_in, wo.at[c, pl.ds(128, 128)]),
         (g_in, wg.at[c, z, y]),
         (u_in, wu.at[c, z, y]),
-        (d_in, wd.at[c, z, :, yl(y)]),
+        (d_in, wd.at[c, z, y]),
     ]
     local = [pltpu.make_async_copy(a, b, loc_sem.at[i]) for i, (a, b) in enumerate(local)]
     for cp in local:
@@ -109,136 +106,18 @@
     ]
     for p in peers:
         pl.semaphore_signal(barrier, inc=1, device_id=there(**p), device_id_type=pl.DeviceIdType.MESH)
-    pl.semaphore_wait(barrier, len(peers))
-
-    tail = pl.ds(T - 16, 16)
-    halos = [
-        go(remote(src.at[tail], halo.at[:, cols], halo_sem.at[0, i], halo_sem.at[1, i], **nxt))
-        for i, (src, cols) in enumerate(
-            ((vs_in, pl.ds(0, 128)), (vl_in, pl.ds(128, 128)), (sp_in, pl.ds(256, 512)))
-        )
-    ]
-
-    names = ("G", "U", "A", "B")
-    own_src = {
-        "G": g_in, "U": u_in,
-        "A": d_in.at[pl.ds(0, CUT)], "B": d_in.at[pl.ds(CUT, CUT)],
-    }
-
-    def unit(name, rz, ry):
-        zz, yy = at(z, rz), at(y, ry)
-        if name == "G":
-            return wg.at[c, zz, yy]
-        if name == "U":
-            return wu.at[c, zz, yy]
-        rows = pl.ds(0, CUT) if name == "A" else pl.ds(CUT, CUT)
-        return wd.at[c, zz, rows, yl(yy)]
-
-    n_sent = [0]
-
-    def w_sem(name, rz, ry):
-        return w_recv.at[names.index(name), rz % 4, ry % 4]
-
-    def wsend(name, rz, ry, dz=0, dy=0):
-        src = own_src[name] if (rz, ry) == (0, 0) else unit(name, rz, ry)
-        k = n_sent[0]
-        n_sent[0] += 1
-        go(remote(
-            src, unit(name, rz, ry), w_send.at[k], w_sem(name, rz - dz, ry - dy),
-            z=at(z, dz), y=at(y, dy),
-        ))
-
-    def wwait(name, rz, ry):
-        ref = unit(name, rz, ry)
-        remote(ref, ref, w_send.at[0], w_sem(name, rz, ry)).wait_recv()
-
-    def send(name, first_axis, second_axis, step):
-        swap = name in ("U", "B")
-        rz, ry = (first_axis, second_axis) if swap else (second_axis, first_axis)
-        dz, dy = step if swap else (step[1], step[0])
-        wsend(name, rz, ry, dz, dy)
-
-    def wait(name, first_axis, second_axis):
-        if name in ("U", "B"):
-            wwait(name, first_axis, second_axis)
-        else:
-            wwait(name, second_axis, first_axis)
-
-    UP, DOWN = 1, -1
-
-    def w_own(pair):
-        for n in pair:
-            send(n, 0, 0, (UP, 0))
-            send(n, 0, 0, (DOWN, 0))
-        for n in pair:
-            send(n, 0, 0, (0, UP))
-            send(n, 0, 0, (0, DOWN))
-
-    def w_first_relay(pair):
-        for n in pair:
-            if n in ("G", "U"):
-                wait(n, -1, 0)
-                send(n, -1, 0, (UP, 0))
-                wait(n, 1, 0)
-            else:
-                wait(n, 1, 0)
-                send(n, 1, 0, (DOWN, 0))
-                wait(n, -1, 0)
-
-    def w_second(pair, r):
-        for n in pair:
-            if r == 2:
-                wait(n, 2, 0)
-            send(n, r, 0, (0, UP))
-            send(n, r, 0, (0, DOWN))
-
-    def w_second_relay(pair, r):
-        for n in pair:
-            if r in (0, 1):
-                wait(n, r, -1)
-                send(n, r, -1, (0, UP))
-                wait(n, r, 1)
-            else:
-                wait(n, r, 1)
-                send(n, r, 1, (0, DOWN))
-                wait(n, r, -1)
-
-    def w_last(pair):
-        for n in pair:
-            for r in (0, 1, -1, 2):
-                wait(n, r, 2)
-
-    n_pair = [0]
-    pair_waits = []
-
-    def plane(name, core, k):
-        if name == "G":
-            return wg.at[core, k]
-        if name == "A":
-            return wd.at[core, k, pl.ds(0, CUT)]
-        if name == "U":
-            return wu.at[core, :, k]
-        return wd.at[core, :, pl.ds(CUT, CUT), yl(k)]
-
-    def share(name, r):
-        k = n_pair[0]
-        n_pair[0] += 1
-        pos = at(y, r) if name in ("U", "B") else at(z, r)
-        go(remote(plane(name, c, pos), plane(name, c, pos), pair_sem.at[0, k], pair_sem.at[1, k], c=o))
-        got = plane(name, o, pos)
-        pair_waits.append((name, remote(got, got, pair_sem.at[0, k], pair_sem.at[1, k], c=o)))
-
-    w_own(("G", "U"))
-
-    wo_copies = [
-        go(remote(src, wo.at[c, rows], hp_sem.at[0, 4 + i], hp_sem.at[1, 4 + i], c=o))
-        for i, (src, rows) in enumerate(((ws_in, pl.ds(0, 128)), (wl_in, pl.ds(128, 128))))
-    ]
-
     lane = lax.broadcasted_iota(jnp.int32, (8, L), 1)
     rows = []
     both = []
     row8 = lax.broadcasted_iota(jnp.int32, (8, L), 0)
+    raw_steps = jnp.concatenate([steps_s[...].astype(F32), steps_l[...].astype(F32)], axis=0)
+    softened = jnp.maximum(raw_steps, 0.0) + jnp.log1p(jnp.exp(-jnp.abs(raw_steps)))
+    head = lax.broadcasted_iota(jnp.int32, (3, T), 0)
+    rate = jnp.where(head == 0, rates_s[0], jnp.where(head == 1, rates_s[1], rates_l[0]))
+    offsets = jnp.concatenate([offs_s[...], offs_l[...]], axis=0)
+    meta = jnp.concatenate(
+        [offsets - jnp.exp(rate) * softened, softened, jnp.zeros((2, T), F32)], axis=0
+    )
     for k in range(NB):
         raw = meta[:, k * L : (k + 1) * L]
         acc = raw
@@ -305,6 +184,140 @@
         fresh[k, :, 0:128] = dot_tn(k_s, (d_s * sh_s).astype(BF16))
         fresh[k, :, 128:256] = dot_tn(k_l, (d_l * sh_l).astype(BF16))
 
+    pl.semaphore_wait(barrier, len(peers))
+
+    tail = pl.ds(T - 16, 16)
+    halos = [
+        go(remote(src.at[tail], halo.at[:, cols], halo_sem.at[0, i], halo_sem.at[1, i], **nxt))
+        for i, (src, cols) in enumerate(
+            ((vs_in, pl.ds(0, 128)), (vl_in, pl.ds(128, 128)), (sp_in, pl.ds(256, 512)))
+        )
+    ]
+
+    names = ("G", "U", "A", "B")
+    own_src = {
+        "G": g_in, "U": u_in,
+        "A": d_in.at[pl.ds(0, CUT)], "B": d_in.at[pl.ds(CUT, CUT)],
+    }
+
+    def unit(name, rz, ry):
+        zz, yy = at(z, rz), at(y, ry)
+        if name == "G":
+            return wg.at[c, zz, yy]
+        if name == "U":
+            return wu.at[c, zz, yy]
+        rows = pl.ds(0, CUT) if name == "A" else pl.ds(CUT, CUT)
+        return wd.at[c, zz, yy, rows]
+
+    n_sent = [0]
+
+    def w_sem(name, rz, ry):
+        return w_recv.at[names.index(name), rz % 4, ry % 4]
+
+    def wsend(name, rz, ry, dz=0, dy=0):
+        src = own_src[name] if (rz, ry) == (0, 0) else unit(name, rz, ry)
+        k = n_sent[0]
+        n_sent[0] += 1
+        go(remote(
+            src, unit(name, rz, ry), w_send.at[k], w_sem(name, rz - dz, ry - dy),
+            z=at(z, dz), y=at(y, dy),
+        ))
+
+    def wwait(name, rz, ry):
+        ref = unit(name, rz, ry)
+        remote(ref, ref, w_send.at[0], w_sem(name, rz, ry)).wait_recv()
+
+    def send(name, first_axis, second_axis, step):
+        swap = name in ("U", "B")
+        rz, ry = (first_axis, second_axis) if swap else (second_axis, first_axis)
+        dz, dy = step if swap else (step[1], step[0])
+        wsend(name, rz, ry, dz, dy)
+
+    def wait(name, first_axis, second_axis):
+        if name in ("U", "B"):
+            wwait(name, first_axis, second_axis)
+        else:
+            wwait(name, second_axis, first_axis)
+
+    UP, DOWN = 1, -1
+
+    def w_own_first(pair):
+        for n in pair:
+            send(n, 0, 0, (UP, 0))
+            send(n, 0, 0, (DOWN, 0))
+
+    def w_own_second(pair):
+        for n in pair:
+            send(n, 0, 0, (0, UP))
+            send(n, 0, 0, (0, DOWN))
+
+    def w_near(pair):
+        for n in pair:
+            wait(n, 1, 0)
+            wait(n, -1, 0)
+
+    def w_first_relay(pair):
+        for n in pair:
+            if n in ("G", "U"):
+                send(n, 1, 0, (DOWN, 0))
+            else:
+                send(n, -1, 0, (UP, 0))
+
+    def w_second(pair, r):
+        for n in pair:
+            if r == 2:
+                wait(n, 2, 0)
+            send(n, r, 0, (0, UP))
+            send(n, r, 0, (0, DOWN))
+
+    def w_second_relay(pair, r):
+        for n in pair:
+            if r in (0, -1):
+                wait(n, r, -1)
+                send(n, r, -1, (0, UP))
+            else:
+                wait(n, r, 1)
+                send(n, r, 1, (0, DOWN))
+
+    def w_second_rest(pair, r):
+        for n in pair:
+            wait(n, r, 1 if r in (0, -1) else -1)
+
+    def w_last(pair):
+        for n in pair:
+            for r in (0, 1, -1, 2):
+                wait(n, r, 2)
+
+    n_pair = [0]
+    pair_waits = []
+
+    def plane(name, core, k):
+        if name == "G":
+            return wg.at[core, k]
+        if name == "A":
+            return wd.at[core, k, :, pl.ds(0, CUT)]
+        if name == "U":
+            return wu.at[core, :, k]
+        return wd.at[core, :, k, pl.ds(CUT, CUT)]
+
+    def share(name, r):
+        k = n_pair[0]
+        n_pair[0] += 1
+        pos = at(y, r) if name in ("U", "B") else at(z, r)
+        go(remote(plane(name, c, pos), plane(name, c, pos), pair_sem.at[0, k], pair_sem.at[1, k], c=o))
+        got = plane(name, o, pos)
+        pair_waits.append((name, remote(got, got, pair_sem.at[0, k], pair_sem.at[1, k], c=o)))
+
+    w_own_first(("G", "U"))
+    send("G", 0, 0, (0, UP))
+    send("G", 0, 0, (0, DOWN))
+    w_own_first(("B",))
+
+    wo_copies = [
+        go(remote(src, wo.at[c, rows], hp_sem.at[0, 4 + i], hp_sem.at[1, 4 + i], c=o))
+        for i, (src, rows) in enumerate(((ws_in, pl.ds(0, 128)), (wl_in, pl.ds(128, 128))))
+    ]
+
     for k in range(1, NB):
         first_pass(k)
     for cp in halos:
@@ -320,9 +333,11 @@
         total = total * decays[k]
 
     st1[0, 0:128] = state.astype(BF16)
-    st1[0, 128:144] = jnp.broadcast_to(total, (16, 256)).astype(BF16)
+    st1[0, 128:136] = jnp.broadcast_to(total, (8, 256)).astype(BF16)
     for r in (1, 2, 3):
         go(remote(st1.at[0], st1.at[r], st_sem.at[0, r], st_sem.at[1, r], y=at(y, r)))
+    send("U", 0, 0, (0, UP))
+    send("U", 0, 0, (0, DOWN))
 
     mask = lax.broadcasted_iota(jnp.int32, (L, L), 0) >= lax.broadcasted_iota(jnp.int32, (L, L), 1)
 
@@ -361,14 +376,16 @@
         inside = jnp.where(j < y, line, inside)
         inside_d = jnp.where(j < y, line_d, inside_d)
     st2[0, 0:128] = line.astype(BF16)
-    st2[0, 128:144] = jnp.broadcast_to(line_d, (16, 256)).astype(BF16)
+    st2[0, 128:136] = jnp.broadcast_to(line_d, (8, 256)).astype(BF16)
     for r in (1, 2, 3):
         go(remote(st2.at[0], st2.at[r], st_sem.at[2, r], st_sem.at[3, r], z=at(z, r)))
 
+    w_near(("G", "U"))
     w_first_relay(("G", "U"))
     w_second(("G", "U"), 1)
     w_second(("G", "U"), -1)
-    w_own(("A", "B"))
+    w_own_first(("A",))
+    w_own_second(("A", "B"))
 
     for k in range(2, NB):
         second_pass(k)
@@ -439,45 +456,50 @@
         def wait_right(self, slot):
             remote(self.right.at[slot], self.right.at[slot], self.sems.at[2, slot], self.sems.at[3, slot]).wait_recv()
 
-        def after_half(self, h):
-            if h == 0:
-                self.to_right(0, x2, 0)
-                self.to_left(1, x3, 0)
+        def after_quarter(self, q):
+            if q < 2:
+                self.to_right(q, x2, q)
+                self.to_left(q + 2, x3, q)
             else:
-                self.to_right(1, x1, 1)
-                self.to_left(0, x2, 1)
-
-        def merge(self):
-            self.wait_left(0)
-            self.parts[x1, 0] = (self.parts[x1, 0].astype(F32) + self.left[0].astype(F32)).astype(BF16)
-            self.to_right(2, x1, 0)
-            self.wait_right(0)
-            self.parts[x3, 1] = (self.parts[x3, 1].astype(F32) + self.right[0].astype(F32)).astype(BF16)
-            self.to_left(2, x3, 1)
-
-        def result(self):
-            self.wait_right(1)
-            self.wait_left(1)
-            self.wait_left(2)
-            self.wait_right(2)
-            lo = self.parts[x, 0].astype(F32) + self.left[2].astype(F32) + self.right[1].astype(F32)
-            hi = self.parts[x, 1].astype(F32) + self.left[1].astype(F32) + self.right[2].astype(F32)
-            return lo, hi
+                self.to_left(q - 2, x2, q)
+                self.to_right(q, x1, q)
+
+        def merge(self, i):
+            p = self.parts
+            self.wait_left(i)
+            p[x1, i] = (p[x1, i].astype(F32) + self.left[i].astype(F32)).astype(BF16)
+            self.to_right(4 + i, x1, i)
+            self.wait_right(i)
+            p[x3, 2 + i] = (p[x3, 2 + i].astype(F32) + self.right[i].astype(F32)).astype(BF16)
+            self.to_left(4 + i, x3, 2 + i)
+
+        def result(self, q):
+            a, b = (4 + q, 2 + q) if q < 2 else (q, 2 + q)
+            self.wait_left(a)
+            self.wait_right(b)
+            return self.parts[x, q].astype(F32) + self.left[a].astype(F32) + self.right[b].astype(F32)
 
     mixed = Sum(psend, rp, rm, rs_sem)
-    for h in range(2):
-        for q in range(4):
-            n = pl.ds(h * H + q * 256, 256)
+    for q in ORDER:
+        for e in range(2):
+            n = pl.ds(q * Q + e * 256, 256)
             acc = dot(own_rows, wo[c, :, n]) + dot(part_rows, wo[o, :, n])
-            psend[:, h, :, q * 256 : (q + 1) * 256] = acc.reshape(4, R, 256).astype(BF16)
-        mixed.after_half(h)
-    mixed.merge()
-
-    w_first_relay(("A", "B"))
+            psend[:, q, :, e * 256 : (e + 1) * 256] = acc.reshape(4, R, 256).astype(BF16)
+        mixed.after_quarter(q)
+    w_second(("G", "U"), 2)
     w_second_relay(("G", "U"), 0)
-
+    w_near(("B",))
+    w_first_relay(("B",))
+    mixed.merge(0)
+    w_second_relay(("G", "U"), 1)
+    w_second_relay(("G", "U"), -1)
+    w_near(("A",))
+    w_first_relay(("A",))
+    mixed.merge(1)
     local[5].wait()
-    lo, hi = mixed.result()
+    sums = [mixed.result(q) for q in (2, 3, 0, 1)]
+    lo = jnp.concatenate(sums[2:], axis=1)
+    hi = jnp.concatenate(sums[:2], axis=1)
     mid_lo = (resv[:, 0:H].astype(F32) + lo).astype(BF16)
     mid_hi = (resv[:, H:DM].astype(F32) + hi).astype(BF16)
     midv[0] = mid_lo
@@ -502,10 +524,10 @@
     ag_right(1, x, 1)
     ag_left(1, x, 0)
 
-    w_second(("G", "U"), 2)
-    w_second_relay(("G", "U"), 1)
-    w_second_relay(("G", "U"), -1)
-
+    w_second_relay(("G", "U"), 2)
+    w_second(("A", "B"), 1)
+    w_second(("A", "B"), -1)
+    w_second(("A", "B"), 2)
     ag_wait(1, 0, x3, 0)
     ag_right(2, x3, 0)
     ag_wait(3, 0, x1, 1)
@@ -513,40 +535,38 @@
 
     for i in (8, 9, 10):
         local[i].wait()
+    w_second_relay(("A", "B"), 0)
+    w_second_relay(("A", "B"), 1)
+    w_second_rest(("G", "U"), 0)
+    for r in (1, -1, 2):
+        w_second_rest(("G", "U"), r)
     for n in ("G", "U"):
         share(n, 0)
-    w_second_relay(("G", "U"), 2)
-    for n in ("G", "U"):
         share(n, 1)
         share(n, -1)
-    w_second(("A", "B"), 1)
-    w_second(("A", "B"), -1)
-    w_second(("A", "B"), 2)
-    for r in (0, 1, -1, 2):
-        w_second_relay(("A", "B"), r)
+    w_second_relay(("A", "B"), -1)
+    w_second_relay(("A", "B"), 2)
     w_last(("G", "U"))
     for n in ("G", "U"):
         share(n, 2)
-    for n in ("A", "B"):
-        share(n, 0)
-        share(n, 1)
-        share(n, -1)
-
     ag_wait(1, 1, x3, 1)
     ag_wait(3, 1, x1, 0)
     ag_wait(1, 2, x2, 0)
     ag_wait(3, 2, x2, 1)
+
+    def lined_up(w, core, h, n0, n):
+        parts = [w[core, 2 * h + j // 4, j % 4, n0 : n0 + n, :] for j in range(8)]
+        return jnp.concatenate(parts, axis=1)
 
     def expand(core):
         for n0, n in ((0, 256), (256, 256), (512, 192)):
             gate = up = None
             for h in range(2):
                 a = ag[:, h].reshape(4 * R, H)
-                zs = slice(2 * h, 2 * h + 2)
-                w_gate = wg[core, zs, :, :, n0 : n0 + n].reshape(H, n)
-                w_up = wu[core, zs, :, :, n0 : n0 + n].reshape(H, n)
-                gate = dot(a, w_gate) if gate is None else gate + dot(a, w_gate)
-                up = dot(a, w_up) if up is None else up + dot(a, w_up)
+                w_gate = lined_up(wg, core, h, n0, n)
+                w_up = lined_up(wu, core, h, n0, n)
+                gate = dot_nt(a, w_gate) if gate is None else gate + dot_nt(a, w_gate)
+                up = dot_nt(a, w_up) if up is None else up + dot_nt(a, w_up)
             hid[core, :, n0 : n0 + n] = (silu(gate) * up).astype(BF16)
 
     expand(c)
@@ -555,6 +575,12 @@
             w.wait_recv()
     expand(o)
 
+    for r in (0, 1, -1, 2):
+        w_second_rest(("A", "B"), r)
+    for n in ("A", "B"):
+        share(n, 0)
+        share(n, 1)
+        share(n, -1)
     w_last(("A", "B"))
     for n in ("A", "B"):
         share(n, 2)
@@ -563,14 +589,19 @@
             w.wait_recv()
 
     down = Sum(psend2, rp2, rm2, rs2_sem)
-    for h in range(2):
-        for q in range(4):
-            zz, n0 = 2 * h + q // 2, (q % 2) * 256
-            acc = dot(hid[0], wd[0, zz, :, n0 : n0 + 256]) + dot(hid[1], wd[1, zz, :, n0 : n0 + 256])
-            psend2[:, h, :, q * 256 : (q + 1) * 256] = acc.reshape(4, R, 256).astype(BF16)
-        down.after_half(h)
-    down.merge()
-    lo, hi = down.result()
+    for q in ORDER:
+        for e in range(2):
+            acc = None
+            for cc in range(2):
+                w_down = jnp.concatenate([wd[cc, q, 2 * e], wd[cc, q, 2 * e + 1]], axis=1)
+                acc = dot(hid[cc], w_down) if acc is None else acc + dot(hid[cc], w_down)
+            psend2[:, q, :, e * 256 : (e + 1) * 256] = acc.reshape(4, R, 256).astype(BF16)
+        down.after_quarter(q)
+    down.merge(0)
+    down.merge(1)
+    sums = [down.result(q) for q in (2, 3, 0, 1)]
+    lo = jnp.concatenate(sums[2:], axis=1)
+    hi = jnp.concatenate(sums[:2], axis=1)
     out[:, 0:H] = (midv[0].astype(F32) + lo).astype(BF16)
     out[:, H:DM] = (midv[1].astype(F32) + hi).astype(BF16)
 
@@ -587,21 +618,16 @@
     up_matrix, down_matrix,
 ):
     flat = state_projections.reshape(T, 512)
-    steps = jnp.concatenate([small_step_inputs, large_step_inputs], axis=1).astype(F32)
-    offsets = jnp.concatenate([small_decay_offsets, large_decay_offsets], axis=1)
-    rates = jnp.concatenate([small_decay_rates, large_decay_rates])
-    dt = jax.nn.softplus(steps)
-    log_decay = -jnp.exp(rates)[None, :] * dt + offsets
-    meta = jnp.concatenate([log_decay.T, dt.T, jnp.zeros((2, T), F32)], axis=0)
 
     anywhere = pl.BlockSpec(memory_space=pl.ANY)
     vmem = pl.BlockSpec(memory_space=pltpu.VMEM)
+    smem = pl.BlockSpec(memory_space=pltpu.SMEM)
     dma = pltpu.SemaphoreType.DMA
     V = pltpu.VMEM
     return pl.pallas_call(
         kernel,
         out_shape=jax.ShapeDtypeStruct((R, DM), BF16),
-        in_specs=[anywhere] * 11 + [vmem] * 7,
+        in_specs=[anywhere] * 11 + [vmem] * 4 + [smem] * 2 + [vmem] * 6,
         out_specs=vmem,
         scratch_shapes=[
             V((T, 768), BF16),
@@ -617,19 +643,19 @@
             V((4, R, 256), BF16),
             V((4, R, 256), BF16),
             V((2, 256, DM), BF16),
-            V((2, 4, 4, KROWS, FD), BF16),
-            V((2, 4, 4, KROWS, FD), BF16),
-            V((2, 4, FD, 512), BF16),
-            V((4, 144, 256), BF16),
-            V((4, 144, 256), BF16),
-            V((4, 2, R, H), BF16),
-            V((3, R, H), BF16),
-            V((3, R, H), BF16),
+            V((2, 4, 4, FD, KROWS), BF16),
+            V((2, 4, 4, FD, KROWS), BF16),
+            V((2, 4, 4, FD, KROWS), BF16),
+            V((4, 136, 256), BF16),
+            V((4, 136, 256), BF16),
+            V((4, 4, R, Q), BF16),
+            V((6, R, Q), BF16),
+            V((6, R, Q), BF16),
             V((4, 2, R, H), BF16),
             V((2, 4 * R, FD), BF16),
-            V((4, 2, R, H), BF16),
-            V((3, R, H), BF16),
-            V((3, R, H), BF16),
+            V((4, 4, R, Q), BF16),
+            V((6, R, Q), BF16),
+            V((6, R, Q), BF16),
             V((2, R, H), BF16),
             dma((11,)),
             dma((2, 3)),
@@ -638,17 +664,18 @@
             dma((2, 16)),
             dma((4, 4)),
             dma((2, 6)),
+            dma((4, 6)),
             dma((4, 3)),
-            dma((4, 3)),
-            dma((4, 3)),
+            dma((4, 6)),
         ],
         compiler_params=pltpu.CompilerParams(
             collective_id=0, has_side_effects=True, vmem_limit_bytes=60 * 1024 * 1024
         ),
     )(
         residual, small_value_inputs, large_value_inputs, small_gate_inputs, large_gate_inputs,
-        flat, small_output_projection, large_output_projection, gate_matrix, up_matrix, down_matrix,
-        meta, small_filter_taps, large_filter_taps, state_filter_taps,
+        flat, small_output_projection, large_output_projection, gate_matrix.T, up_matrix.T, down_matrix,
+        small_step_inputs.T, large_step_inputs.T, small_decay_offsets.T, large_decay_offsets.T,
+        small_decay_rates, large_decay_rates, small_filter_taps, large_filter_taps, state_filter_taps,
         small_head_gains.reshape(1, 128), large_head_gains.reshape(1, 128),
         channel_norm_gain.reshape(1, DM),
     )

time: 101 us -> 87.4 us (0.87)
  the two profiles are of different devices: /device:TPU:1 before, /device:TPU:24 now
where the time goes in v2:
time: 87.4 us; the launch traced here: 87.2 us
  Pallas kernels  82.8 us (95%)
  local copies, waits for them, and re-layouts  3.74 us (4%)
    pallas_call x1, Pallas kernels, on_device(): pl.pallas_call(kernel, out_shape=jax.ShapeDtypeStruct((R, DM), BF16), in_...  82.8 us
    unnamed x2, local copies, waits for them, and re-layouts  3.74 us

profile of v2, /device:TPU:24, one launch (start us, length us, event | category | flops | bytes accessed | tf_op | source)
XLA Modules:
  0.0 87.2 jit_solution(8391176950104646207)
XLA Ops:
  0.7 2.0 %copy.26 = bf16[80,8,4,128]{3,1,2,0:T(8,128)(2,1)} copy(bf16[80,8,4,128]{3,2,1,0:T(4,128)(2,1)} %bitcast.14) | data formatting | bytes 1310720
  2.7 82.8 %shard_map.217 = bf16[80,2048]{1,0:T(8,128)(2,1)} custom-call(bf16[80,2048]{1,0:T(8,128)(2,1)} %res_in.1, bf16[640,128]{1,0:T(8,128)(2,1)} %vs_in.1, bf16[640,128]{1,0:T(8,128)(2,1)} %vl_in.1, bf16[640,128]{1,0:T(8,128)(2,1)} %gs_in.1, bf16[640,128]{1,0:T(8,128)(2,1)} %gl_in.1, bf16[640,512]{1,0:T(8,128)(2,1)} %bitcast.13, bf16[128,2048]{1,0:T(8,128)(2,1)} %ws_in.1, ...), custom_call_target="tpu_custom_call" | custom-call | tf_op jit(solution)/shard_map/pallas_call | solution.py:627
  85.5 1.7 %copy.29 = bf16[80,2048]{1,0:T(8,128)(2,1)} copy(bf16[80,2048]{1,0:T(8,128)(2,1)} %shard_map.217) | data formatting | bytes 655360

commit v3 on v2

--- a/solution.py
+++ b/solution.py
@@ -23,6 +23,53 @@
 CUT = 352
 Q = 512
 ORDER = (0, 2, 1, 3)
+STEPS = (0, 1, -1, 2)
+COLUMNS = (
+    ((0, 0), (0, 1), (1, 0), (0, -1)),
+    ((-1, 0), (1, 1), (0, 2), (1, -1)),
+    ((2, 0), (-1, 1), (-1, -1), (2, 1)),
+    ((1, 2), (2, -1), (-1, 2), (2, 2)),
+)
+SENDS = (
+    ((0, 0, 0, 0, 1), (0, 0, 0, 0, -1), (1, 0, 0, 0, 1), (1, 0, 0, 0, -1), (0, 0, 0, 1, 1), (0, 0, 0, 1, -1)),
+    ((1, 0, 0, 1, -1), (1, 0, 0, 1, 1)),
+    ((0, 1, 0, 0, -1),),
+    ((1, 1, 0, 0, -1), (1, 1, 0, 1, 1), (0, 1, 0, 1, 1)),
+    ((1, 1, 0, 1, -1), (0, 1, 0, 1, -1), (1, -1, 0, 1, 1), (0, -1, 0, 1, 1)),
+    ((1, -1, 0, 1, -1), (0, -1, 0, 1, -1)),
+    ((1, 2, 0, 1, 1), (0, 2, 0, 1, 1), (1, 2, 0, 1, -1), (0, 2, 0, 1, -1), (1, 0, -1, 1, 1)),
+    ((0, 0, -1, 1, 1), (1, 1, 1, 1, -1), (0, 1, 1, 1, -1)),
+    ((1, -1, -1, 1, 1), (0, -1, -1, 1, 1)),
+    ((1, 2, -1, 1, 1), (0, 2, -1, 1, 1), (2, 0, 0, 0, -1), (3, 0, 0, 0, -1), (3, 0, 0, 1, -1)),
+    ((2, 0, 0, 0, 1), (3, 0, 0, 0, 1), (2, 0, 0, 1, -1), (3, 0, 0, 1, 1), (2, 0, 0, 1, 1)),
+    ((2, 1, 0, 0, -1), (3, 1, 0, 0, -1), (3, 1, 0, 1, 1), (2, 1, 0, 1, -1), (3, 1, 0, 1, -1), (2, 1, 0, 1, 1), (3, 0, 1, 1, -1)),
+    ((2, -1, 0, 1, -1), (2, -1, 0, 1, 1), (2, 0, 1, 1, -1)),
+    ((3, 2, 0, 1, 1), (3, 2, 0, 1, -1), (2, 2, 0, 1, 1), (2, 2, 0, 1, -1), (3, -1, 0, 1, 1), (3, -1, 0, 1, -1)),
+    ((2, 1, -1, 1, 1), (3, 1, -1, 1, 1)),
+    ((3, 2, 1, 1, -1), (2, -1, -1, 1, 1)),
+    ((2, 2, -1, 1, 1), (3, -1, -1, 1, 1)),
+    (),
+)
+SHARES = (
+    ((0, 0, 0), (1, 0, 0), (2, 0, 0), (3, 0, 0)),
+    (),
+    ((0, -1, 0), (0, 1, 0), (1, -1, 0), (1, 1, 0)),
+    ((0, 0, -1), (0, 0, 1)),
+    (),
+    ((1, 0, 1), (1, 0, -1)),
+    ((0, 2, 0), (1, 2, 0)),
+    ((1, 1, -1), (0, 1, -1), (1, 1, 1), (0, 1, 1)),
+    ((1, -1, -1), (0, -1, -1), (1, -1, 1)),
+    ((0, -1, 1), (1, 2, -1), (0, 2, -1)),
+    ((1, 2, 1), (0, 2, 1), (1, 0, 2), (0, 0, 2)),
+    ((1, 1, 2), (0, 1, 2), (1, -1, 2), (2, 1, 0), (0, -1, 2), (3, 1, 0), (3, 0, 1)),
+    ((2, 0, 1), (1, 2, 2), (0, 2, 2), (2, -1, 0)),
+    ((3, -1, 0), (3, 0, -1), (2, 2, 0), (3, 2, 0), (2, 0, -1)),
+    ((3, 1, -1), (2, 1, 1), (3, 1, 1), (2, 1, -1)),
+    ((3, 0, 2), (2, -1, 1), (2, -1, -1), (2, 0, 2), (3, 2, -1), (3, 2, 1)),
+    ((2, 2, -1), (2, 2, 1), (3, -1, -1), (3, -1, 1), (2, 1, 2)),
+    ((3, 1, 2), (3, 2, 2), (2, -1, 2), (2, 2, 2), (3, -1, 2)),
+)
 
 head_eps = 1e-05
 row_eps = 1e-06
@@ -167,22 +214,15 @@
         cbuf[8 + k * L : 8 + (k + 1) * L, :] = xin[k * L : (k + 1) * L, :].astype(F32)
     decays = [block_decay(k) for k in range(NB)]
 
-    def first_pass(k):
-        dt_s, dt_l = spread(cols, k, 3)
-        sh_s, sh_l = spread(shrunk, k, 0)
-        d_s = conv(k, 0) * dt_s
-        d_l = conv(k, 1) * dt_l
-        blk = pl.ds(k * L, L)
-        drive[blk, 0:128] = d_s.astype(BF16)
-        drive[blk, 128:256] = d_l.astype(BF16)
-        k_s = conv(k, 2).astype(BF16)
-        k_l = conv(k, 4).astype(BF16)
-        conv_k[blk, 0:128] = k_s
-        conv_k[blk, 128:256] = conv(k, 3).astype(BF16)
-        conv_k[blk, 256:384] = k_l
-        conv_k[blk, 384:512] = conv(k, 5).astype(BF16)
-        fresh[k, :, 0:128] = dot_tn(k_s, (d_s * sh_s).astype(BF16))
-        fresh[k, :, 128:256] = dot_tn(k_l, (d_l * sh_l).astype(BF16))
+    def first_pass(k, kind):
+        dt, sh = spread(cols, k, 3)[kind], spread(shrunk, k, 0)[kind]
+        blk, at_kind = pl.ds(k * L, L), pl.ds(kind * 128, 128)
+        d = conv(k, kind) * dt
+        drive[blk, at_kind] = d.astype(BF16)
+        key = conv(k, 2 + 2 * kind).astype(BF16)
+        conv_k[blk, 256 * kind : 256 * kind + 128] = key
+        conv_k[blk, 256 * kind + 128 : 256 * kind + 256] = conv(k, 3 + 2 * kind).astype(BF16)
+        fresh[k, :, at_kind] = dot_tn(key, (d * sh).astype(BF16))
 
     pl.semaphore_wait(barrier, len(peers))
 
@@ -200,144 +240,118 @@
         "A": d_in.at[pl.ds(0, CUT)], "B": d_in.at[pl.ds(CUT, CUT)],
     }
 
-    def unit(name, rz, ry):
+    def unit(name, rz, ry, core):
         zz, yy = at(z, rz), at(y, ry)
         if name == "G":
-            return wg.at[c, zz, yy]
+            return wg.at[core, zz, yy]
         if name == "U":
-            return wu.at[c, zz, yy]
+            return wu.at[core, zz, yy]
         rows = pl.ds(0, CUT) if name == "A" else pl.ds(CUT, CUT)
-        return wd.at[c, zz, yy, rows]
-
-    n_sent = [0]
+        return wd.at[core, zz, yy, rows]
+
+    def place(name, f, s):
+        return (f, s) if name in ("U", "B") else (s, f)
+
+    def source(name, f, s):
+        return own_src[name] if (f, s) == (0, 0) else unit(name, *place(name, f, s), c)
 
     def w_sem(name, rz, ry):
         return w_recv.at[names.index(name), rz % 4, ry % 4]
 
-    def wsend(name, rz, ry, dz=0, dy=0):
-        src = own_src[name] if (rz, ry) == (0, 0) else unit(name, rz, ry)
+    n_sent = [0]
+    here = {(n, 0, 0) for n in names}
+
+    def w_wait(name, f, s):
+        if (name, f, s) not in here:
+            here.add((name, f, s))
+            ref = unit(name, *place(name, f, s), c)
+            remote(ref, ref, w_send.at[0], w_sem(name, *place(name, f, s))).wait_recv()
+
+    def w_go(name, f, s, second, step):
+        w_wait(name, f, s)
+        dz, dy = place(name, 0, step) if second else place(name, step, 0)
+        rz, ry = place(name, f, s)
         k = n_sent[0]
         n_sent[0] += 1
         go(remote(
-            src, unit(name, rz, ry), w_send.at[k], w_sem(name, rz - dz, ry - dy),
+            source(name, f, s), unit(name, rz, ry, c), w_send.at[k], w_sem(name, rz - dz, ry - dy),
             z=at(z, dz), y=at(y, dy),
         ))
 
-    def wwait(name, rz, ry):
-        ref = unit(name, rz, ry)
-        remote(ref, ref, w_send.at[0], w_sem(name, rz, ry)).wait_recv()
-
-    def send(name, first_axis, second_axis, step):
-        swap = name in ("U", "B")
-        rz, ry = (first_axis, second_axis) if swap else (second_axis, first_axis)
-        dz, dy = step if swap else (step[1], step[0])
-        wsend(name, rz, ry, dz, dy)
-
-    def wait(name, first_axis, second_axis):
-        if name in ("U", "B"):
-            wwait(name, first_axis, second_axis)
-        else:
-            wwait(name, second_axis, first_axis)
-
-    UP, DOWN = 1, -1
-
-    def w_own_first(pair):
-        for n in pair:
-            send(n, 0, 0, (UP, 0))
-            send(n, 0, 0, (DOWN, 0))
-
-    def w_own_second(pair):
-        for n in pair:
-            send(n, 0, 0, (0, UP))
-            send(n, 0, 0, (0, DOWN))
-
-    def w_near(pair):
-        for n in pair:
-            wait(n, 1, 0)
-            wait(n, -1, 0)
-
-    def w_first_relay(pair):
-        for n in pair:
-            if n in ("G", "U"):
-                send(n, 1, 0, (DOWN, 0))
-            else:
-                send(n, -1, 0, (UP, 0))
-
-    def w_second(pair, r):
-        for n in pair:
-            if r == 2:
-                wait(n, 2, 0)
-            send(n, r, 0, (0, UP))
-            send(n, r, 0, (0, DOWN))
-
-    def w_second_relay(pair, r):
-        for n in pair:
-            if r in (0, -1):
-                wait(n, r, -1)
-                send(n, r, -1, (0, UP))
-            else:
-                wait(n, r, 1)
-                send(n, r, 1, (0, DOWN))
-
-    def w_second_rest(pair, r):
-        for n in pair:
-            wait(n, r, 1 if r in (0, -1) else -1)
-
-    def w_last(pair):
-        for n in pair:
-            for r in (0, 1, -1, 2):
-                wait(n, r, 2)
-
-    n_pair = [0]
-    pair_waits = []
-
-    def plane(name, core, k):
-        if name == "G":
-            return wg.at[core, k]
-        if name == "A":
-            return wd.at[core, k, :, pl.ds(0, CUT)]
-        if name == "U":
-            return wu.at[core, :, k]
-        return wd.at[core, :, k, pl.ds(CUT, CUT)]
-
-    def share(name, r):
-        k = n_pair[0]
-        n_pair[0] += 1
-        pos = at(y, r) if name in ("U", "B") else at(z, r)
-        go(remote(plane(name, c, pos), plane(name, c, pos), pair_sem.at[0, k], pair_sem.at[1, k], c=o))
-        got = plane(name, o, pos)
-        pair_waits.append((name, remote(got, got, pair_sem.at[0, k], pair_sem.at[1, k], c=o)))
-
-    w_own_first(("G", "U"))
-    send("G", 0, 0, (0, UP))
-    send("G", 0, 0, (0, DOWN))
-    w_own_first(("B",))
+    pair_index = {}
+
+    def share(name, f, s):
+        w_wait(name, f, s)
+        k = pair_index.setdefault((name, f, s), len(pair_index))
+        go(remote(
+            source(name, f, s), unit(name, *place(name, f, s), c),
+            pair_sem.at[0, k], pair_sem.at[1, k], c=o,
+        ))
+
+    def pair_wait(name, f, s):
+        k = pair_index[(name, f, s)]
+        ref = unit(name, *place(name, f, s), o)
+        remote(ref, ref, pair_sem.at[0, k], pair_sem.at[1, k], c=o).wait_recv()
+
+    def pump(i):
+        for n, f, s, second, step in SENDS[i]:
+            w_go(names[n], f, s, second, step)
+        for n, f, s in SHARES[i]:
+            share(names[n], f, s)
+
+    pump(0)
 
     wo_copies = [
         go(remote(src, wo.at[c, rows], hp_sem.at[0, 4 + i], hp_sem.at[1, 4 + i], c=o))
         for i, (src, rows) in enumerate(((ws_in, pl.ds(0, 128)), (wl_in, pl.ds(128, 128))))
     ]
 
-    for k in range(1, NB):
-        first_pass(k)
+    for kind in range(2):
+        for k in range(1, NB):
+            first_pass(k, kind)
     for cp in halos:
         cp.wait_recv()
     start = jnp.where(jnp.logical_and(z == 0, y == 0), 0.0, 1.0)
     cbuf[0:8, :] = halo[8:16, :].astype(F32) * start
-    first_pass(0)
-
-    state = fresh[0]
-    total = decays[0]
-    for k in range(1, NB):
-        state = state * decays[k] + fresh[k]
-        total = total * decays[k]
-
-    st1[0, 0:128] = state.astype(BF16)
-    st1[0, 128:136] = jnp.broadcast_to(total, (8, 256)).astype(BF16)
-    for r in (1, 2, 3):
-        go(remote(st1.at[0], st1.at[r], st_sem.at[0, r], st_sem.at[1, r], y=at(y, r)))
-    send("U", 0, 0, (0, UP))
-    send("U", 0, 0, (0, DOWN))
+
+    def state_out(buf, kind, state, total, stage, **axis):
+        buf[kind, 0, 0:128] = state.astype(BF16)
+        buf[kind, 0, 128:136] = jnp.broadcast_to(total, (8, 128)).astype(BF16)
+        for r in (1, 2, 3):
+            ((name, me),) = axis.items()
+            go(remote(
+                buf.at[kind, 0], buf.at[kind, r],
+                st_sem.at[2 * stage, kind, r], st_sem.at[2 * stage + 1, kind, r],
+                **{name: at(me, r)},
+            ))
+
+    def states_in(buf, kind, stage):
+        for r in (1, 2, 3):
+            remote(
+                buf.at[kind, 0], buf.at[kind, r],
+                st_sem.at[2 * stage, kind, r], st_sem.at[2 * stage + 1, kind, r],
+            ).wait_recv()
+
+    def chained(buf, kind, me):
+        line, line_d = jnp.zeros((128, 128), F32), jnp.ones((1, 128), F32)
+        before, before_d = line, line_d
+        for j in range(4):
+            blob = buf[kind, rem(me - j + 4, 4)].astype(F32)
+            line = line * blob[128:129] + blob[0:128]
+            line_d = line_d * blob[128:129]
+            before = jnp.where(j < me, line, before)
+            before_d = jnp.where(j < me, line_d, before_d)
+        return before, before_d, line, line_d
+
+    for kind in range(2):
+        first_pass(0, kind)
+        own = slice(kind * 128, kind * 128 + 128)
+        state, total = fresh[0, :, own], decays[0][:, own]
+        for k in range(1, NB):
+            state = state * decays[k][:, own] + fresh[k, :, own]
+            total = total * decays[k][:, own]
+        state_out(st1, kind, state, total, 0, y=y)
+    pump(1)
 
     mask = lax.broadcasted_iota(jnp.int32, (L, L), 0) >= lax.broadcasted_iota(jnp.int32, (L, L), 1)
 
@@ -356,71 +370,48 @@
         inner[blk, 0:128] = jnp.where(half, o_0, o_1)
         inner[blk, 128:256] = dot((s_l * weights_of(k, 2)).astype(BF16), drive[blk, 128:256])
 
-    second_pass(0)
-    second_pass(1)
-
-    def slot_of(buf, me, other):
-        return buf[rem(me - other + 4, 4)].astype(F32)
-
-    for r in (1, 2, 3):
-        remote(st1.at[0], st1.at[r], st_sem.at[0, r], st_sem.at[1, r]).wait_recv()
-    inside = jnp.zeros((128, 256), F32)
-    inside_d = jnp.ones((1, 256), F32)
-    line = jnp.zeros((128, 256), F32)
-    line_d = jnp.ones((1, 256), F32)
-    for j in range(4):
-        blob = slot_of(st1, y, j)
-        s_j, d_j = blob[0:128], blob[128:129]
-        line = line * d_j + s_j
-        line_d = line_d * d_j
-        inside = jnp.where(j < y, line, inside)
-        inside_d = jnp.where(j < y, line_d, inside_d)
-    st2[0, 0:128] = line.astype(BF16)
-    st2[0, 128:136] = jnp.broadcast_to(line_d, (8, 256)).astype(BF16)
-    for r in (1, 2, 3):
-        go(remote(st2.at[0], st2.at[r], st_sem.at[2, r], st_sem.at[3, r], z=at(z, r)))
-
-    w_near(("G", "U"))
-    w_first_relay(("G", "U"))
-    w_second(("G", "U"), 1)
-    w_second(("G", "U"), -1)
-    w_own_first(("A",))
-    w_own_second(("A", "B"))
-
-    for k in range(2, NB):
+    for k in range(NB):
         second_pass(k)
-
-    for r in (1, 2, 3):
-        remote(st2.at[0], st2.at[r], st_sem.at[2, r], st_sem.at[3, r]).wait_recv()
-    before = jnp.zeros((128, 256), F32)
-    run = jnp.zeros((128, 256), F32)
-    for j in range(4):
-        blob = slot_of(st2, z, j)
-        run = run * blob[128:129] + blob[0:128]
-        before = jnp.where(j < z, run, before)
-    carry = before * inside_d + inside
+    inside = []
+    for kind in range(2):
+        states_in(st1, kind, 0)
+        before, before_d, line, line_d = chained(st1, kind, y)
+        inside.append((before, before_d))
+        state_out(st2, kind, line, line_d, 1, z=z)
+        if kind == 0:
+            pump(2)
+    pump(3)
 
     for i in (3, 4):
         local[i].wait()
 
-    for k in range(NB):
-        blk = pl.ds(k * L, L)
-        gr_s, gr_l = spread(grown, k, 0)
-        h_in = carry.astype(BF16)
-        o_s = inner[blk, 0:128] + dot(conv_k[blk, 128:256], h_in[:, 0:128]) * gr_s
-        o_l = inner[blk, 128:256] + dot(conv_k[blk, 384:512], h_in[:, 128:256]) * gr_l
-        carry = carry * decays[k] + fresh[k]
-        o_s = o_s * silu(gin[blk, 0:128].astype(F32))
-        o_l = o_l * silu(gin[blk, 128:256].astype(F32))
-        q = o_s * o_s
-        q_0 = jnp.sum(jnp.where(half, q, 0.0), axis=1, keepdims=True)
-        q_1 = jnp.sum(jnp.where(half, 0.0, q), axis=1, keepdims=True)
-        q_l = jnp.sum(o_l * o_l, axis=1, keepdims=True)
-        sc_0 = lax.rsqrt(q_0 * (1.0 / 64) + head_eps)
-        sc_1 = lax.rsqrt(q_1 * (1.0 / 64) + head_eps)
-        sc_l = lax.rsqrt(q_l * (1.0 / 128) + head_eps)
-        heads[blk, 0:128] = (o_s * jnp.where(half, sc_0, sc_1) * gain_s[...]).astype(BF16)
-        heads[blk, 128:256] = (o_l * sc_l * gain_l[...]).astype(BF16)
+    def third_pass(k, kind, carry):
+        blk, cols_k = pl.ds(k * L, L), pl.ds(kind * 128, 128)
+        own = slice(kind * 128, kind * 128 + 128)
+        reads = conv_k[blk, 256 * kind + 128 : 256 * kind + 256]
+        out_k = inner[blk, cols_k] + dot(reads, carry.astype(BF16)) * spread(grown, k, 0)[kind]
+        carry = carry * decays[k][:, own] + fresh[k, :, own]
+        out_k = out_k * silu(gin[blk, cols_k].astype(F32))
+        sq = out_k * out_k
+        if kind == 0:
+            sq_0 = jnp.sum(jnp.where(half, sq, 0.0), axis=1, keepdims=True)
+            sq_1 = jnp.sum(jnp.where(half, 0.0, sq), axis=1, keepdims=True)
+            mean = jnp.where(half, sq_0, sq_1) * (1.0 / 64)
+            gain = gain_s[...]
+        else:
+            mean = jnp.sum(sq, axis=1, keepdims=True) * (1.0 / 128)
+            gain = gain_l[...]
+        heads[blk, cols_k] = (out_k * lax.rsqrt(mean + head_eps) * gain).astype(BF16)
+        return carry
+
+    for kind in range(2):
+        states_in(st2, kind, 1)
+        before = chained(st2, kind, z)[0]
+        carry = before * inside[kind][1] + inside[kind][0]
+        for k in range(NB):
+            carry = third_pass(k, kind, carry)
+        if kind == 0:
+            pump(4)
 
     def rows_of(b, core):
         return pl.ds(pl.multiple_of((2 * b + core) * R, 16), R)
@@ -434,6 +425,7 @@
     own_rows = lhs[...].reshape(4 * R, 256)
     for cp in wo_copies:
         cp.wait_recv()
+    pump(5)
     for b in range(4):
         remote(hpart.at[b], hpart.at[b], hp_sem.at[0, b], hp_sem.at[1, b]).wait_recv()
     part_rows = hpart[...].reshape(4 * R, 256)
@@ -486,24 +478,21 @@
             acc = dot(own_rows, wo[c, :, n]) + dot(part_rows, wo[o, :, n])
             psend[:, q, :, e * 256 : (e + 1) * 256] = acc.reshape(4, R, 256).astype(BF16)
         mixed.after_quarter(q)
-    w_second(("G", "U"), 2)
-    w_second_relay(("G", "U"), 0)
-    w_near(("B",))
-    w_first_relay(("B",))
+    pump(6)
     mixed.merge(0)
-    w_second_relay(("G", "U"), 1)
-    w_second_relay(("G", "U"), -1)
-    w_near(("A",))
-    w_first_relay(("A",))
+    pump(7)
     mixed.merge(1)
+    pump(8)
     local[5].wait()
-    sums = [mixed.result(q) for q in (2, 3, 0, 1)]
-    lo = jnp.concatenate(sums[2:], axis=1)
-    hi = jnp.concatenate(sums[:2], axis=1)
+    sums = {q: mixed.result(q) for q in (2, 3)}
+    pump(9)
+    sums.update({q: mixed.result(q) for q in (0, 1)})
+    lo = jnp.concatenate([sums[0], sums[1]], axis=1)
+    hi = jnp.concatenate([sums[2], sums[3]], axis=1)
     mid_lo = (resv[:, 0:H].astype(F32) + lo).astype(BF16)
     mid_hi = (resv[:, H:DM].astype(F32) + hi).astype(BF16)
-    midv[0] = mid_lo
-    midv[1] = mid_hi
+    midv[:, 0:H] = mid_lo
+    midv[:, H:DM] = mid_hi
     f_lo, f_hi = mid_lo.astype(F32), mid_hi.astype(F32)
     square = jnp.sum(f_lo * f_lo, axis=1, keepdims=True) + jnp.sum(f_hi * f_hi, axis=1, keepdims=True)
     scale = lax.rsqrt(square * (1.0 / DM) + row_eps)
@@ -524,36 +513,20 @@
     ag_right(1, x, 1)
     ag_left(1, x, 0)
 
-    w_second_relay(("G", "U"), 2)
-    w_second(("A", "B"), 1)
-    w_second(("A", "B"), -1)
-    w_second(("A", "B"), 2)
+    pump(10)
     ag_wait(1, 0, x3, 0)
     ag_right(2, x3, 0)
     ag_wait(3, 0, x1, 1)
     ag_left(2, x1, 1)
-
+    pump(11)
+    ag_wait(1, 1, x3, 1)
+    ag_wait(3, 1, x1, 0)
+    pump(12)
+    ag_wait(1, 2, x2, 0)
+    ag_wait(3, 2, x2, 1)
+    pump(13)
     for i in (8, 9, 10):
         local[i].wait()
-    w_second_relay(("A", "B"), 0)
-    w_second_relay(("A", "B"), 1)
-    w_second_rest(("G", "U"), 0)
-    for r in (1, -1, 2):
-        w_second_rest(("G", "U"), r)
-    for n in ("G", "U"):
-        share(n, 0)
-        share(n, 1)
-        share(n, -1)
-    w_second_relay(("A", "B"), -1)
-    w_second_relay(("A", "B"), 2)
-    w_last(("G", "U"))
-    for n in ("G", "U"):
-        share(n, 2)
-    ag_wait(1, 1, x3, 1)
-    ag_wait(3, 1, x1, 0)
-    ag_wait(1, 2, x2, 0)
-    ag_wait(3, 2, x2, 1)
-
     def lined_up(w, core, h, n0, n):
         parts = [w[core, 2 * h + j // 4, j % 4, n0 : n0 + n, :] for j in range(8)]
         return jnp.concatenate(parts, axis=1)
@@ -570,40 +543,38 @@
             hid[core, :, n0 : n0 + n] = (silu(gate) * up).astype(BF16)
 
     expand(c)
-    for name, w in pair_waits:
-        if name in ("G", "U"):
-            w.wait_recv()
+    pump(14)
+    for name in ("G", "U"):
+        for f in STEPS:
+            for s in STEPS:
+                pair_wait(name, f, s)
     expand(o)
-
-    for r in (0, 1, -1, 2):
-        w_second_rest(("A", "B"), r)
-    for n in ("A", "B"):
-        share(n, 0)
-        share(n, 1)
-        share(n, -1)
-    w_last(("A", "B"))
-    for n in ("A", "B"):
-        share(n, 2)
-    for name, w in pair_waits:
-        if name in ("A", "B"):
-            w.wait_recv()
+    pump(15)
 
     down = Sum(psend2, rp2, rm2, rs2_sem)
-    for q in ORDER:
+    for i, q in enumerate(ORDER):
+        if i >= 2:
+            pump(14 + i)
+        for rz, ry in COLUMNS[i]:
+            for name in ("A", "B"):
+                f, s = place(name, rz, ry)
+                pair_wait(name, f, s)
         for e in range(2):
             acc = None
             for cc in range(2):
-                w_down = jnp.concatenate([wd[cc, q, 2 * e], wd[cc, q, 2 * e + 1]], axis=1)
+                w_down = jnp.concatenate(
+                    [wd[cc, at(z, rz), at(y, ry)] for rz, ry in COLUMNS[i][2 * e : 2 * e + 2]], axis=1
+                )
                 acc = dot(hid[cc], w_down) if acc is None else acc + dot(hid[cc], w_down)
             psend2[:, q, :, e * 256 : (e + 1) * 256] = acc.reshape(4, R, 256).astype(BF16)
         down.after_quarter(q)
     down.merge(0)
     down.merge(1)
-    sums = [down.result(q) for q in (2, 3, 0, 1)]
-    lo = jnp.concatenate(sums[2:], axis=1)
-    hi = jnp.concatenate(sums[:2], axis=1)
-    out[:, 0:H] = (midv[0].astype(F32) + lo).astype(BF16)
-    out[:, H:DM] = (midv[1].astype(F32) + hi).astype(BF16)
+    for i, q in ((1, 2), (3, 3), (0, 0), (2, 1)):
+        total = down.result(q)
+        for j, (rz, ry) in enumerate(COLUMNS[i]):
+            n = pl.ds(pl.multiple_of((at(z, rz) * 4 + at(y, ry)) * 128, 128), 128)
+            out[:, n] = (midv[:, n].astype(F32) + total[:, 128 * j : 128 * j + 128]).astype(BF16)
 
     for cp in pending:
         cp.wait_send()
@@ -646,8 +617,8 @@
             V((2, 4, 4, FD, KROWS), BF16),
             V((2, 4, 4, FD, KROWS), BF16),
             V((2, 4, 4, FD, KROWS), BF16),
-            V((4, 136, 256), BF16),
-            V((4, 136, 256), BF16),
+            V((2, 4, 136, 128), BF16),
+            V((2, 4, 136, 128), BF16),
             V((4, 4, R, Q), BF16),
             V((6, R, Q), BF16),
             V((6, R, Q), BF16),
@@ -656,13 +627,13 @@
             V((4, 4, R, Q), BF16),
             V((6, R, Q), BF16),
             V((6, R, Q), BF16),
-            V((2, R, H), BF16),
+            V((R, DM), BF16),
             dma((11,)),
             dma((2, 3)),
             dma((60,)),
             dma((4, 4, 4)),
-            dma((2, 16)),
-            dma((4, 4)),
+            dma((2, 64)),
+            dma((4, 2, 4)),
             dma((2, 6)),
             dma((4, 6)),
             dma((4, 3)),

time: 87.4 us -> 81.8 us (0.936)
  the two profiles are of different devices: /device:TPU:24 before, /device:TPU:1 now
where the time goes in v3:
time: 81.8 us; the launch traced here: 81.5 us
  Pallas kernels  77.1 us (94%)
  local copies, waits for them, and re-layouts  3.74 us (5%)
    pallas_call x1, Pallas kernels, on_device(): pl.pallas_call(kernel, out_shape=jax.ShapeDtypeStruct((R, DM), BF16), in_...  77.1 us
    unnamed x2, local copies, waits for them, and re-layouts  3.74 us

profile of v3, /device:TPU:1, one launch (start us, length us, event | category | flops | bytes accessed | tf_op | source)
XLA Modules:
  0.0 81.5 jit_solution(14177273907357820400)
XLA Ops:
  0.7 2.0 %copy.26 = bf16[80,8,4,128]{3,1,2,0:T(8,128)(2,1)} copy(bf16[80,8,4,128]{3,2,1,0:T(4,128)(2,1)} %bitcast.14) | data formatting | bytes 1310720
  2.7 77.1 %shard_map.217 = bf16[80,2048]{1,0:T(8,128)(2,1)} custom-call(bf16[80,2048]{1,0:T(8,128)(2,1)} %res_in.1, bf16[640,128]{1,0:T(8,128)(2,1)} %vs_in.1, bf16[640,128]{1,0:T(8,128)(2,1)} %vl_in.1, bf16[640,128]{1,0:T(8,128)(2,1)} %gs_in.1, bf16[640,128]{1,0:T(8,128)(2,1)} %gl_in.1, bf16[640,512]{1,0:T(8,128)(2,1)} %bitcast.13, bf16[128,2048]{1,0:T(8,128)(2,1)} %ws_in.1, ...), custom_call_target="tpu_custom_call" | custom-call | tf_op jit(solution)/shard_map/pallas_call | solution.py:598
  79.8 1.7 %copy.29 = bf16[80,2048]{1,0:T(8,128)(2,1)} copy(bf16[80,2048]{1,0:T(8,128)(2,1)} %shard_map.217) | data formatting | bytes 655360

commit v4 on v3

--- a/solution.py
+++ b/solution.py
@@ -1,3 +1,5 @@
+import functools
+
 import jax
 import jax.numpy as jnp
 from jax import lax
@@ -25,50 +27,58 @@
 ORDER = (0, 2, 1, 3)
 STEPS = (0, 1, -1, 2)
 COLUMNS = (
-    ((0, 0), (0, 1), (1, 0), (0, -1)),
-    ((-1, 0), (1, 1), (0, 2), (1, -1)),
-    ((2, 0), (-1, 1), (-1, -1), (2, 1)),
-    ((1, 2), (2, -1), (-1, 2), (2, 2)),
+    ((0, 0), (0, 1), (0, -1), (1, 0)),
+    ((-1, 0), (-1, 1), (1, 1), (1, -1)),
+    ((-1, -1), (0, 2), (1, 2), (2, 0)),
+    ((2, 1), (-1, 2), (2, -1), (2, 2)),
 )
 SENDS = (
     ((0, 0, 0, 0, 1), (0, 0, 0, 0, -1), (1, 0, 0, 0, 1), (1, 0, 0, 0, -1), (0, 0, 0, 1, 1), (0, 0, 0, 1, -1)),
     ((1, 0, 0, 1, -1), (1, 0, 0, 1, 1)),
     ((0, 1, 0, 0, -1),),
-    ((1, 1, 0, 0, -1), (1, 1, 0, 1, 1), (0, 1, 0, 1, 1)),
-    ((1, 1, 0, 1, -1), (0, 1, 0, 1, -1), (1, -1, 0, 1, 1), (0, -1, 0, 1, 1)),
-    ((1, -1, 0, 1, -1), (0, -1, 0, 1, -1)),
-    ((1, 2, 0, 1, 1), (0, 2, 0, 1, 1), (1, 2, 0, 1, -1), (0, 2, 0, 1, -1), (1, 0, -1, 1, 1)),
-    ((0, 0, -1, 1, 1), (1, 1, 1, 1, -1), (0, 1, 1, 1, -1)),
-    ((1, -1, -1, 1, 1), (0, -1, -1, 1, 1)),
-    ((1, 2, -1, 1, 1), (0, 2, -1, 1, 1), (2, 0, 0, 0, -1), (3, 0, 0, 0, -1), (3, 0, 0, 1, -1)),
-    ((2, 0, 0, 0, 1), (3, 0, 0, 0, 1), (2, 0, 0, 1, -1), (3, 0, 0, 1, 1), (2, 0, 0, 1, 1)),
-    ((2, 1, 0, 0, -1), (3, 1, 0, 0, -1), (3, 1, 0, 1, 1), (2, 1, 0, 1, -1), (3, 1, 0, 1, -1), (2, 1, 0, 1, 1), (3, 0, 1, 1, -1)),
-    ((2, -1, 0, 1, -1), (2, -1, 0, 1, 1), (2, 0, 1, 1, -1)),
-    ((3, 2, 0, 1, 1), (3, 2, 0, 1, -1), (2, 2, 0, 1, 1), (2, 2, 0, 1, -1), (3, -1, 0, 1, 1), (3, -1, 0, 1, -1)),
-    ((2, 1, -1, 1, 1), (3, 1, -1, 1, 1)),
-    ((3, 2, 1, 1, -1), (2, -1, -1, 1, 1)),
-    ((2, 2, -1, 1, 1), (3, -1, -1, 1, 1)),
+    ((1, 1, 0, 0, -1), (1, 1, 0, 1, 1), (0, 1, 0, 1, 1), (1, 1, 0, 1, -1)),
+    ((0, 1, 0, 1, -1),),
+    ((1, -1, 0, 1, 1), (0, -1, 0, 1, 1), (1, -1, 0, 1, -1), (0, -1, 0, 1, -1)),
+    ((1, 2, 0, 1, 1), (0, 2, 0, 1, 1), (1, 2, 0, 1, -1), (0, 2, 0, 1, -1)),
+    ((2, 0, 0, 0, 1), (3, 0, 0, 0, 1), (2, 0, 0, 0, -1), (3, 0, 0, 0, -1), (1, 0, -1, 1, 1), (0, 0, -1, 1, 1)),
+    ((1, 1, 1, 1, -1), (0, 1, 1, 1, -1), (1, -1, -1, 1, 1), (0, -1, -1, 1, 1)),
+    (),
+    ((1, 2, 1, 1, -1), (2, -1, 0, 0, 1), (0, 2, 1, 1, -1), (3, -1, 0, 0, 1), (3, 0, 0, 1, -1), (3, 0, 0, 1, 1), (2, 0, 0, 1, -1), (2, 0, 0, 1, 1), (3, -1, 0, 1, -1)),
+    ((3, 1, 0, 1, 1), (2, 1, 0, 1, -1), (2, 1, 0, 1, 1), (3, 1, 0, 1, -1), (3, -1, 0, 1, 1), (2, -1, 0, 1, -1), (2, -1, 0, 1, 1)),
+    ((3, 2, 0, 1, -1), (3, 2, 0, 1, 1), (2, 2, 0, 1, -1), (2, 2, 0, 1, 1)),
+    ((3, 0, 1, 1, -1), (3, 1, -1, 1, 1), (2, 0, 1, 1, -1), (2, 1, -1, 1, 1)),
+    ((3, -1, 1, 1, -1),),
+    (),
+    ((2, -1, 1, 1, -1),),
+    (),
+    ((2, 2, -1, 1, 1), (3, 2, -1, 1, 1)),
+    (),
+    (),
     (),
 )
 SHARES = (
     ((0, 0, 0), (1, 0, 0), (2, 0, 0), (3, 0, 0)),
     (),
     ((0, -1, 0), (0, 1, 0), (1, -1, 0), (1, 1, 0)),
-    ((0, 0, -1), (0, 0, 1)),
-    (),
-    ((1, 0, 1), (1, 0, -1)),
-    ((0, 2, 0), (1, 2, 0)),
+    (),
+    ((0, 0, -1), (0, 0, 1), (1, 0, 1)),
+    (),
+    ((1, 0, -1), (0, 2, 0), (1, 2, 0)),
     ((1, 1, -1), (0, 1, -1), (1, 1, 1), (0, 1, 1)),
-    ((1, -1, -1), (0, -1, -1), (1, -1, 1)),
-    ((0, -1, 1), (1, 2, -1), (0, 2, -1)),
-    ((1, 2, 1), (0, 2, 1), (1, 0, 2), (0, 0, 2)),
-    ((1, 1, 2), (0, 1, 2), (1, -1, 2), (2, 1, 0), (0, -1, 2), (3, 1, 0), (3, 0, 1)),
-    ((2, 0, 1), (1, 2, 2), (0, 2, 2), (2, -1, 0)),
-    ((3, -1, 0), (3, 0, -1), (2, 2, 0), (3, 2, 0), (2, 0, -1)),
-    ((3, 1, -1), (2, 1, 1), (3, 1, 1), (2, 1, -1)),
-    ((3, 0, 2), (2, -1, 1), (2, -1, -1), (2, 0, 2), (3, 2, -1), (3, 2, 1)),
-    ((2, 2, -1), (2, 2, 1), (3, -1, -1), (3, -1, 1), (2, 1, 2)),
-    ((3, 1, 2), (3, 2, 2), (2, -1, 2), (2, 2, 2), (3, -1, 2)),
+    ((1, -1, -1), (0, -1, -1), (1, -1, 1), (0, -1, 1)),
+    ((1, 2, -1), (0, 2, -1), (1, 2, 1), (2, -1, 0), (0, 2, 1), (3, -1, 0)),
+    (),
+    ((2, 1, 0), (3, 1, 0), (1, 0, 2), (0, 0, 2), (1, 1, 2), (0, 1, 2)),
+    ((1, -1, 2), (0, -1, 2), (1, 2, 2), (2, 2, 0), (0, 2, 2), (3, 2, 0)),
+    ((3, 0, 1), (3, 0, -1), (2, 0, 1), (2, 0, -1), (3, -1, 1), (3, 1, -1), (2, 1, 1), (2, 1, -1)),
+    ((3, 1, 1),),
+    ((3, -1, -1),),
+    ((2, -1, 1), (2, -1, -1)),
+    ((3, 2, 1),),
+    ((3, 2, -1), (2, 2, 1), (2, 2, -1)),
+    (),
+    ((3, 0, 2), (3, 1, 2), (2, 0, 2), (2, 1, 2)),
+    ((3, -1, 2), (2, -1, 2), (2, 2, 2), (3, 2, 2)),
 )
 
 head_eps = 1e-05
@@ -95,7 +105,7 @@
     res_in, vs_in, vl_in, gs_in, gl_in, sp_in, ws_in, wl_in, g_in, u_in, d_in,
     steps_s, steps_l, offs_s, offs_l, rates_s, rates_l, taps_s, taps_l, taps_m, gain_s, gain_l, gain_n,
     out,
-    xin, gin, resv, halo, cbuf, conv_k, drive, fresh, inner, heads, hpart, lhs,
+    xin, sxin, gin, resv, halo, halo_m, cbuf, cmaps, conv_k, drive, fresh, inner, heads, hpart, lhs,
     wo, wg, wu, wd, st1, st2, psend, rp, rm, ag, hid, psend2, rp2, rm2, midv,
     loc_sem, halo_sem, w_send, w_recv, pair_sem, st_sem, hp_sem, rs_sem, ag_sem, rs2_sem,
 ):
@@ -130,7 +140,7 @@
     local = [
         (vs_in, xin.at[:, pl.ds(0, 128)]),
         (vl_in, xin.at[:, pl.ds(128, 128)]),
-        (sp_in, xin.at[:, pl.ds(256, 512)]),
+        (sp_in, sxin),
         (gs_in, gin.at[:, pl.ds(0, 128)]),
         (gl_in, gin.at[:, pl.ds(128, 128)]),
         (res_in, resv),
@@ -153,6 +163,90 @@
     ]
     for p in peers:
         pl.semaphore_signal(barrier, inc=1, device_id=there(**p), device_id_type=pl.DeviceIdType.MESH)
+    pl.semaphore_wait(barrier, len(peers))
+
+    tail = pl.ds(T - 16, 16)
+    halos = [
+        go(remote(src, dst, halo_sem.at[0, i], halo_sem.at[1, i], **nxt))
+        for i, (src, dst) in enumerate((
+            (vs_in.at[tail], halo.at[:, pl.ds(0, 128)]),
+            (vl_in.at[tail], halo.at[:, pl.ds(128, 128)]),
+            (sp_in.at[pl.ds(4 * T - 64, 64)], halo_m),
+        ))
+    ]
+
+    names = ("G", "U", "A", "B")
+    own_src = {
+        "G": g_in, "U": u_in,
+        "A": d_in.at[pl.ds(0, CUT)], "B": d_in.at[pl.ds(CUT, CUT)],
+    }
+
+    def unit(name, rz, ry, core):
+        zz, yy = at(z, rz), at(y, ry)
+        if name == "G":
+            return wg.at[core, zz, yy]
+        if name == "U":
+            return wu.at[core, zz, yy]
+        rows = pl.ds(0, CUT) if name == "A" else pl.ds(CUT, CUT)
+        return wd.at[core, zz, yy, rows]
+
+    def place(name, f, s):
+        return (f, s) if name in ("U", "B") else (s, f)
+
+    def source(name, f, s):
+        return own_src[name] if (f, s) == (0, 0) else unit(name, *place(name, f, s), c)
+
+    def w_sem(name, rz, ry):
+        return w_recv.at[names.index(name), rz % 4, ry % 4]
+
+    n_sent = [0]
+    here = {(n, 0, 0) for n in names}
+
+    def w_wait(name, f, s):
+        if (name, f, s) not in here:
+            here.add((name, f, s))
+            ref = unit(name, *place(name, f, s), c)
+            remote(ref, ref, w_send.at[0], w_sem(name, *place(name, f, s))).wait_recv()
+
+    def w_go(name, f, s, second, step):
+        w_wait(name, f, s)
+        dz, dy = place(name, 0, step) if second else place(name, step, 0)
+        rz, ry = place(name, f, s)
+        k = n_sent[0]
+        n_sent[0] += 1
+        go(remote(
+            source(name, f, s), unit(name, rz, ry, c), w_send.at[k], w_sem(name, rz - dz, ry - dy),
+            z=at(z, dz), y=at(y, dy),
+        ))
+
+    pair_index = {}
+
+    def share(name, f, s):
+        w_wait(name, f, s)
+        k = pair_index.setdefault((name, f, s), len(pair_index))
+        go(remote(
+            source(name, f, s), unit(name, *place(name, f, s), c),
+            pair_sem.at[0, k], pair_sem.at[1, k], c=o,
+        ))
+
+    def pair_wait(name, f, s):
+        k = pair_index[(name, f, s)]
+        ref = unit(name, *place(name, f, s), o)
+        remote(ref, ref, pair_sem.at[0, k], pair_sem.at[1, k], c=o).wait_recv()
+
+    def pump(i):
+        for n, f, s, second, step in SENDS[i]:
+            w_go(names[n], f, s, second, step)
+        for n, f, s in SHARES[i]:
+            share(names[n], f, s)
+
+    pump(0)
+
+    wo_copies = [
+        go(remote(src, wo.at[c, rows], hp_sem.at[0, 4 + i], hp_sem.at[1, 4 + i], c=o))
+        for i, (src, rows) in enumerate(((ws_in, pl.ds(0, 128)), (wl_in, pl.ds(128, 128))))
+    ]
+
     lane = lax.broadcasted_iota(jnp.int32, (8, L), 1)
     rows = []
     both = []
@@ -204,7 +298,12 @@
     def conv(k, g):
         total = None
         for j in range(4):
-            part = tap_rows[j][g] * cbuf[k * L + 5 + j : k * L + 5 + j + L, g * 128 : g * 128 + 128]
+            row = k * L + 5 + j
+            if g < 2:
+                rows_j = cbuf[row : row + L, g * 128 : g * 128 + 128]
+            else:
+                rows_j = cmaps[pl.ds(4 * row + g - 2, L, 4), :]
+            part = tap_rows[j][g] * rows_j
             total = part if total is None else total + part
         return silu(total)
 
@@ -212,6 +311,8 @@
         local[i].wait()
     for k in range(NB):
         cbuf[8 + k * L : 8 + (k + 1) * L, :] = xin[k * L : (k + 1) * L, :].astype(F32)
+        maps_k = pl.ds(32 + 4 * k * L, 4 * L)
+        cmaps[maps_k, :] = sxin[4 * k * L : 4 * (k + 1) * L, :].astype(F32)
     decays = [block_decay(k) for k in range(NB)]
 
     def first_pass(k, kind):
@@ -224,88 +325,6 @@
         conv_k[blk, 256 * kind + 128 : 256 * kind + 256] = conv(k, 3 + 2 * kind).astype(BF16)
         fresh[k, :, at_kind] = dot_tn(key, (d * sh).astype(BF16))
 
-    pl.semaphore_wait(barrier, len(peers))
-
-    tail = pl.ds(T - 16, 16)
-    halos = [
-        go(remote(src.at[tail], halo.at[:, cols], halo_sem.at[0, i], halo_sem.at[1, i], **nxt))
-        for i, (src, cols) in enumerate(
-            ((vs_in, pl.ds(0, 128)), (vl_in, pl.ds(128, 128)), (sp_in, pl.ds(256, 512)))
-        )
-    ]
-
-    names = ("G", "U", "A", "B")
-    own_src = {
-        "G": g_in, "U": u_in,
-        "A": d_in.at[pl.ds(0, CUT)], "B": d_in.at[pl.ds(CUT, CUT)],
-    }
-
-    def unit(name, rz, ry, core):
-        zz, yy = at(z, rz), at(y, ry)
-        if name == "G":
-            return wg.at[core, zz, yy]
-        if name == "U":
-            return wu.at[core, zz, yy]
-        rows = pl.ds(0, CUT) if name == "A" else pl.ds(CUT, CUT)
-        return wd.at[core, zz, yy, rows]
-
-    def place(name, f, s):
-        return (f, s) if name in ("U", "B") else (s, f)
-
-    def source(name, f, s):
-        return own_src[name] if (f, s) == (0, 0) else unit(name, *place(name, f, s), c)
-
-    def w_sem(name, rz, ry):
-        return w_recv.at[names.index(name), rz % 4, ry % 4]
-
-    n_sent = [0]
-    here = {(n, 0, 0) for n in names}
-
-    def w_wait(name, f, s):
-        if (name, f, s) not in here:
-            here.add((name, f, s))
-            ref = unit(name, *place(name, f, s), c)
-            remote(ref, ref, w_send.at[0], w_sem(name, *place(name, f, s))).wait_recv()
-
-    def w_go(name, f, s, second, step):
-        w_wait(name, f, s)
-        dz, dy = place(name, 0, step) if second else place(name, step, 0)
-        rz, ry = place(name, f, s)
-        k = n_sent[0]
-        n_sent[0] += 1
-        go(remote(
-            source(name, f, s), unit(name, rz, ry, c), w_send.at[k], w_sem(name, rz - dz, ry - dy),
-            z=at(z, dz), y=at(y, dy),
-        ))
-
-    pair_index = {}
-
-    def share(name, f, s):
-        w_wait(name, f, s)
-        k = pair_index.setdefault((name, f, s), len(pair_index))
-        go(remote(
-            source(name, f, s), unit(name, *place(name, f, s), c),
-            pair_sem.at[0, k], pair_sem.at[1, k], c=o,
-        ))
-
-    def pair_wait(name, f, s):
-        k = pair_index[(name, f, s)]
-        ref = unit(name, *place(name, f, s), o)
-        remote(ref, ref, pair_sem.at[0, k], pair_sem.at[1, k], c=o).wait_recv()
-
-    def pump(i):
-        for n, f, s, second, step in SENDS[i]:
-            w_go(names[n], f, s, second, step)
-        for n, f, s in SHARES[i]:
-            share(names[n], f, s)
-
-    pump(0)
-
-    wo_copies = [
-        go(remote(src, wo.at[c, rows], hp_sem.at[0, 4 + i], hp_sem.at[1, 4 + i], c=o))
-        for i, (src, rows) in enumerate(((ws_in, pl.ds(0, 128)), (wl_in, pl.ds(128, 128))))
-    ]
-
     for kind in range(2):
         for k in range(1, NB):
             first_pass(k, kind)
@@ -313,17 +332,26 @@
         cp.wait_recv()
     start = jnp.where(jnp.logical_and(z == 0, y == 0), 0.0, 1.0)
     cbuf[0:8, :] = halo[8:16, :].astype(F32) * start
+    cmaps[0:32, :] = halo_m[32:64, :].astype(F32) * start
 
     def state_out(buf, kind, state, total, stage, **axis):
         buf[kind, 0, 0:128] = state.astype(BF16)
         buf[kind, 0, 128:136] = jnp.broadcast_to(total, (8, 128)).astype(BF16)
-        for r in (1, 2, 3):
-            ((name, me),) = axis.items()
-            go(remote(
+        ((name, me),) = axis.items()
+        copies = [
+            remote(
                 buf.at[kind, 0], buf.at[kind, r],
                 st_sem.at[2 * stage, kind, r], st_sem.at[2 * stage + 1, kind, r],
                 **{name: at(me, r)},
-            ))
+            )
+            for r in (1, 2, 3)
+        ]
+        pending.extend(copies)
+        return copies
+
+    def start_all(copies):
+        for cp in copies:
+            cp.start()
 
     def states_in(buf, kind, stage):
         for r in (1, 2, 3):
@@ -343,6 +371,7 @@
             before_d = jnp.where(j < me, line_d, before_d)
         return before, before_d, line, line_d
 
+    later = []
     for kind in range(2):
         first_pass(0, kind)
         own = slice(kind * 128, kind * 128 + 128)
@@ -350,8 +379,9 @@
         for k in range(1, NB):
             state = state * decays[k][:, own] + fresh[k, :, own]
             total = total * decays[k][:, own]
-        state_out(st1, kind, state, total, 0, y=y)
-    pump(1)
+        copies = state_out(st1, kind, state, total, 0, y=y)
+        pl.when(c == 0)(functools.partial(start_all, copies))
+        later += copies
 
     mask = lax.broadcasted_iota(jnp.int32, (L, L), 0) >= lax.broadcasted_iota(jnp.int32, (L, L), 1)
 
@@ -372,12 +402,14 @@
 
     for k in range(NB):
         second_pass(k)
+    pl.when(c == 1)(functools.partial(start_all, later))
+    pump(1)
     inside = []
     for kind in range(2):
         states_in(st1, kind, 0)
         before, before_d, line, line_d = chained(st1, kind, y)
         inside.append((before, before_d))
-        state_out(st2, kind, line, line_d, 1, z=z)
+        start_all(state_out(st2, kind, line, line_d, 1, z=z))
         if kind == 0:
             pump(2)
     pump(3)
@@ -531,8 +563,10 @@
         parts = [w[core, 2 * h + j // 4, j % 4, n0 : n0 + n, :] for j in range(8)]
         return jnp.concatenate(parts, axis=1)
 
-    def expand(core):
+    def expand(core, points):
         for n0, n in ((0, 256), (256, 256), (512, 192)):
+            if n0 > 0:
+                pump(points[n0 // 256 - 1])
             gate = up = None
             for h in range(2):
                 a = ag[:, h].reshape(4 * R, H)
@@ -542,19 +576,19 @@
                 up = dot_nt(a, w_up) if up is None else up + dot_nt(a, w_up)
             hid[core, :, n0 : n0 + n] = (silu(gate) * up).astype(BF16)
 
-    expand(c)
-    pump(14)
+    expand(c, (14, 15))
+    pump(16)
     for name in ("G", "U"):
         for f in STEPS:
             for s in STEPS:
                 pair_wait(name, f, s)
-    expand(o)
-    pump(15)
+    expand(o, (17, 18))
+    pump(19)
 
     down = Sum(psend2, rp2, rm2, rs2_sem)
     for i, q in enumerate(ORDER):
         if i >= 2:
-            pump(14 + i)
+            pump(18 + i)
         for rz, ry in COLUMNS[i]:
             for name in ("A", "B"):
                 f, s = place(name, rz, ry)
@@ -588,7 +622,7 @@
     small_output_projection, large_output_projection, channel_norm_gain, gate_matrix,
     up_matrix, down_matrix,
 ):
-    flat = state_projections.reshape(T, 512)
+    flat = state_projections.reshape(4 * T, 128)
 
     anywhere = pl.BlockSpec(memory_space=pl.ANY)
     vmem = pl.BlockSpec(memory_space=pltpu.VMEM)
@@ -601,11 +635,14 @@
         in_specs=[anywhere] * 11 + [vmem] * 4 + [smem] * 2 + [vmem] * 6,
         out_specs=vmem,
         scratch_shapes=[
-            V((T, 768), BF16),
+            V((T, 256), BF16),
+            V((4 * T, 128), BF16),
             V((T, 256), BF16),
             V((R, DM), BF16),
-            V((16, 768), BF16),
-            V((T + 8, 768), F32),
+            V((16, 256), BF16),
+            V((64, 128), BF16),
+            V((T + 8, 256), F32),
+            V((4 * T + 32, 128), F32),
             V((T, 512), BF16),
             V((T, 256), BF16),
             V((NB, 128, 256), F32),

time: 81.8 us -> 78.1 us (0.955)
  local copies, waits for them, and re-layouts: 3.74 us -> 1.72 us
  Pallas kernels: 77.1 us -> 75.5 us
    unnamed x2 -> x1, local copies, waits for them, and re-layouts: 3.74 us -> 1.72 us
    pallas_call x1, Pallas kernels: 77.1 us -> 75.5 us  [on_device(): pl.pallas_call(kernel, out_shape=jax.ShapeDtypeStruct((R, DM), BF16), in_...]
where the time goes in v4:
time: 78.1 us; the launch traced here: 77.9 us
  Pallas kernels  75.5 us (97%)
  local copies, waits for them, and re-layouts  1.72 us (2%)
    pallas_call x1, Pallas kernels, on_device(): pl.pallas_call(kernel, out_shape=jax.ShapeDtypeStruct((R, DM), BF16), in_...  75.5 us
    unnamed x1, local copies, waits for them, and re-layouts  1.72 us

profile of v4, /device:TPU:1, one launch (start us, length us, event | category | flops | bytes accessed | tf_op | source)
XLA Modules:
  0.0 77.9 jit_solution(7367816507691876520)
XLA Ops:
  0.7 75.5 %shard_map.217 = bf16[80,2048]{1,0:T(8,128)(2,1)} custom-call(bf16[80,2048]{1,0:T(8,128)(2,1)} %res_in.1, bf16[640,128]{1,0:T(8,128)(2,1)} %vs_in.1, bf16[640,128]{1,0:T(8,128)(2,1)} %vl_in.1, bf16[640,128]{1,0:T(8,128)(2,1)} %gs_in.1, bf16[640,128]{1,0:T(8,128)(2,1)} %gl_in.1, bf16[2560,128]{1,0:T(8,128)(2,1)} %bitcast.10, bf16[128,2048]{1,0:T(8,128)(2,1)} %ws_in.1, ...), custom_call_target="tpu_custom_call" | custom-call | tf_op jit(solution)/shard_map/pallas_call | solution.py:632
  76.2 1.7 %copy.26 = bf16[80,2048]{1,0:T(8,128)(2,1)} copy(bf16[80,2048]{1,0:T(8,128)(2,1)} %shard_map.217) | data formatting | bytes 655360

commit v5 on v4

--- a/solution.py
+++ b/solution.py
@@ -23,35 +23,35 @@
 H = 1024
 KROWS = 128
 CUT = 352
-Q = 512
-ORDER = (0, 2, 1, 3)
+AFTER = (((0,), ()), ((1,), ()), ((2,), (0,)), ((), (1,)), ((3, 4), ()))
+WIDTHS = (512, 256, 512, 512, 256)
+LOTS = ((0, 48), (48, 32))
 STEPS = (0, 1, -1, 2)
 COLUMNS = (
-    ((0, 0), (0, 1), (0, -1), (1, 0)),
-    ((-1, 0), (-1, 1), (1, 1), (1, -1)),
-    ((-1, -1), (0, 2), (1, 2), (2, 0)),
-    ((2, 1), (-1, 2), (2, -1), (2, 2)),
+    ((0, 0), (-1, 0), (0, -1), (0, 1)),
+    ((1, 0), (-1, -1)),
+    ((1, 1), (0, 2), (2, 0), (-1, 1)),
+    ((1, -1), (2, 1), (1, 2), (-1, 2)),
+    ((2, -1), (2, 2)),
 )
 SENDS = (
     ((0, 0, 0, 0, 1), (0, 0, 0, 0, -1), (1, 0, 0, 0, 1), (1, 0, 0, 0, -1), (0, 0, 0, 1, 1), (0, 0, 0, 1, -1)),
-    ((1, 0, 0, 1, -1), (1, 0, 0, 1, 1)),
-    ((0, 1, 0, 0, -1),),
-    ((1, 1, 0, 0, -1), (1, 1, 0, 1, 1), (0, 1, 0, 1, 1), (1, 1, 0, 1, -1)),
-    ((0, 1, 0, 1, -1),),
-    ((1, -1, 0, 1, 1), (0, -1, 0, 1, 1), (1, -1, 0, 1, -1), (0, -1, 0, 1, -1)),
-    ((1, 2, 0, 1, 1), (0, 2, 0, 1, 1), (1, 2, 0, 1, -1), (0, 2, 0, 1, -1)),
-    ((2, 0, 0, 0, 1), (3, 0, 0, 0, 1), (2, 0, 0, 0, -1), (3, 0, 0, 0, -1), (1, 0, -1, 1, 1), (0, 0, -1, 1, 1)),
-    ((1, 1, 1, 1, -1), (0, 1, 1, 1, -1), (1, -1, -1, 1, 1), (0, -1, -1, 1, 1)),
+    ((1, 0, 0, 1, -1),),
+    ((1, 0, 0, 1, 1),),
+    ((0, 1, 0, 0, -1), (1, 1, 0, 0, -1), (0, 1, 0, 1, 1), (1, 1, 0, 1, 1)),
+    ((1, 1, 0, 1, -1), (0, 1, 0, 1, -1)),
+    ((0, -1, 0, 1, 1), (1, -1, 0, 1, 1), (1, -1, 0, 1, -1)),
+    ((0, 2, 0, 1, -1), (0, 2, 0, 1, 1), (1, 2, 0, 1, 1), (1, 2, 0, 1, -1)),
+    ((0, -1, 0, 1, -1), (3, 0, 0, 0, 1), (2, 0, 0, 0, 1)),
+    ((2, 0, 0, 0, -1), (3, 0, 0, 0, -1), (0, 0, -1, 1, 1), (0, 2, 1, 1, -1), (1, 0, -1, 1, 1), (1, 1, 1, 1, -1)),
+    ((1, 2, -1, 1, 1), (0, 1, -1, 1, 1)),
+    ((2, 1, 0, 0, -1), (3, 1, 0, 0, -1)),
+    ((1, -1, 1, 1, -1), (0, -1, 1, 1, -1), (2, 0, 0, 1, 1), (3, 0, 0, 1, 1), (2, 1, 0, 1, 1)),
+    ((3, 0, 0, 1, -1), (2, 0, 0, 1, -1), (3, 1, 0, 1, 1), (2, -1, 0, 1, 1), (3, -1, 0, 1, 1)),
+    ((3, 2, 0, 1, -1), (2, 2, 0, 1, -1), (2, 2, 0, 1, 1), (3, 2, 0, 1, 1), (3, 1, 0, 1, -1), (2, 1, 0, 1, -1), (3, -1, 0, 1, -1)),
+    ((2, -1, 0, 1, -1), (2, 0, -1, 1, 1), (3, 0, -1, 1, 1), (2, 1, -1, 1, 1), (3, 1, -1, 1, 1)),
+    ((2, 2, 1, 1, -1), (3, 2, 1, 1, -1), (2, -1, -1, 1, 1), (3, -1, -1, 1, 1)),
     (),
-    ((1, 2, 1, 1, -1), (2, -1, 0, 0, 1), (0, 2, 1, 1, -1), (3, -1, 0, 0, 1), (3, 0, 0, 1, -1), (3, 0, 0, 1, 1), (2, 0, 0, 1, -1), (2, 0, 0, 1, 1), (3, -1, 0, 1, -1)),
-    ((3, 1, 0, 1, 1), (2, 1, 0, 1, -1), (2, 1, 0, 1, 1), (3, 1, 0, 1, -1), (3, -1, 0, 1, 1), (2, -1, 0, 1, -1), (2, -1, 0, 1, 1)),
-    ((3, 2, 0, 1, -1), (3, 2, 0, 1, 1), (2, 2, 0, 1, -1), (2, 2, 0, 1, 1)),
-    ((3, 0, 1, 1, -1), (3, 1, -1, 1, 1), (2, 0, 1, 1, -1), (2, 1, -1, 1, 1)),
-    ((3, -1, 1, 1, -1),),
-    (),
-    ((2, -1, 1, 1, -1),),
-    (),
-    ((2, 2, -1, 1, 1), (3, 2, -1, 1, 1)),
     (),
     (),
     (),
@@ -61,24 +61,22 @@
     (),
     ((0, -1, 0), (0, 1, 0), (1, -1, 0), (1, 1, 0)),
     (),
-    ((0, 0, -1), (0, 0, 1), (1, 0, 1)),
+    ((0, 0, -1), (0, 0, 1)),
+    ((1, 0, 1),),
+    ((1, 0, -1), (0, 2, 0), (1, 2, 0)),
+    ((0, 1, -1), (1, 1, -1), (1, 1, 1), (0, 1, 1)),
+    ((0, -1, -1), (1, -1, -1), (1, -1, 1), (0, 2, 1)),
+    ((0, 2, -1), (1, 2, -1)),
+    ((1, 2, 1), (0, -1, 1), (3, -1, 0), (2, -1, 0), (2, 1, 0), (3, 1, 0)),
     (),
-    ((1, 0, -1), (0, 2, 0), (1, 2, 0)),
-    ((1, 1, -1), (0, 1, -1), (1, 1, 1), (0, 1, 1)),
-    ((1, -1, -1), (0, -1, -1), (1, -1, 1), (0, -1, 1)),
-    ((1, 2, -1), (0, 2, -1), (1, 2, 1), (2, -1, 0), (0, 2, 1), (3, -1, 0)),
+    ((0, 0, 2), (1, 0, 2), (1, 1, 2), (0, 2, 2)),
+    ((2, 2, 0), (3, 2, 0), (0, 1, 2), (1, 2, 2), (1, -1, 2), (0, -1, 2)),
+    ((2, 0, -1), (3, 0, -1), (2, 1, -1), (3, 1, -1), (3, 0, 1), (2, 0, 1), (2, -1, -1), (3, -1, -1)),
+    ((3, 2, 1), (2, 2, 1), (2, 2, -1), (3, 2, -1), (3, 1, 1), (2, 1, 1), (2, 0, 2), (3, 0, 2), (3, -1, 1)),
+    ((2, -1, 1), (2, 1, 2), (3, 1, 2), (3, -1, 2)),
+    ((2, 2, 2), (3, 2, 2), (2, -1, 2)),
     (),
-    ((2, 1, 0), (3, 1, 0), (1, 0, 2), (0, 0, 2), (1, 1, 2), (0, 1, 2)),
-    ((1, -1, 2), (0, -1, 2), (1, 2, 2), (2, 2, 0), (0, 2, 2), (3, 2, 0)),
-    ((3, 0, 1), (3, 0, -1), (2, 0, 1), (2, 0, -1), (3, -1, 1), (3, 1, -1), (2, 1, 1), (2, 1, -1)),
-    ((3, 1, 1),),
-    ((3, -1, -1),),
-    ((2, -1, 1), (2, -1, -1)),
-    ((3, 2, 1),),
-    ((3, 2, -1), (2, 2, 1), (2, 2, -1)),
     (),
-    ((3, 0, 2), (3, 1, 2), (2, 0, 2), (2, 1, 2)),
-    ((3, -1, 2), (2, -1, 2), (2, 2, 2), (3, 2, 2)),
 )
 
 head_eps = 1e-05
@@ -103,10 +101,13 @@
 
 def kernel(
     res_in, vs_in, vl_in, gs_in, gl_in, sp_in, ws_in, wl_in, g_in, u_in, d_in,
-    steps_s, steps_l, offs_s, offs_l, rates_s, rates_l, taps_s, taps_l, taps_m, gain_s, gain_l, gain_n,
-    out,
-    xin, sxin, gin, resv, halo, halo_m, cbuf, cmaps, conv_k, drive, fresh, inner, heads, hpart, lhs,
-    wo, wg, wu, wd, st1, st2, psend, rp, rm, ag, hid, psend2, rp2, rm2, midv,
+    small_in_0, small_in_1, small_in_2, small_in_3, small_in_4, small_in_5, small_in_6, small_in_7,
+    small_in_8, small_in_9, small_in_10, small_in_11,
+    out_hbm,
+    small, out, out_sem,
+    xin, sxin, gin, resv, halo, halo_m, cbuf, cmaps, conv_k, drive, fresh, inner, heads, hpart_0, hpart_1, lhs_0, lhs_1,
+    wo, wg, wu, wd, st1, st2, parts_0, parts_1, left_0, left_1, right_0, right_1, ag, hid,
+    dparts, dleft, dright, mid_0, mid_1,
     loc_sem, halo_sem, w_send, w_recv, pair_sem, st_sem, hp_sem, rs_sem, ag_sem, rs2_sem,
 ):
     z, y, x, c = (lax.axis_index(n) for n in ("z", "y", "x", "c"))
@@ -137,7 +138,20 @@
         pending.append(cp)
         return cp
 
+    barrier = pltpu.get_barrier_semaphore()
+    peers = [
+        dict(c=o), dict(x=at(x, 1)), dict(x=at(x, 3)),
+        dict(y=at(y, 1)), dict(y=at(y, 2)), dict(y=at(y, 3)),
+        dict(z=at(z, 1)), dict(z=at(z, 2)), dict(z=at(z, 3)),
+        nxt, prv,
+    ]
+    for p in peers:
+        pl.semaphore_signal(barrier, inc=1, device_id=there(**p), device_id_type=pl.DeviceIdType.MESH)
     local = [
+        *zip(
+            (small_in_0, small_in_1, small_in_2, small_in_3, small_in_4, small_in_5, small_in_6,
+             small_in_7, small_in_8, small_in_9, small_in_10, small_in_11), small,
+        ),
         (vs_in, xin.at[:, pl.ds(0, 128)]),
         (vl_in, xin.at[:, pl.ds(128, 128)]),
         (sp_in, sxin),
@@ -153,16 +167,9 @@
     local = [pltpu.make_async_copy(a, b, loc_sem.at[i]) for i, (a, b) in enumerate(local)]
     for cp in local:
         cp.start()
-
-    barrier = pltpu.get_barrier_semaphore()
-    peers = [
-        dict(c=o), dict(x=at(x, 1)), dict(x=at(x, 3)),
-        dict(y=at(y, 1)), dict(y=at(y, 2)), dict(y=at(y, 3)),
-        dict(z=at(z, 1)), dict(z=at(z, 2)), dict(z=at(z, 3)),
-        nxt, prv,
-    ]
-    for p in peers:
-        pl.semaphore_signal(barrier, inc=1, device_id=there(**p), device_id_type=pl.DeviceIdType.MESH)
+    fetched, local = local[:12], local[12:]
+    steps_s, steps_l, offs_s, offs_l, rates_s, rates_l, taps_s, taps_l, taps_m, gain_s, gain_l, gain_n = small
+
     pl.semaphore_wait(barrier, len(peers))
 
     tail = pl.ds(T - 16, 16)
@@ -243,10 +250,12 @@
     pump(0)
 
     wo_copies = [
-        go(remote(src, wo.at[c, rows], hp_sem.at[0, 4 + i], hp_sem.at[1, 4 + i], c=o))
+        go(remote(src, wo.at[c, rows], hp_sem.at[0, 8 + i], hp_sem.at[1, 8 + i], c=o))
         for i, (src, rows) in enumerate(((ws_in, pl.ds(0, 128)), (wl_in, pl.ds(128, 128))))
     ]
 
+    for cp in fetched:
+        cp.wait()
     lane = lax.broadcasted_iota(jnp.int32, (8, L), 1)
     rows = []
     both = []
@@ -254,7 +263,7 @@
     raw_steps = jnp.concatenate([steps_s[...].astype(F32), steps_l[...].astype(F32)], axis=0)
     softened = jnp.maximum(raw_steps, 0.0) + jnp.log1p(jnp.exp(-jnp.abs(raw_steps)))
     head = lax.broadcasted_iota(jnp.int32, (3, T), 0)
-    rate = jnp.where(head == 0, rates_s[0], jnp.where(head == 1, rates_s[1], rates_l[0]))
+    rate = jnp.where(head == 0, rates_s[0:1, 0:1], jnp.where(head == 1, rates_s[0:1, 1:2], rates_l[0:1, 0:1]))
     offsets = jnp.concatenate([offs_s[...], offs_l[...]], axis=0)
     meta = jnp.concatenate(
         [offsets - jnp.exp(rate) * softened, softened, jnp.zeros((2, T), F32)], axis=0
@@ -445,171 +454,257 @@
         if kind == 0:
             pump(4)
 
-    def rows_of(b, core):
-        return pl.ds(pl.multiple_of((2 * b + core) * R, 16), R)
-
-    for b in range(4):
-        go(remote(heads.at[rows_of(b, o)], hpart.at[b], hp_sem.at[0, b], hp_sem.at[1, b], c=o))
-    for b in range(4):
-        lhs[b] = heads[rows_of(b, c), :]
+    hpart, lhs = (hpart_0, hpart_1), (lhs_0, lhs_1)
+    parts, left, right = (parts_0, parts_1), (left_0, left_1), (right_0, right_1)
+    mid = (mid_0, mid_1)
+
+    def rows_of(b, core, t):
+        first, n = LOTS[t]
+        return pl.ds(pl.multiple_of((2 * b + core) * R + first, 16), n)
+
+    def block_of(b, t):
+        n = LOTS[t][1]
+        return pl.ds(b * n if isinstance(b, int) else pl.multiple_of(b * n, 16), n)
+
+    def row_of(b, t):
+        first, n = LOTS[t]
+        return pl.ds(pl.multiple_of(4 * first + b * n, 16), n)
+
+    hp_copies = [
+        [
+            go(remote(
+                heads.at[rows_of(b, o, t)], hpart[t].at[block_of(b, t)],
+                hp_sem.at[0, 4 * t + b], hp_sem.at[1, 4 * t + b], c=o,
+            ))
+            for b in range(4)
+        ]
+        for t in range(2)
+    ]
+    for t in range(2):
+        for b in range(4):
+            lhs[t][block_of(b, t), :] = heads[rows_of(b, c, t), :]
+    pump(5)
     for i in (6, 7):
         local[i].wait()
-    own_rows = lhs[...].reshape(4 * R, 256)
     for cp in wo_copies:
         cp.wait_recv()
-    pump(5)
-    for b in range(4):
-        remote(hpart.at[b], hpart.at[b], hp_sem.at[0, b], hp_sem.at[1, b]).wait_recv()
-    part_rows = hpart[...].reshape(4 * R, 256)
 
     x1, x2, x3 = at(x, 1), at(x, 2), at(x, 3)
 
     class Sum:
-        def __init__(self, parts, from_left, from_right, sems):
-            self.parts, self.left, self.right, self.sems = parts, from_left, from_right, sems
-
-        def to_right(self, slot, block, h):
-            go(remote(self.parts.at[block, h], self.left.at[slot], self.sems.at[0, slot], self.sems.at[1, slot], x=x1))
-
-        def to_left(self, slot, block, h):
-            go(remote(self.parts.at[block, h], self.right.at[slot], self.sems.at[2, slot], self.sems.at[3, slot], x=x3))
+        def __init__(self, part, from_left, from_right, sem):
+            self.part, self.left, self.right, self.sem = part, from_left, from_right, sem
+
+        def to_right(self, slot, block, role):
+            go(remote(self.part(block, role), self.left(slot), self.sem(0, slot), self.sem(1, slot), x=x1))
+
+        def to_left(self, slot, block, role):
+            go(remote(self.part(block, role), self.right(slot), self.sem(2, slot), self.sem(3, slot), x=x3))
 
         def wait_left(self, slot):
-            remote(self.left.at[slot], self.left.at[slot], self.sems.at[0, slot], self.sems.at[1, slot]).wait_recv()
+            ref = self.left(slot)
+            remote(ref, ref, self.sem(0, slot), self.sem(1, slot)).wait_recv()
+            return ref[...].astype(F32)
 
         def wait_right(self, slot):
-            remote(self.right.at[slot], self.right.at[slot], self.sems.at[2, slot], self.sems.at[3, slot]).wait_recv()
-
-        def after_quarter(self, q):
-            if q < 2:
-                self.to_right(q, x2, q)
-                self.to_left(q + 2, x3, q)
-            else:
-                self.to_left(q - 2, x2, q)
-                self.to_right(q, x1, q)
-
-        def merge(self, i):
-            p = self.parts
-            self.wait_left(i)
-            p[x1, i] = (p[x1, i].astype(F32) + self.left[i].astype(F32)).astype(BF16)
-            self.to_right(4 + i, x1, i)
-            self.wait_right(i)
-            p[x3, 2 + i] = (p[x3, 2 + i].astype(F32) + self.right[i].astype(F32)).astype(BF16)
-            self.to_left(4 + i, x3, 2 + i)
-
-        def result(self, q):
-            a, b = (4 + q, 2 + q) if q < 2 else (q, 2 + q)
-            self.wait_left(a)
-            self.wait_right(b)
-            return self.parts[x, q].astype(F32) + self.left[a].astype(F32) + self.right[b].astype(F32)
-
-    mixed = Sum(psend, rp, rm, rs_sem)
-    for q in ORDER:
-        for e in range(2):
-            n = pl.ds(q * Q + e * 256, 256)
-            acc = dot(own_rows, wo[c, :, n]) + dot(part_rows, wo[o, :, n])
-            psend[:, q, :, e * 256 : (e + 1) * 256] = acc.reshape(4, R, 256).astype(BF16)
-        mixed.after_quarter(q)
+            ref = self.right(slot)
+            remote(ref, ref, self.sem(2, slot), self.sem(3, slot)).wait_recv()
+            return ref[...].astype(F32)
+
+        def relayed(self):
+            self.to_right(0, x2, 0)
+            self.to_left(0, x2, 1)
+
+        def direct(self):
+            self.to_right(1, x1, 1)
+            self.to_left(1, x3, 0)
+
+        def merge(self):
+            mine = self.part(x1, 0)
+            mine[...] = (self.wait_left(0) + mine[...].astype(F32)).astype(BF16)
+            self.to_right(2, x1, 0)
+            mine = self.part(x3, 1)
+            mine[...] = (self.wait_right(0) + mine[...].astype(F32)).astype(BF16)
+            self.to_left(2, x3, 1)
+
+        def result(self, role):
+            a, b = (2, 1) if role == 0 else (1, 2)
+            return self.part(x, role)[...].astype(F32) + self.wait_left(a) + self.wait_right(b)
+
+    def mixed_sum(t):
+        return Sum(
+            lambda block, role: parts[t].at[block, role],
+            lambda slot: left[t].at[slot], lambda slot: right[t].at[slot],
+            lambda k, slot: rs_sem.at[t, k, slot],
+        )
+
+    mixed = [mixed_sum(0), mixed_sum(1)]
+
+    def project(t):
+        n = LOTS[t][1]
+        for cp in hp_copies[t]:
+            cp.wait_recv()
+        mine, other = lhs[t][...], hpart[t][...]
+        for role in range(2):
+            for e in range(4):
+                cols_e = pl.ds(role * H + e * 256, 256)
+                acc = dot(mine, wo[c, :, cols_e]) + dot(other, wo[o, :, cols_e])
+                parts[t][:, role, :, e * 256 : (e + 1) * 256] = acc.reshape(4, n, 256).astype(BF16)
+
+    project(0)
+    mixed[0].relayed()
+    mixed[0].direct()
+    project(1)
+    mixed[1].relayed()
     pump(6)
-    mixed.merge(0)
+    mixed[0].merge()
+    mixed[1].direct()
     pump(7)
-    mixed.merge(1)
+    mixed[1].merge()
     pump(8)
     local[5].wait()
-    sums = {q: mixed.result(q) for q in (2, 3)}
+
+    def norm(t):
+        first, n = LOTS[t]
+        wide = []
+        for role in range(2):
+            at_role = slice(role * H, role * H + H)
+            m = (resv[first : first + n, at_role].astype(F32) + mixed[t].result(role)).astype(BF16)
+            mid[t][:, at_role] = m
+            wide.append(m.astype(F32))
+        square = sum(jnp.sum(w * w, axis=1, keepdims=True) for w in wide)
+        scale = lax.rsqrt(square * (1.0 / DM) + row_eps)
+        for role in range(2):
+            at_role = slice(role * H, role * H + H)
+            ag[role, row_of(x, t), :] = (wide[role] * scale * gain_n[:, at_role]).astype(BF16)
+
+    def ag_right(t, slot, block, role):
+        ref = ag.at[role, row_of(block, t)]
+        go(remote(ref, ref, ag_sem.at[t, 0, slot], ag_sem.at[t, 1, slot], x=x1))
+
+    def ag_left(t, slot, block, role):
+        ref = ag.at[role, row_of(block, t)]
+        go(remote(ref, ref, ag_sem.at[t, 2, slot], ag_sem.at[t, 3, slot], x=x3))
+
+    def ag_wait(t, side, slot, block, role):
+        ref = ag.at[role, row_of(block, t)]
+        remote(ref, ref, ag_sem.at[t, 0, slot], ag_sem.at[t, side, slot]).wait_recv()
+
+    def ag_relay(t):
+        ag_wait(t, 1, 0, x3, 0)
+        ag_right(t, 2, x3, 0)
+        ag_wait(t, 3, 0, x1, 1)
+        ag_left(t, 2, x1, 1)
+
+    def ag_rest(t):
+        ag_wait(t, 1, 1, x3, 1)
+        ag_wait(t, 3, 1, x1, 0)
+        ag_wait(t, 1, 2, x2, 0)
+        ag_wait(t, 3, 2, x2, 1)
+
+    norm(0)
+    ag_right(0, 0, x, 0)
+    ag_left(0, 0, x, 1)
+    ag_right(0, 1, x, 1)
+    ag_left(0, 1, x, 0)
     pump(9)
-    sums.update({q: mixed.result(q) for q in (0, 1)})
-    lo = jnp.concatenate([sums[0], sums[1]], axis=1)
-    hi = jnp.concatenate([sums[2], sums[3]], axis=1)
-    mid_lo = (resv[:, 0:H].astype(F32) + lo).astype(BF16)
-    mid_hi = (resv[:, H:DM].astype(F32) + hi).astype(BF16)
-    midv[:, 0:H] = mid_lo
-    midv[:, H:DM] = mid_hi
-    f_lo, f_hi = mid_lo.astype(F32), mid_hi.astype(F32)
-    square = jnp.sum(f_lo * f_lo, axis=1, keepdims=True) + jnp.sum(f_hi * f_hi, axis=1, keepdims=True)
-    scale = lax.rsqrt(square * (1.0 / DM) + row_eps)
-    ag[x, 0] = (f_lo * scale * gain_n[:, 0:H]).astype(BF16)
-    ag[x, 1] = (f_hi * scale * gain_n[:, H:DM]).astype(BF16)
-
-    def ag_right(slot, block, h):
-        go(remote(ag.at[block, h], ag.at[block, h], ag_sem.at[0, slot], ag_sem.at[1, slot], x=x1))
-
-    def ag_left(slot, block, h):
-        go(remote(ag.at[block, h], ag.at[block, h], ag_sem.at[2, slot], ag_sem.at[3, slot], x=x3))
-
-    def ag_wait(side, slot, block, h):
-        remote(ag.at[block, h], ag.at[block, h], ag_sem.at[0, slot], ag_sem.at[side, slot]).wait_recv()
-
-    ag_right(0, x, 0)
-    ag_left(0, x, 1)
-    ag_right(1, x, 1)
-    ag_left(1, x, 0)
-
+    norm(1)
+    ag_right(1, 0, x, 0)
+    ag_left(1, 0, x, 1)
     pump(10)
-    ag_wait(1, 0, x3, 0)
-    ag_right(2, x3, 0)
-    ag_wait(3, 0, x1, 1)
-    ag_left(2, x1, 1)
+    ag_relay(0)
+    ag_right(1, 1, x, 1)
+    ag_left(1, 1, x, 0)
     pump(11)
-    ag_wait(1, 1, x3, 1)
-    ag_wait(3, 1, x1, 0)
+    ag_relay(1)
     pump(12)
-    ag_wait(1, 2, x2, 0)
-    ag_wait(3, 2, x2, 1)
+    ag_rest(0)
     pump(13)
+    ag_rest(1)
     for i in (8, 9, 10):
         local[i].wait()
+
     def lined_up(w, core, h, n0, n):
-        parts = [w[core, 2 * h + j // 4, j % 4, n0 : n0 + n, :] for j in range(8)]
-        return jnp.concatenate(parts, axis=1)
-
-    def expand(core, points):
+        pieces = [w[core, 2 * h + j // 4, j % 4, n0 : n0 + n, :] for j in range(8)]
+        return jnp.concatenate(pieces, axis=1)
+
+    def expand(core):
         for n0, n in ((0, 256), (256, 256), (512, 192)):
-            if n0 > 0:
-                pump(points[n0 // 256 - 1])
             gate = up = None
             for h in range(2):
-                a = ag[:, h].reshape(4 * R, H)
+                a = ag[h]
                 w_gate = lined_up(wg, core, h, n0, n)
                 w_up = lined_up(wu, core, h, n0, n)
                 gate = dot_nt(a, w_gate) if gate is None else gate + dot_nt(a, w_gate)
                 up = dot_nt(a, w_up) if up is None else up + dot_nt(a, w_up)
             hid[core, :, n0 : n0 + n] = (silu(gate) * up).astype(BF16)
 
-    expand(c, (14, 15))
-    pump(16)
+    expand(c)
+    pump(14)
     for name in ("G", "U"):
         for f in STEPS:
-            for s in STEPS:
-                pair_wait(name, f, s)
-    expand(o, (17, 18))
-    pump(19)
-
-    down = Sum(psend2, rp2, rm2, rs2_sem)
-    for i, q in enumerate(ORDER):
-        if i >= 2:
-            pump(18 + i)
+            for st in STEPS:
+                pair_wait(name, f, st)
+    expand(o)
+
+    def rows_in(i, role):
+        return role if i % 2 == 0 else 1 - role
+
+    def down_sum(i):
+        return Sum(
+            lambda block, role: dparts[i][rows_in(i, role)].at[block],
+            lambda slot: dleft[i][rows_in(i, slot % 2)].at[slot],
+            lambda slot: dright[i][rows_in(i, 1 - slot % 2)].at[slot],
+            lambda k, slot: rs2_sem.at[i, k, slot],
+        )
+
+    down = [down_sum(i) for i in range(5)]
+
+    outgoing = []
+
+    def finish(i):
+        for role in range(2):
+            t = rows_in(i, role)
+            first, n = LOTS[t]
+            total = down[i].result(role)
+            for j, (rz, ry) in enumerate(COLUMNS[i]):
+                at_j = pl.ds(pl.multiple_of((at(z, rz) * 4 + at(y, ry)) * 128, 128), 128)
+                out[first : first + n, at_j] = (
+                    mid[t][:, at_j].astype(F32) + total[:, 128 * j : 128 * j + 128]
+                ).astype(BF16)
+                place_j = (pl.ds(first, n), at_j)
+                cp = pltpu.make_async_copy(out.at[place_j], out_hbm.at[place_j], out_sem.at[len(outgoing)])
+                cp.start()
+                outgoing.append(cp)
+
+    for i in range(5):
         for rz, ry in COLUMNS[i]:
             for name in ("A", "B"):
-                f, s = place(name, rz, ry)
-                pair_wait(name, f, s)
-        for e in range(2):
+                pair_wait(name, *place(name, rz, ry))
+        for e in range(WIDTHS[i] // 256):
             acc = None
             for cc in range(2):
                 w_down = jnp.concatenate(
                     [wd[cc, at(z, rz), at(y, ry)] for rz, ry in COLUMNS[i][2 * e : 2 * e + 2]], axis=1
                 )
                 acc = dot(hid[cc], w_down) if acc is None else acc + dot(hid[cc], w_down)
-            psend2[:, q, :, e * 256 : (e + 1) * 256] = acc.reshape(4, R, 256).astype(BF16)
-        down.after_quarter(q)
-    down.merge(0)
-    down.merge(1)
-    for i, q in ((1, 2), (3, 3), (0, 0), (2, 1)):
-        total = down.result(q)
-        for j, (rz, ry) in enumerate(COLUMNS[i]):
-            n = pl.ds(pl.multiple_of((at(z, rz) * 4 + at(y, ry)) * 128, 128), 128)
-            out[:, n] = (midv[:, n].astype(F32) + total[:, 128 * j : 128 * j + 128]).astype(BF16)
-
+            for t, (first, n) in enumerate(LOTS):
+                lot_acc = acc[4 * first : 4 * first + 4 * n].reshape(4, n, 256)
+                dparts[i][t][:, :, e * 256 : (e + 1) * 256] = lot_acc.astype(BF16)
+        down[i].relayed()
+        for j in AFTER[i][0]:
+            down[j].direct()
+        for j in AFTER[i][1]:
+            down[j].merge()
+        pump(15 + i)
+    down[2].merge()
+    down[3].merge()
+    down[4].merge()
+    for i in range(5):
+        finish(i)
+
+    for cp in outgoing:
+        cp.wait()
     for cp in pending:
         cp.wait_send()
 
@@ -625,16 +720,21 @@
     flat = state_projections.reshape(4 * T, 128)
 
     anywhere = pl.BlockSpec(memory_space=pl.ANY)
-    vmem = pl.BlockSpec(memory_space=pltpu.VMEM)
-    smem = pl.BlockSpec(memory_space=pltpu.SMEM)
     dma = pltpu.SemaphoreType.DMA
     V = pltpu.VMEM
     return pl.pallas_call(
         kernel,
         out_shape=jax.ShapeDtypeStruct((R, DM), BF16),
-        in_specs=[anywhere] * 11 + [vmem] * 4 + [smem] * 2 + [vmem] * 6,
-        out_specs=vmem,
+        in_specs=[anywhere] * 23,
+        out_specs=anywhere,
         scratch_shapes=[
+            [
+                V((2, T), BF16), V((1, T), BF16), V((2, T), F32), V((1, T), F32), V((1, 2), F32), V((1, 1), F32),
+                V((4, 128), BF16), V((4, 128), BF16), V((4, 4, 128), BF16), V((1, 128), F32), V((1, 128), F32),
+                V((1, DM), F32),
+            ],
+            V((R, DM), BF16),
+            dma((32,)),
             V((T, 256), BF16),
             V((4 * T, 128), BF16),
             V((T, 256), BF16),
@@ -648,33 +748,33 @@
             V((NB, 128, 256), F32),
             V((T, 256), F32),
             V((T, 256), BF16),
-            V((4, R, 256), BF16),
-            V((4, R, 256), BF16),
+            *[V((4 * n, 256), BF16) for _, n in LOTS],
+            *[V((4 * n, 256), BF16) for _, n in LOTS],
             V((2, 256, DM), BF16),
             V((2, 4, 4, FD, KROWS), BF16),
             V((2, 4, 4, FD, KROWS), BF16),
             V((2, 4, 4, FD, KROWS), BF16),
             V((2, 4, 136, 128), BF16),
             V((2, 4, 136, 128), BF16),
-            V((4, 4, R, Q), BF16),
-            V((6, R, Q), BF16),
-            V((6, R, Q), BF16),
-            V((4, 2, R, H), BF16),
+            *[V((4, 2, n, H), BF16) for _, n in LOTS],
+            *[V((3, n, H), BF16) for _, n in LOTS],
+            *[V((3, n, H), BF16) for _, n in LOTS],
+            V((2, 4 * R, H), BF16),
             V((2, 4 * R, FD), BF16),
-            V((4, 4, R, Q), BF16),
-            V((6, R, Q), BF16),
-            V((6, R, Q), BF16),
-            V((R, DM), BF16),
-            dma((11,)),
+            [[V((4, n, w), BF16) for _, n in LOTS] for w in WIDTHS],
+            [[V((3, n, w), BF16) for _, n in LOTS] for w in WIDTHS],
+            [[V((3, n, w), BF16) for _, n in LOTS] for w in WIDTHS],
+            *[V((n, DM), BF16) for _, n in LOTS],
+            dma((23,)),
             dma((2, 3)),
             dma((60,)),
             dma((4, 4, 4)),
             dma((2, 64)),
             dma((4, 2, 4)),
-            dma((2, 6)),
-            dma((4, 6)),
-            dma((4, 3)),
-            dma((4, 6)),
+            dma((2, 10)),
+            dma((2, 4, 3)),
+            dma((2, 4, 3)),
+            dma((5, 4, 3)),
         ],
         compiler_params=pltpu.CompilerParams(
             collective_id=0, has_side_effects=True, vmem_limit_bytes=60 * 1024 * 1024
@@ -683,7 +783,7 @@
         residual, small_value_inputs, large_value_inputs, small_gate_inputs, large_gate_inputs,
         flat, small_output_projection, large_output_projection, gate_matrix.T, up_matrix.T, down_matrix,
         small_step_inputs.T, large_step_inputs.T, small_decay_offsets.T, large_decay_offsets.T,
-        small_decay_rates, large_decay_rates, small_filter_taps, large_filter_taps, state_filter_taps,
+        small_decay_rates.reshape(1, 2), large_decay_rates.reshape(1, 1), small_filter_taps, large_filter_taps, state_filter_taps,
         small_head_gains.reshape(1, 128), large_head_gains.reshape(1, 128),
         channel_norm_gain.reshape(1, DM),
     )

time: 78.1 us -> 76.3 us (0.977)
  Pallas kernels: 75.5 us -> 73.8 us
    pallas_call x1, Pallas kernels: 75.5 us -> 73.8 us  [on_device(): pl.pallas_call(kernel, out_shape=jax.ShapeDtypeStruct((R, DM), BF16), in_...]
where the time goes in v5:
time: 76.3 us; the launch traced here: 76.2 us
  Pallas kernels  73.8 us (97%)
  local copies, waits for them, and re-layouts  1.72 us (2%)
    pallas_call x1, Pallas kernels, on_device(): pl.pallas_call(kernel, out_shape=jax.ShapeDtypeStruct((R, DM), BF16), in_...  73.8 us
    unnamed x1, local copies, waits for them, and re-layouts  1.72 us

profile of v5, /device:TPU:1, one launch (start us, length us, event | category | flops | bytes accessed | tf_op | source)
XLA Modules:
  0.0 76.2 jit_solution(14427861123351771830)
XLA Ops:
  0.7 73.8 %shard_map.217 = bf16[80,2048]{1,0:T(8,128)(2,1)} custom-call(bf16[80,2048]{1,0:T(8,128)(2,1)} %res_in.1, bf16[640,128]{1,0:T(8,128)(2,1)} %vs_in.1, bf16[640,128]{1,0:T(8,128)(2,1)} %vl_in.1, bf16[640,128]{1,0:T(8,128)(2,1)} %gs_in.1, bf16[640,128]{1,0:T(8,128)(2,1)} %gl_in.1, bf16[2560,128]{1,0:T(8,128)(2,1)} %bitcast.13, bf16[128,2048]{1,0:T(8,128)(2,1)} %ws_in.1, ...), custom_call_target="tpu_custom_call" | custom-call | tf_op jit(solution)/shard_map/pallas_call | solution.py:725
  74.5 1.7 %copy.26 = bf16[80,2048]{1,0:T(8,128)(2,1)} copy(bf16[80,2048]{1,0:T(8,128)(2,1)} %shard_map.217) | data formatting | bytes 655360

commit v6 on v5

--- a/solution.py
+++ b/solution.py
@@ -23,7 +23,7 @@
 H = 1024
 KROWS = 128
 CUT = 352
-AFTER = (((0,), ()), ((1,), ()), ((2,), (0,)), ((), (1,)), ((3, 4), ()))
+AFTER = (((0,), (), ()), ((1,), (), (15,)), ((2,), (0,), (16, 17)), ((), (1,), ()), ((3, 4), (), (18, 19)))
 WIDTHS = (512, 256, 512, 512, 256)
 LOTS = ((0, 48), (48, 32))
 STEPS = (0, 1, -1, 2)
@@ -103,8 +103,8 @@
     res_in, vs_in, vl_in, gs_in, gl_in, sp_in, ws_in, wl_in, g_in, u_in, d_in,
     small_in_0, small_in_1, small_in_2, small_in_3, small_in_4, small_in_5, small_in_6, small_in_7,
     small_in_8, small_in_9, small_in_10, small_in_11,
-    out_hbm,
-    small, out, out_sem,
+    out,
+    small,
     xin, sxin, gin, resv, halo, halo_m, cbuf, cmaps, conv_k, drive, fresh, inner, heads, hpart_0, hpart_1, lhs_0, lhs_1,
     wo, wg, wu, wd, st1, st2, parts_0, parts_1, left_0, left_1, right_0, right_1, ag, hid,
     dparts, dleft, dright, mid_0, mid_1,
@@ -660,8 +660,6 @@
 
     down = [down_sum(i) for i in range(5)]
 
-    outgoing = []
-
     def finish(i):
         for role in range(2):
             t = rows_in(i, role)
@@ -672,12 +670,10 @@
                 out[first : first + n, at_j] = (
                     mid[t][:, at_j].astype(F32) + total[:, 128 * j : 128 * j + 128]
                 ).astype(BF16)
-                place_j = (pl.ds(first, n), at_j)
-                cp = pltpu.make_async_copy(out.at[place_j], out_hbm.at[place_j], out_sem.at[len(outgoing)])
-                cp.start()
-                outgoing.append(cp)
 
     for i in range(5):
+        if i == 2:
+            settled = len(pending)
         for rz, ry in COLUMNS[i]:
             for name in ("A", "B"):
                 pair_wait(name, *place(name, rz, ry))
@@ -696,15 +692,17 @@
             down[j].direct()
         for j in AFTER[i][1]:
             down[j].merge()
-        pump(15 + i)
+        for j in AFTER[i][2]:
+            pump(j)
     down[2].merge()
+    for cp in pending[:settled]:
+        cp.wait_send()
+    del pending[:settled]
     down[3].merge()
     down[4].merge()
     for i in range(5):
         finish(i)
 
-    for cp in outgoing:
-        cp.wait()
     for cp in pending:
         cp.wait_send()
 
@@ -724,17 +722,15 @@
     V = pltpu.VMEM
     return pl.pallas_call(
         kernel,
-        out_shape=jax.ShapeDtypeStruct((R, DM), BF16),
+        out_shape=pltpu.VMEM((R, DM), BF16),
         in_specs=[anywhere] * 23,
-        out_specs=anywhere,
+        out_specs=pl.BlockSpec(memory_space=pltpu.VMEM),
         scratch_shapes=[
             [
                 V((2, T), BF16), V((1, T), BF16), V((2, T), F32), V((1, T), F32), V((1, 2), F32), V((1, 1), F32),
                 V((4, 128), BF16), V((4, 128), BF16), V((4, 4, 128), BF16), V((1, 128), F32), V((1, 128), F32),
                 V((1, DM), F32),
             ],
-            V((R, DM), BF16),
-            dma((32,)),
             V((T, 256), BF16),
             V((4 * T, 128), BF16),
             V((T, 256), BF16),

time: 76.3 us -> 74 us (0.970)
  Pallas kernels: 73.8 us -> 72.5 us
  local copies, waits for them, and re-layouts: 1.72 us -> 0.73 us
    pallas_call x1, Pallas kernels: 73.8 us -> 72.5 us  [on_device(): pl.pallas_call(kernel, out_shape=pltpu.VMEM((R, DM), BF16), in_specs=[any...]
    unnamed x1, local copies, waits for them, and re-layouts: 1.72 us -> 0.73 us
where the time goes in v6:
time: 74 us; the launch traced here: 73.9 us
  Pallas kernels  72.5 us (98%)
    pallas_call x1, Pallas kernels, on_device(): pl.pallas_call(kernel, out_shape=pltpu.VMEM((R, DM), BF16), in_specs=[any...  72.5 us

profile of v6, /device:TPU:1, one launch (start us, length us, event | category | flops | bytes accessed | tf_op | source)
XLA Modules:
  0.0 73.9 jit_solution(4273652792897005601)
XLA Ops:
  0.7 72.5 %shard_map.217 = bf16[80,2048]{1,0:T(8,128)(2,1)S(1)} custom-call(bf16[80,2048]{1,0:T(8,128)(2,1)} %res_in.1, bf16[640,128]{1,0:T(8,128)(2,1)} %vs_in.1, bf16[640,128]{1,0:T(8,128)(2,1)} %vl_in.1, bf16[640,128]{1,0:T(8,128)(2,1)} %gs_in.1, bf16[640,128]{1,0:T(8,128)(2,1)} %gl_in.1, bf16[2560,128]{1,0:T(8,128)(2,1)} %bitcast.13, bf16[128,2048]{1,0:T(8,128)(2,1)} %ws_in.1, ...), custom_call_target="tpu_custom_call" | custom-call | tf_op jit(solution)/shard_map/pallas_call | solution.py:723
  73.2 0.7 copy.25

commit v7 on v6

--- a/solution.py
+++ b/solution.py
@@ -28,29 +28,29 @@
 LOTS = ((0, 48), (48, 32))
 STEPS = (0, 1, -1, 2)
 COLUMNS = (
-    ((0, 0), (-1, 0), (0, -1), (0, 1)),
-    ((1, 0), (-1, -1)),
-    ((1, 1), (0, 2), (2, 0), (-1, 1)),
-    ((1, -1), (2, 1), (1, 2), (-1, 2)),
+    ((0, 0), (1, 0), (0, 1), (-1, 0)),
+    ((0, -1), (1, 1)),
+    ((1, -1), (-1, 1), (-1, -1), (2, 0)),
+    ((0, 2), (1, 2), (2, 1), (-1, 2)),
     ((2, -1), (2, 2)),
 )
 SENDS = (
     ((0, 0, 0, 0, 1), (0, 0, 0, 0, -1), (1, 0, 0, 0, 1), (1, 0, 0, 0, -1), (0, 0, 0, 1, 1), (0, 0, 0, 1, -1)),
-    ((1, 0, 0, 1, -1),),
-    ((1, 0, 0, 1, 1),),
-    ((0, 1, 0, 0, -1), (1, 1, 0, 0, -1), (0, 1, 0, 1, 1), (1, 1, 0, 1, 1)),
-    ((1, 1, 0, 1, -1), (0, 1, 0, 1, -1)),
-    ((0, -1, 0, 1, 1), (1, -1, 0, 1, 1), (1, -1, 0, 1, -1)),
-    ((0, 2, 0, 1, -1), (0, 2, 0, 1, 1), (1, 2, 0, 1, 1), (1, 2, 0, 1, -1)),
-    ((0, -1, 0, 1, -1), (3, 0, 0, 0, 1), (2, 0, 0, 0, 1)),
-    ((2, 0, 0, 0, -1), (3, 0, 0, 0, -1), (0, 0, -1, 1, 1), (0, 2, 1, 1, -1), (1, 0, -1, 1, 1), (1, 1, 1, 1, -1)),
-    ((1, 2, -1, 1, 1), (0, 1, -1, 1, 1)),
-    ((2, 1, 0, 0, -1), (3, 1, 0, 0, -1)),
-    ((1, -1, 1, 1, -1), (0, -1, 1, 1, -1), (2, 0, 0, 1, 1), (3, 0, 0, 1, 1), (2, 1, 0, 1, 1)),
-    ((3, 0, 0, 1, -1), (2, 0, 0, 1, -1), (3, 1, 0, 1, 1), (2, -1, 0, 1, 1), (3, -1, 0, 1, 1)),
-    ((3, 2, 0, 1, -1), (2, 2, 0, 1, -1), (2, 2, 0, 1, 1), (3, 2, 0, 1, 1), (3, 1, 0, 1, -1), (2, 1, 0, 1, -1), (3, -1, 0, 1, -1)),
-    ((2, -1, 0, 1, -1), (2, 0, -1, 1, 1), (3, 0, -1, 1, 1), (2, 1, -1, 1, 1), (3, 1, -1, 1, 1)),
-    ((2, 2, 1, 1, -1), (3, 2, 1, 1, -1), (2, -1, -1, 1, 1), (3, -1, -1, 1, 1)),
+    ((1, 0, 0, 1, 1), (1, 0, 0, 1, -1)),
+    (),
+    ((1, -1, 0, 0, 1), (0, -1, 0, 0, 1), (0, 1, 0, 1, -1), (1, 1, 0, 1, -1)),
+    ((0, 1, 0, 1, 1), (0, -1, 0, 1, -1), (1, 1, 0, 1, 1), (1, -1, 0, 1, -1)),
+    (),
+    ((0, -1, 0, 1, 1), (1, -1, 0, 1, 1), (3, 0, 0, 0, -1), (2, 0, 0, 0, -1), (0, 0, 1, 1, -1), (1, 0, 1, 1, -1)),
+    ((0, 2, 0, 1, 1), (1, 2, 0, 1, 1), (0, 2, 0, 1, -1), (1, 2, 0, 1, -1)),
+    ((3, 0, 0, 0, 1), (2, 0, 0, 0, 1)),
+    ((0, 1, -1, 1, 1), (0, -1, 1, 1, -1), (1, 1, -1, 1, 1), (1, -1, 1, 1, -1)),
+    ((0, 2, -1, 1, 1), (1, 2, -1, 1, 1), (3, 1, 0, 0, -1), (2, 1, 0, 0, -1)),
+    ((2, 0, 0, 1, -1), (3, 0, 0, 1, -1), (2, 0, 0, 1, 1), (2, 1, 0, 1, -1), (3, 0, 0, 1, 1), (3, 1, 0, 1, -1)),
+    ((2, 1, 0, 1, 1), (2, -1, 0, 1, -1), (3, 1, 0, 1, 1), (3, -1, 0, 1, -1)),
+    ((2, 2, 0, 1, 1), (2, 2, 0, 1, -1), (3, 2, 0, 1, 1), (3, 2, 0, 1, -1), (2, -1, 0, 1, 1), (3, -1, 0, 1, 1)),
+    ((2, 0, 1, 1, -1), (3, 0, 1, 1, -1), (2, 1, 1, 1, -1), (3, 1, 1, 1, -1)),
+    ((2, 2, -1, 1, 1), (3, 2, -1, 1, 1), (2, -1, 1, 1, -1), (3, -1, 1, 1, -1)),
     (),
     (),
     (),
@@ -62,18 +62,18 @@
     ((0, -1, 0), (0, 1, 0), (1, -1, 0), (1, 1, 0)),
     (),
     ((0, 0, -1), (0, 0, 1)),
-    ((1, 0, 1),),
-    ((1, 0, -1), (0, 2, 0), (1, 2, 0)),
-    ((0, 1, -1), (1, 1, -1), (1, 1, 1), (0, 1, 1)),
-    ((0, -1, -1), (1, -1, -1), (1, -1, 1), (0, 2, 1)),
-    ((0, 2, -1), (1, 2, -1)),
-    ((1, 2, 1), (0, -1, 1), (3, -1, 0), (2, -1, 0), (2, 1, 0), (3, 1, 0)),
-    (),
-    ((0, 0, 2), (1, 0, 2), (1, 1, 2), (0, 2, 2)),
-    ((2, 2, 0), (3, 2, 0), (0, 1, 2), (1, 2, 2), (1, -1, 2), (0, -1, 2)),
-    ((2, 0, -1), (3, 0, -1), (2, 1, -1), (3, 1, -1), (3, 0, 1), (2, 0, 1), (2, -1, -1), (3, -1, -1)),
-    ((3, 2, 1), (2, 2, 1), (2, 2, -1), (3, 2, -1), (3, 1, 1), (2, 1, 1), (2, 0, 2), (3, 0, 2), (3, -1, 1)),
-    ((2, -1, 1), (2, 1, 2), (3, 1, 2), (3, -1, 2)),
+    ((1, 0, -1), (1, 0, 1)),
+    (),
+    ((1, 2, 0), (0, 1, 1), (0, 2, 0), (1, 1, 1)),
+    ((0, 1, -1), (0, -1, 1), (1, 1, -1), (1, -1, 1), (3, 1, 0), (2, 1, 0)),
+    ((0, -1, -1), (1, -1, -1)),
+    ((0, 0, 2), (1, 0, 2), (0, 2, -1), (1, 2, -1)),
+    ((0, 2, 1), (3, -1, 0), (1, 2, 1), (2, -1, 0)),
+    ((0, 1, 2), (0, -1, 2), (1, 1, 2), (1, -1, 2)),
+    ((3, 2, 0), (2, 2, 0), (0, 2, 2), (1, 2, 2)),
+    ((2, 0, 1), (3, 0, 1), (2, 0, -1), (2, 1, 1), (3, 0, -1), (3, 1, 1)),
+    ((2, 1, -1), (2, -1, 1), (3, 1, -1), (3, -1, 1), (2, 2, -1), (2, 2, 1), (3, 2, -1), (3, 2, 1), (2, -1, -1), (3, -1, -1), (2, 0, 2)),
+    ((3, 0, 2), (2, 1, 2), (3, 1, 2), (3, -1, 2)),
     ((2, 2, 2), (3, 2, 2), (2, -1, 2)),
     (),
     (),

time: 74 us -> 73 us (0.986)
  Pallas kernels: 72.5 us -> 71.5 us
    pallas_call x1, Pallas kernels: 72.5 us -> 71.5 us  [on_device(): pl.pallas_call(kernel, out_shape=pltpu.VMEM((R, DM), BF16), in_specs=[any...]
where the time goes in v7:
time: 73 us; the launch traced here: 72.9 us
  Pallas kernels  71.5 us (98%)
  local copies, waits for them, and re-layouts  0.73 us (1%)
    pallas_call x1, Pallas kernels, on_device(): pl.pallas_call(kernel, out_shape=pltpu.VMEM((R, DM), BF16), in_specs=[any...  71.5 us

profile of v7, /device:TPU:1, one launch (start us, length us, event | category | flops | bytes accessed | tf_op | source)
XLA Modules:
  0.0 72.9 jit_solution(1951686181166373402)
XLA Ops:
  0.7 71.5 %shard_map.217 = bf16[80,2048]{1,0:T(8,128)(2,1)S(1)} custom-call(bf16[80,2048]{1,0:T(8,128)(2,1)} %res_in.1, bf16[640,128]{1,0:T(8,128)(2,1)} %vs_in.1, bf16[640,128]{1,0:T(8,128)(2,1)} %vl_in.1, bf16[640,128]{1,0:T(8,128)(2,1)} %gs_in.1, bf16[640,128]{1,0:T(8,128)(2,1)} %gl_in.1, bf16[2560,128]{1,0:T(8,128)(2,1)} %bitcast.13, bf16[128,2048]{1,0:T(8,128)(2,1)} %ws_in.1, ...), custom_call_target="tpu_custom_call" | custom-call | tf_op jit(solution)/shard_map/pallas_call | solution.py:723
  72.1 0.7 copy.25

commit v8 on v7

--- a/solution.py
+++ b/solution.py
@@ -30,9 +30,9 @@
 COLUMNS = (
     ((0, 0), (1, 0), (0, 1), (-1, 0)),
     ((0, -1), (1, 1)),
-    ((1, -1), (-1, 1), (-1, -1), (2, 0)),
-    ((0, 2), (1, 2), (2, 1), (-1, 2)),
-    ((2, -1), (2, 2)),
+    ((1, -1), (-1, 1), (2, 0), (-1, -1)),
+    ((0, 2), (2, 1), (1, 2), (2, -1)),
+    ((2, 2), (-1, 2)),
 )
 SENDS = (
     ((0, 0, 0, 0, 1), (0, 0, 0, 0, -1), (1, 0, 0, 0, 1), (1, 0, 0, 0, -1), (0, 0, 0, 1, 1), (0, 0, 0, 1, -1)),
@@ -57,24 +57,24 @@
     (),
 )
 SHARES = (
+    (),
+    (),
+    ((0, -1, 0), (0, 1, 0), (1, -1, 0), (1, 1, 0)),
     ((0, 0, 0), (1, 0, 0), (2, 0, 0), (3, 0, 0)),
-    (),
-    ((0, -1, 0), (0, 1, 0), (1, -1, 0), (1, 1, 0)),
-    (),
     ((0, 0, -1), (0, 0, 1)),
     ((1, 0, -1), (1, 0, 1)),
     (),
-    ((1, 2, 0), (0, 1, 1), (0, 2, 0), (1, 1, 1)),
-    ((0, 1, -1), (0, -1, 1), (1, 1, -1), (1, -1, 1), (3, 1, 0), (2, 1, 0)),
-    ((0, -1, -1), (1, -1, -1)),
-    ((0, 0, 2), (1, 0, 2), (0, 2, -1), (1, 2, -1)),
+    ((1, 2, 0), (0, 1, 1), (0, 2, 0), (1, 1, 1), (0, 1, -1), (0, -1, 1)),
+    ((1, 1, -1), (1, -1, 1), (3, 1, 0), (2, 1, 0)),
+    ((0, -1, -1), (1, -1, -1), (0, 0, 2)),
+    ((1, 0, 2), (0, 2, -1), (1, 2, -1)),
     ((0, 2, 1), (3, -1, 0), (1, 2, 1), (2, -1, 0)),
     ((0, 1, 2), (0, -1, 2), (1, 1, 2), (1, -1, 2)),
     ((3, 2, 0), (2, 2, 0), (0, 2, 2), (1, 2, 2)),
     ((2, 0, 1), (3, 0, 1), (2, 0, -1), (2, 1, 1), (3, 0, -1), (3, 1, 1)),
-    ((2, 1, -1), (2, -1, 1), (3, 1, -1), (3, -1, 1), (2, 2, -1), (2, 2, 1), (3, 2, -1), (3, 2, 1), (2, -1, -1), (3, -1, -1), (2, 0, 2)),
-    ((3, 0, 2), (2, 1, 2), (3, 1, 2), (3, -1, 2)),
-    ((2, 2, 2), (3, 2, 2), (2, -1, 2)),
+    ((2, 1, -1), (2, -1, 1), (3, 1, -1), (3, -1, 1), (2, 2, -1), (2, 2, 1), (3, 2, -1), (3, 2, 1), (2, -1, -1), (2, 0, 2), (3, -1, -1)),
+    ((3, 0, 2), (2, 1, 2), (3, 1, 2), (2, -1, 2)),
+    ((2, 2, 2), (3, 2, 2), (3, -1, 2)),
     (),
     (),
 )
@@ -249,10 +249,6 @@
 
     pump(0)
 
-    wo_copies = [
-        go(remote(src, wo.at[c, rows], hp_sem.at[0, 8 + i], hp_sem.at[1, 8 + i], c=o))
-        for i, (src, rows) in enumerate(((ws_in, pl.ds(0, 128)), (wl_in, pl.ds(128, 128))))
-    ]
 
     for cp in fetched:
         cp.wait()
@@ -413,6 +409,11 @@
         second_pass(k)
     pl.when(c == 1)(functools.partial(start_all, later))
     pump(1)
+
+    wo_copies = [
+        go(remote(src, wo.at[c, rows], hp_sem.at[0, 8 + i], hp_sem.at[1, 8 + i], c=o))
+        for i, (src, rows) in enumerate(((ws_in, pl.ds(0, 128)), (wl_in, pl.ds(128, 128))))
+    ]
     inside = []
     for kind in range(2):
         states_in(st1, kind, 0)

time: 73 us -> 72.7 us (level)
  no operation moved by 1% of the time
where the time goes in v8:
time: 72.7 us; the launch traced here: 72.6 us
  Pallas kernels  71.2 us (98%)
  local copies, waits for them, and re-layouts  0.73 us (1%)
    pallas_call x1, Pallas kernels, on_device(): pl.pallas_call(kernel, out_shape=pltpu.VMEM((R, DM), BF16), in_specs=[any...  71.2 us

profile of v8, /device:TPU:1, one launch (start us, length us, event | category | flops | bytes accessed | tf_op | source)
XLA Modules:
  0.0 72.6 jit_solution(349254736950280001)
XLA Ops:
  0.7 71.2 %shard_map.217 = bf16[80,2048]{1,0:T(8,128)(2,1)S(1)} custom-call(bf16[80,2048]{1,0:T(8,128)(2,1)} %res_in.1, bf16[640,128]{1,0:T(8,128)(2,1)} %vs_in.1, bf16[640,128]{1,0:T(8,128)(2,1)} %vl_in.1, bf16[640,128]{1,0:T(8,128)(2,1)} %gs_in.1, bf16[640,128]{1,0:T(8,128)(2,1)} %gl_in.1, bf16[2560,128]{1,0:T(8,128)(2,1)} %bitcast.13, bf16[128,2048]{1,0:T(8,128)(2,1)} %ws_in.1, ...), custom_call_target="tpu_custom_call" | custom-call | tf_op jit(solution)/shard_map/pallas_call | solution.py:724
  71.9 0.7 %copy.25 = bf16[80,2048]{1,0:T(8,128)(2,1)} copy(bf16[80,2048]{1,0:T(8,128)(2,1)S(1)} %shard_map.217) | data formatting | bytes 655360

commit v9 on v8

--- a/solution.py
+++ b/solution.py
@@ -551,12 +551,14 @@
                 cols_e = pl.ds(role * H + e * 256, 256)
                 acc = dot(mine, wo[c, :, cols_e]) + dot(other, wo[o, :, cols_e])
                 parts[t][:, role, :, e * 256 : (e + 1) * 256] = acc.reshape(4, n, 256).astype(BF16)
+            if role == 0:
+                mixed[t].to_right(0, x2, 0)
+            else:
+                mixed[t].to_left(0, x2, 1)
 
     project(0)
-    mixed[0].relayed()
     mixed[0].direct()
     project(1)
-    mixed[1].relayed()
     pump(6)
     mixed[0].merge()
     mixed[1].direct()

time: 72.7 us -> 72.8 us (level)
  no operation moved by 1% of the time
where the time goes in v9:
time: 72.8 us; the launch traced here: 72.7 us
  Pallas kernels  71.3 us (98%)
  local copies, waits for them, and re-layouts  0.73 us (1%)
    pallas_call x1, Pallas kernels, on_device(): pl.pallas_call(kernel, out_shape=pltpu.VMEM((R, DM), BF16), in_specs=[any...  71.3 us

profile of v9, /device:TPU:1, one launch (start us, length us, event | category | flops | bytes accessed | tf_op | source)
XLA Modules:
  0.0 72.7 jit_solution(11422615869041316327)
XLA Ops:
  0.7 71.3 %shard_map.217 = bf16[80,2048]{1,0:T(8,128)(2,1)S(1)} custom-call(bf16[80,2048]{1,0:T(8,128)(2,1)} %res_in.1, bf16[640,128]{1,0:T(8,128)(2,1)} %vs_in.1, bf16[640,128]{1,0:T(8,128)(2,1)} %vl_in.1, bf16[640,128]{1,0:T(8,128)(2,1)} %gs_in.1, bf16[640,128]{1,0:T(8,128)(2,1)} %gl_in.1, bf16[2560,128]{1,0:T(8,128)(2,1)} %bitcast.13, bf16[128,2048]{1,0:T(8,128)(2,1)} %ws_in.1, ...), custom_call_target="tpu_custom_call" | custom-call | tf_op jit(solution)/shard_map/pallas_call | solution.py:726
  71.9 0.7 %copy.25 = bf16[80,2048]{1,0:T(8,128)(2,1)} copy(bf16[80,2048]{1,0:T(8,128)(2,1)S(1)} %shard_map.217) | data formatting | bytes 655360
